TPU v7x, 512 devices: a whole 4x8x8 slice. The times are simulated.
512 devices in a mesh: sp: 32 (over z, x), tp: 16 (over y, core).
Axes of the slice: x: 4, y: 8, z: 8, core: 2. Of those that a mesh axis runs over, the one named last changes fastest.
Arguments:
- pool_input: bfloat16 [4096, 1024], P('sp', 'tp'), may hold values from -12 to 12
- doc_ids: int32 [4096], P('sp'), may hold values from 0 to 7, as said below
- residual: bfloat16 [4096, 2048], P('sp', 'tp'), may hold values from -30 to 30
- pool_gain: float32 [1024], P('tp'), may hold values from 0.1 to 1.9
- out_proj: bfloat16 [1024, 2048], P('tp'), may hold values from -0.25 to 0.25
- norm_gain: float32 [2048], P('tp'), may hold values from 0.1 to 1.9
- routes: int32 [4096, 2], P('sp'), may hold values from 0 to 31, all different within a row; in each aligned block of 128 rows (0 to 127, 128 to 255, ...) at most 16 rows name the same one
- route_weights: float32 [4096, 2], P('sp'), may hold values from 0.2 to 1.2
- expert_gate: bfloat16 [32, 2048, 4096], P('sp', None, 'tp'), may hold values from -0.125 to 0.125
- expert_up: bfloat16 [32, 2048, 4096], P('sp', None, 'tp'), may hold values from -0.125 to 0.125
- expert_down: bfloat16 [32, 4096, 2048], P('sp', 'tp'), may hold values from -0.125 to 0.125
- shared_gate: bfloat16 [2048, 1024], P(None, 'tp'), may hold values from -0.125 to 0.125
- shared_up: bfloat16 [2048, 1024], P(None, 'tp'), may hold values from -0.125 to 0.125
- shared_down: bfloat16 [1024, 2048], P('tp'), may hold values from -0.25 to 0.25
Outputs:
- layer_out: bfloat16 [4096, 2048], P('sp', 'tp')
Inputs may be any that keep to these rules, and one draw needn't show every extreme that they name: `routes`: each row names 2 different experts. In each aligned block of 128 rows no expert is named by more than 16 rows; in some blocks one expert is named by exactly 16 rows. `doc_ids`: document numbers start at 0, never fall along the sequence and rise by one at each document's start.
All inputs are finite; a program needn't handle non-finite values.
Results may differ from a plain program's by a relative error of at most 0.015.
Values may be sent and summed in bfloat16 or wider, within the bound.
No kernel may reach another device: no remote copies, remote signals or barrier semaphores. Data moves between devices by JAX's collectives and lax.ppermute only.
A program may use at most 64 MiB of HBM per device.

v0:
```python
import jax
import jax.numpy as jnp
from jax import lax
from jax.sharding import PartitionSpec as P


def copy_for_each(value, axis):
    copies = jnp.broadcast_to(value, (lax.axis_size(axis), *value.shape))
    return lax.all_to_all(copies, axis, split_axis=0, concat_axis=0, tiled=True)


def gathered_once(value, axis):
    leaves = jax.tree.leaves(value)
    sequence = sorted(range(len(leaves)), key=lambda k: -leaves[k].size)
    width = (1, *leaves[sequence[0]].shape)[-1]
    lines = [
        jnp.pad(leaves[k].reshape(-1), (0, -leaves[k].size % width)).reshape(-1, width)
        for k in sequence
    ]
    both, at, found = (copy_for_each(jnp.concatenate(lines), axis), 0, {})
    for k, line in zip(sequence, lines):
        section = both[:, at : at + len(line)].reshape(len(both), -1)
        found[k] = section[:, : leaves[k].size].reshape(-1, *leaves[k].shape)
        at += len(line)
    numbers = iter(range(len(leaves)))
    return jax.tree.map(lambda _: found[next(numbers)], value)


def folded_in_pairs(pieces, combine):
    while len(jax.tree.leaves(pieces)[0]) > 1:
        pieces = jax.vmap(combine)(
            *(jax.tree.map(lambda part: part[side::2], pieces) for side in (0, 1))
        )
    return jax.tree.map(lambda part: part[0], pieces)


def carried_in(value, axis, combine, identity):
    size, position = (lax.axis_size(axis), lax.axis_index(axis))
    passed = jnp.arange(size) < position

    def kept(part, zero, own):
        part = jnp.where(
            passed.reshape(-1, *(1 for _ in own.shape)), part, jnp.asarray(zero, own.dtype)
        )
        return part

    pieces = gathered_once(value, axis)
    return folded_in_pairs(jax.tree.map(kept, pieces, identity, value), combine)


def from_behind(value, axis, by):
    size = lax.axis_size(axis)
    pairs = [(i, i + by) for i in range(size) if 0 <= i + by < size]
    return lax.ppermute(value, axis, pairs)


def split_up(value, dim, size):
    before, after = (value.shape[:dim], value.shape[dim + 1 :])
    return jnp.moveaxis(value.reshape(*before, size, -1, *after), dim, 0)


def sum_at_owner(value, axis, dim):
    blocks = split_up(value, dim, lax.axis_size(axis))
    arrived = lax.all_to_all(blocks, axis, split_axis=0, concat_axis=0, tiled=True)
    return arrived.astype(jnp.float32).sum(axis=0)


def over_copies(value, axis):
    return copy_for_each(value, axis).sum(axis=0)


def laid_out(blocks, dim):
    blocks = jnp.moveaxis(blocks, 0, dim)
    shape = blocks.shape
    return blocks.reshape(*shape[:dim], shape[dim] * shape[dim + 1], *shape[dim + 2 :])


def gathered_copies(value, axis, dim):
    blocks = copy_for_each(value, axis)
    return laid_out(blocks, dim)


def join_documents(earlier, later):
    earlier_sum, earlier_length, earlier_first, earlier_last, earlier_inner = earlier
    later_sum, later_length, later_first, later_last, later_inner = later
    boundary = later_first != earlier_last
    restart = (later_inner > 0) | boundary
    merged = (
        jnp.where(restart, later_sum, earlier_sum + later_sum),
        jnp.where(restart, later_length, earlier_length + later_length),
        earlier_first,
        later_last,
        jnp.maximum(jnp.maximum(earlier_inner, later_inner), boundary.astype(jnp.float32)),
    )
    earlier_empty = earlier_first < 0
    later_empty = later_first < 0
    return tuple(
        (
            jnp.where(earlier_empty, second, jnp.where(later_empty, first_value, joined))
            for first_value, second, joined in zip(earlier, later, merged)
        )
    )


def expert_terms(arrived, gate_weight, up_weight, down_weight):
    local_experts = gate_weight.shape[0]
    sources = arrived.shape[0] // local_experts
    grouped = arrived.reshape(sources, local_experts, arrived.shape[1], arrived.shape[2])
    gate = jnp.einsum("secd,edf->secf", grouped, gate_weight, preferred_element_type=jnp.float32)
    upper = jnp.einsum("secd,edf->secf", grouped, up_weight, preferred_element_type=jnp.float32)
    hidden = (jax.nn.silu(gate) * upper).astype(jnp.bfloat16)
    output = jnp.einsum("secf,efd->secd", hidden, down_weight, preferred_element_type=jnp.float32)
    return output.reshape(arrived.shape[0], arrived.shape[1], down_weight.shape[2])


def body(
    pool_input,
    doc_ids,
    residual,
    pool_gain,
    out_proj,
    norm_gain,
    routes,
    route_weights,
    expert_gate,
    expert_up,
    expert_down,
    shared_gate,
    shared_up,
    shared_down,
):
    row_count, channels = pool_input.shape
    values = pool_input.astype(jnp.float32)
    positions = jnp.arange(row_count, dtype=jnp.int32)
    inner_begin = jnp.concatenate([jnp.zeros((1,), bool), doc_ids[1:] != doc_ids[:-1]])
    running = jnp.cumsum(values[:, 3::4], axis=0)
    shifted = jnp.concatenate([jnp.zeros((1, running.shape[1]), jnp.float32), running], 0)
    inner_last = jnp.max(jnp.where(inner_begin, positions, 0))
    own_terms = (
        running[-1] - shifted[inner_last],
        (row_count - inner_last).astype(jnp.float32),
        doc_ids[0].astype(jnp.float32),
        doc_ids[-1].astype(jnp.float32),
        jnp.any(inner_begin).astype(jnp.float32),
    )
    identity = (
        jnp.zeros((running.shape[1],), jnp.float32),
        jnp.zeros((), jnp.float32),
        jnp.full((), -1.0, jnp.float32),
        jnp.full((), -1.0, jnp.float32),
        jnp.zeros((), jnp.float32),
    )
    before = carried_in(own_terms, "sp", join_documents, identity)
    fresh = (before[2] < 0) | (doc_ids[0].astype(jnp.float32) != before[3])
    begins = jnp.concatenate([fresh[None], inner_begin[1:]])
    doc_start = lax.cummax(jnp.where(begins, positions, -1), axis=0)
    found = doc_start >= 0
    carry_sum = jnp.where(fresh, 0.0, before[0])
    carry_length = jnp.where(fresh, 0.0, before[1])
    length = jnp.where(
        found,
        (positions - doc_start + 1).astype(jnp.float32),
        carry_length + (positions + 1).astype(jnp.float32),
    )
    start_rows = jnp.take(shifted, jnp.maximum(doc_start, 0), axis=0)
    doc_sum = jnp.where(found[:, None], running - start_rows, carry_sum[None, :] + running)
    doc_mean = doc_sum / length[:, None]
    rim = from_behind(pool_input[row_count - 15 :], "sp", 1)
    extended = jnp.concatenate([rim, pool_input], 0).astype(jnp.float32)
    scale_index = jnp.arange(channels, dtype=jnp.int32) % 4
    window_size = jnp.where(scale_index == 0, 2.0, jnp.where(scale_index == 1, 8.0, 16.0))
    window_total = jnp.zeros((row_count, channels), jnp.float32)
    for offset in range(16):
        inside = (offset < length[:, None]) & (offset < window_size[None, :])
        window_total = window_total + jnp.where(
            inside, extended[15 - offset : 15 - offset + row_count], 0.0
        )
    window_mean = window_total / jnp.minimum(length[:, None], window_size[None, :])
    pool_mean = jnp.concatenate(
        [window_mean.reshape(row_count, channels // 4, 4)[..., :3], doc_mean[..., None]], -1
    )
    pool_mean = pool_mean.reshape(row_count, channels)
    pooled = ((pool_mean - values) * pool_gain).astype(jnp.bfloat16)
    terms = jnp.dot(pooled, out_proj, preferred_element_type=jnp.float32)
    projected = sum_at_owner(terms.astype(jnp.bfloat16), "tp", 1).astype(jnp.bfloat16)
    hidden_state = residual.astype(jnp.float32) + projected.astype(jnp.float32)
    squares = over_copies(jnp.sum(hidden_state * hidden_state, axis=1), "tp")
    model_width = residual.shape[1] * lax.axis_size("tp")
    scaling = lax.rsqrt(squares / model_width + 1e-06)
    normed_columns = (hidden_state * scaling[:, None] * norm_gain).astype(jnp.bfloat16)
    normed = gathered_copies(normed_columns, "tp", 1)
    shared_gate_out = jnp.dot(normed, shared_gate, preferred_element_type=jnp.float32)
    shared_up_out = jnp.dot(normed, shared_up, preferred_element_type=jnp.float32)
    shared_hidden = (jax.nn.silu(shared_gate_out) * shared_up_out).astype(jnp.bfloat16)
    shared_terms = jnp.dot(shared_hidden, shared_down, preferred_element_type=jnp.float32)
    group_size = lax.axis_size("tp")
    experts = expert_gate.shape[0] * lax.axis_size("sp")
    top = routes.shape[1]
    capacity = group_size * max(1, 2 * row_count * top // (experts * group_size))
    flat_experts = routes.reshape(-1)
    onehot = (flat_experts[:, None] == jnp.arange(experts, dtype=jnp.int32)[None, :]).astype(
        jnp.int32
    )
    ranks = jnp.sum((jnp.cumsum(onehot, axis=0) - 1) * onehot, axis=1)
    slots = flat_experts * capacity + ranks
    token_index = jnp.arange(row_count * top, dtype=jnp.int32) // top
    slot_token = jnp.full((experts * capacity,), row_count, jnp.int32).at[slots].set(token_index)
    with_blank = jnp.concatenate([normed, jnp.zeros((1, normed.shape[1]), jnp.bfloat16)], 0)
    outgoing = jnp.take(with_blank, slot_token, axis=0).reshape(experts, capacity, normed.shape[1])
    expert_parts = expert_terms(
        lax.all_to_all(outgoing, "sp", split_axis=0, concat_axis=0, tiled=True),
        expert_gate,
        expert_up,
        expert_down,
    )
    routed_sum, shared_sum = (
        sum_at_owner(expert_parts.astype(jnp.bfloat16), "tp", 2),
        sum_at_owner(shared_terms[None].astype(jnp.bfloat16), "tp", 2),
    )
    returned = lax.all_to_all(
        routed_sum.astype(jnp.bfloat16), "sp", split_axis=0, concat_axis=0, tiled=True
    )
    flat_back = returned.reshape(experts * capacity, returned.shape[2])
    picked = (
        jnp.take(flat_back, slots, axis=0).astype(jnp.float32) * route_weights.reshape(-1)[:, None]
    )
    routed = jnp.sum(picked.reshape(row_count, top, flat_back.shape[1]), axis=1)
    shared_out = shared_sum[0].astype(jnp.bfloat16).astype(jnp.float32)
    return (hidden_state + routed + shared_out).astype(jnp.bfloat16)


def solution(mesh):
    placed = (
        P("sp", "tp"),
        P("sp"),
        P("sp", "tp"),
        P("tp"),
        P("tp", None),
        P("tp"),
        P("sp", None),
        P("sp", None),
        P("sp", None, "tp"),
        P("sp", None, "tp"),
        P("sp", "tp", None),
        P(None, "tp"),
        P(None, "tp"),
        P("tp", None),
    )
    return jax.shard_map(body, mesh=mesh, in_specs=placed, out_specs=P("sp", "tp"), check_vma=False)
```

profile of v0, /device:TPU:1, one launch (start us, length us, event | category | flops | bytes accessed | tf_op | source)
XLA Modules:
  0.0 278.8 jit_solution(7757600359169477122)
XLA Ops:
  0.0 1.5 fusion.75
  9.9 13.7 %all-to-all-start = ((f32[32,5,16]{2,1,0:T(8,128)}), f32[32,5,16]{2,1,0:T(8,128)S(1)}, u32[]{:S(2)}, u32[]{:S(2)}) async-start(f32[32,5,16]{2,1,0:T(8,128)} %broadcast_in_dim.215), calls=%async_computation | async-start | bytes 262144 | tf_op jit(solution)/shard_map/all_to_all | solution.py:9
  24.5 3.1 %collective-permute-start = (bf16[15,64]{0,1:T(8,128)(2,1)S(1)}, bf16[15,64]{0,1:T(8,128)(2,1)S(1)}, u32[]{:S(2)}, u32[]{:S(2)}) collective-permute-start(bf16[15,64]{0,1:T(8,128)(2,1)S(1)} %slice.315), channel_id=1, source_target_pairs={{0,16},{16,32},{32,48},{48,64},{64,80},{80,96},{96,112},{112,128},... | collective-permute-start | bytes 5768 | tf_op jit(solution)/shard_map/ppermute | solution.py:54
  29.2 3.8 %all-to-all-done = f32[32,5,16]{2,1,0:T(8,128)S(1)} async-done(((f32[32,5,16]{2,1,0:T(8,128)}), f32[32,5,16]{2,1,0:T(8,128)S(1)}, u32[]{:S(2)}, u32[]{:S(2)}) %all-to-all-start) | async-done | bytes 10272 | tf_op jit(solution)/shard_map/all_to_all | solution.py:9
  52.5 9.2 %all-to-all-start.1 = ((bf16[16,128,128]{2,1,0:T(8,128)(2,1)}), bf16[16,128,128]{2,1,0:T(8,128)(2,1)S(1)}, u32[]{:S(2)}, u32[]{:S(2)}) async-start(bf16[16,128,128]{2,1,0:T(8,128)(2,1)} %bitcast.147), calls=%async_computation.1 | async-start | bytes 1048576 | tf_op jit(solution)/shard_map/all_to_all | solution.py:64
  62.6 16.3 %all-to-all-done.1 = bf16[16,128,128]{2,1,0:T(8,128)(2,1)S(1)} async-done(((bf16[16,128,128]{2,1,0:T(8,128)(2,1)}), bf16[16,128,128]{2,1,0:T(8,128)(2,1)S(1)}, u32[]{:S(2)}, u32[]{:S(2)}) %all-to-all-start.1) | async-done | bytes 524320 | tf_op jit(solution)/shard_map/all_to_all | solution.py:64
  79.7 3.4 %all-to-all-start.2 = ((f32[16,1,128]{2,1,0:T(1,128)}), f32[16,1,128]{2,1,0:T(1,128)S(1)}, u32[]{:S(2)}, u32[]{:S(2)}) async-start(f32[16,1,128]{2,1,0:T(1,128)} %broadcast_in_dim.248), calls=%async_computation.2 | async-start | bytes 16384 | tf_op jit(solution)/shard_map/all_to_all | solution.py:9
  83.7 6.0 %all-to-all-done.2 = f32[16,1,128]{2,1,0:T(1,128)S(1)} async-done(((f32[16,1,128]{2,1,0:T(1,128)}), f32[16,1,128]{2,1,0:T(1,128)S(1)}, u32[]{:S(2)}, u32[]{:S(2)}) %all-to-all-start.2) | async-done | bytes 8224 | tf_op jit(solution)/shard_map/all_to_all | solution.py:9
  90.7 4.0 %all-to-all-start.3 = ((bf16[16,128,128]{2,1,0:T(8,128)(2,1)}), bf16[16,128,128]{2,1,0:T(8,128)(2,1)S(1)}, u32[]{:S(2)}, u32[]{:S(2)}) async-start(bf16[16,128,128]{2,1,0:T(8,128)(2,1)} %broadcast_in_dim.249), calls=%async_computation.3 | async-start | bytes 1048576 | tf_op jit(solution)/shard_map/all_to_all | solution.py:9
  96.3 15.7 %all-to-all-done.3 = bf16[16,128,128]{2,1,0:T(8,128)(2,1)S(1)} async-done(((bf16[16,128,128]{2,1,0:T(8,128)(2,1)}), bf16[16,128,128]{2,1,0:T(8,128)(2,1)S(1)}, u32[]{:S(2)}, u32[]{:S(2)}) %all-to-all-start.3) | async-done | bytes 524320 | tf_op jit(solution)/shard_map/all_to_all | solution.py:9
  112.9 3.3 %gather_fusion.1 = bf16[512,2048]{1,0:T(8,128)(2,1)} fusion(bf16[129,2048]{1,0:T(8,128)(2,1)S(1)} %concatenate.40, s32[1024]{0:T(1024)S(1)} %pad_clamp_fusion.1), kind=kCustom, calls=%fused_computation.1 | custom fusion | bytes 4196352 | tf_op jit(solution)/shard_map/jit(_take)/gather | solution.py:209
  116.3 1.8 broadcast_select_fusion
  118.1 57.3 %all_to_all.41 = bf16[32,16,2048]{2,1,0:T(8,128)(2,1)S(1)} all-to-all(bf16[32,16,2048]{2,1,0:T(8,128)(2,1)S(1)} %broadcast_select_fusion), channel_id=1, replica_groups=mesh['sp'=32,'tp'=16] {'sp'}, dimensions={0} | all-to-all | bytes 4194304 | tf_op jit(solution)/shard_map/all_to_all | solution.py:211
  175.4 1.5 convolution_bitcast_fusion.1
  176.9 5.0 %convolution_convert_fusion = bf16[32,16,2048]{2,1,0:T(8,128)(2,1)} fusion(bf16[32,16,2048]{2,1,0:T(8,128)(2,1)S(1)} %all_to_all.41, bf16[1,256,2048]{2,1,0:T(8,128)(2,1)S(1)} %copy-done, bf16[1,2048,256]{2,1,0:T(8,128)(2,1)} %param.23, f32[32,1,16,256]{3,2,0,1:T(8,128)} %convolution_bitcast_fusion.1), kind=kOutput, calls=%fused_computation.4 | convolution fusion | flops 1075576832 | bytes 6815744 | tf_op jit(solution)/shard_map/secf,efd->secd/dot_general | solution.py:112
  182.0 2.2 copy.85
  184.2 1.9 copy.95
  186.1 4.0 %all-to-all-start.5 = ((bf16[16,32,16,128]{3,2,1,0:T(8,128)(2,1)}), bf16[16,32,16,128]{3,2,1,0:T(8,128)(2,1)S(1)}, u32[]{:S(2)}, u32[]{:S(2)}) async-start(bf16[16,32,16,128]{3,2,1,0:T(8,128)(2,1)} %bitcast.151), calls=%async_computation.5 | async-start | bytes 4194304 | tf_op jit(solution)/shard_map/all_to_all | solution.py:64
  191.5 2.8 fusion.1
  196.4 42.8 %all-to-all-done.5 = bf16[16,32,16,128]{3,2,1,0:T(8,128)(2,1)S(1)} async-done(((bf16[16,32,16,128]{3,2,1,0:T(8,128)(2,1)}), bf16[16,32,16,128]{3,2,1,0:T(8,128)(2,1)S(1)}, u32[]{:S(2)}, u32[]{:S(2)}) %all-to-all-start.5) | async-done | bytes 2097184 | tf_op jit(solution)/shard_map/all_to_all | solution.py:64
  239.2 4.8 %all-to-all-start.7 = ((bf16[16,1,128,128]{3,2,1,0:T(8,128)(2,1)}), bf16[16,1,128,128]{3,2,1,0:T(8,128)(2,1)}, u32[]{:S(2)}, u32[]{:S(2)}) async-start(bf16[16,1,128,128]{3,2,1,0:T(8,128)(2,1)} %bitcast.155), calls=%async_computation.7 | async-start | bytes 1048576 | tf_op jit(solution)/shard_map/all_to_all | solution.py:64
  245.2 16.1 %all-to-all-done.7 = bf16[16,1,128,128]{3,2,1,0:T(8,128)(2,1)} async-done(((bf16[16,1,128,128]{3,2,1,0:T(8,128)(2,1)}), bf16[16,1,128,128]{3,2,1,0:T(8,128)(2,1)}, u32[]{:S(2)}, u32[]{:S(2)}) %all-to-all-start.7) | async-done | bytes 524320 | tf_op jit(solution)/shard_map/all_to_all | solution.py:64
  261.4 5.2 %all-to-all-start.6 = ((bf16[32,16,128]{2,1,0:T(8,128)(2,1)}), bf16[32,16,128]{2,1,0:T(8,128)(2,1)S(1)}, u32[]{:S(2)}, u32[]{:S(2)}) async-start(bf16[32,16,128]{2,1,0:T(8,128)(2,1)} %reduce_sum.82), calls=%async_computation.6 | async-start | bytes 262144 | tf_op jit(solution)/shard_map/all_to_all | solution.py:220
  267.9 9.0 %all-to-all-done.6 = bf16[32,16,128]{2,1,0:T(8,128)(2,1)S(1)} async-done(((bf16[32,16,128]{2,1,0:T(8,128)(2,1)}), bf16[32,16,128]{2,1,0:T(8,128)(2,1)S(1)}, u32[]{:S(2)}, u32[]{:S(2)}) %all-to-all-start.6) | async-done | bytes 131104 | tf_op jit(solution)/shard_map/all_to_all | solution.py:220
  (175 shorter events, 30.3 us)
Async XLA Ops:
  0.0 176.9 %copy-start = (bf16[1,256,2048]{2,1,0:T(8,128)(2,1)S(1)}, bf16[1,256,2048]{2,1,0:T(8,128)(2,1)}, u32[]{:S(2)}) copy-start(bf16[1,256,2048]{2,1,0:T(8,128)(2,1)} %param.24) | copy-start | bytes 3145732
  0.0 51.2 %copy-start.5 = (bf16[128,64]{0,1:T(8,128)(2,1)S(1)}, bf16[128,64]{0,1:T(8,128)(2,1)}, u32[]{:S(2)}) copy-start(bf16[128,64]{0,1:T(8,128)(2,1)} %param.14) | copy-start | bytes 49156
  0.0 51.2 %copy-start.3 = (bf16[64,2048]{1,0:T(8,128)(2,1)S(1)}, bf16[64,2048]{1,0:T(8,128)(2,1)}, u32[]{:S(2)}) copy-start(bf16[64,2048]{1,0:T(8,128)(2,1)} %param.18) | copy-start | bytes 786436
  0.0 51.2 %copy-start.9 = (f32[64]{0:T(128)S(1)}, f32[64]{0:T(128)}, u32[]{:S(2)}) copy-start(f32[64]{0:T(128)} %param.17) | copy-start | bytes 772
  9.9 23.1 %all-to-all-start = ((f32[32,5,16]{2,1,0:T(8,128)}), f32[32,5,16]{2,1,0:T(8,128)S(1)}, u32[]{:S(2)}, u32[]{:S(2)}) async-start(f32[32,5,16]{2,1,0:T(8,128)} %broadcast_in_dim.215), calls=%async_computation | async-start | bytes 262144 | tf_op jit(solution)/shard_map/all_to_all | solution.py:9
  24.5 4.0 %collective-permute-start = (bf16[15,64]{0,1:T(8,128)(2,1)S(1)}, bf16[15,64]{0,1:T(8,128)(2,1)S(1)}, u32[]{:S(2)}, u32[]{:S(2)}) collective-permute-start(bf16[15,64]{0,1:T(8,128)(2,1)S(1)} %slice.315), channel_id=1, source_target_pairs={{0,16},{16,32},{32,48},{48,64},{64,80},{80,96},{96,112},{112,128},... | collective-permute-start | bytes 5768 | tf_op jit(solution)/shard_map/ppermute | solution.py:54
  44.8 16.9 %copy-start.6 = (s32[128,2]{0,1:T(2,128)S(1)}, s32[128,2]{0,1:T(2,128)}, u32[]{:S(2)}) copy-start(s32[128,2]{0,1:T(2,128)} %param.20) | copy-start | bytes 3076
  50.8 28.2 %copy-start.2 = (bf16[128,128]{1,0:T(8,128)(2,1)S(1)}, bf16[128,128]{1,0:T(8,128)(2,1)}, u32[]{:S(2)}) copy-start(bf16[128,128]{1,0:T(8,128)(2,1)} %param.16) | copy-start | bytes 98308
  51.1 38.6 %copy-start.8 = (f32[128]{0:T(128)S(1)}, f32[128]{0:T(128)}, u32[]{:S(2)}) copy-start(f32[128]{0:T(128)} %param.19) | copy-start | bytes 1540
  52.5 26.4 %all-to-all-start.1 = ((bf16[16,128,128]{2,1,0:T(8,128)(2,1)}), bf16[16,128,128]{2,1,0:T(8,128)(2,1)S(1)}, u32[]{:S(2)}, u32[]{:S(2)}) async-start(bf16[16,128,128]{2,1,0:T(8,128)(2,1)} %bitcast.147), calls=%async_computation.1 | async-start | bytes 1048576 | tf_op jit(solution)/shard_map/all_to_all | solution.py:64
  79.7 10.0 %all-to-all-start.2 = ((f32[16,1,128]{2,1,0:T(1,128)}), f32[16,1,128]{2,1,0:T(1,128)S(1)}, u32[]{:S(2)}, u32[]{:S(2)}) async-start(f32[16,1,128]{2,1,0:T(1,128)} %broadcast_in_dim.248), calls=%async_computation.2 | async-start | bytes 16384 | tf_op jit(solution)/shard_map/all_to_all | solution.py:9
  90.7 21.3 %all-to-all-start.3 = ((bf16[16,128,128]{2,1,0:T(8,128)(2,1)}), bf16[16,128,128]{2,1,0:T(8,128)(2,1)S(1)}, u32[]{:S(2)}, u32[]{:S(2)}) async-start(bf16[16,128,128]{2,1,0:T(8,128)(2,1)} %broadcast_in_dim.249), calls=%async_computation.3 | async-start | bytes 1048576 | tf_op jit(solution)/shard_map/all_to_all | solution.py:9
  112.0 0.8 copy-start.1
  118.1 57.3 %copy-start.10 = (bf16[1,2048,256]{2,1,0:T(8,128)(2,1)S(1)}, bf16[1,2048,256]{2,1,0:T(8,128)(2,1)}, u32[]{:S(2)}) copy-start(bf16[1,2048,256]{2,1,0:T(8,128)(2,1)} %param.22) | copy-start | bytes 3145732
  186.1 5.4 %copy-start.4 = (bf16[64,2048]{1,0:T(8,128)(2,1)S(1)}, bf16[64,2048]{1,0:T(8,128)(2,1)}, u32[]{:S(2)}) copy-start(bf16[64,2048]{1,0:T(8,128)(2,1)} %param.27) | copy-start | bytes 786436
  186.1 53.1 %all-to-all-start.5 = ((bf16[16,32,16,128]{3,2,1,0:T(8,128)(2,1)}), bf16[16,32,16,128]{3,2,1,0:T(8,128)(2,1)S(1)}, u32[]{:S(2)}, u32[]{:S(2)}) async-start(bf16[16,32,16,128]{3,2,1,0:T(8,128)(2,1)} %bitcast.151), calls=%async_computation.5 | async-start | bytes 4194304 | tf_op jit(solution)/shard_map/all_to_all | solution.py:64
  196.4 70.3 %copy-start.7 = (f32[128,2]{0,1:T(2,128)S(1)}, f32[128,2]{0,1:T(2,128)}, u32[]{:S(2)}) copy-start(f32[128,2]{0,1:T(2,128)} %param.21) | copy-start | bytes 3076
  239.2 22.1 %all-to-all-start.7 = ((bf16[16,1,128,128]{3,2,1,0:T(8,128)(2,1)}), bf16[16,1,128,128]{3,2,1,0:T(8,128)(2,1)}, u32[]{:S(2)}, u32[]{:S(2)}) async-start(bf16[16,1,128,128]{3,2,1,0:T(8,128)(2,1)} %bitcast.155), calls=%async_computation.7 | async-start | bytes 1048576 | tf_op jit(solution)/shard_map/all_to_all | solution.py:64
  261.4 15.6 %all-to-all-start.6 = ((bf16[32,16,128]{2,1,0:T(8,128)(2,1)}), bf16[32,16,128]{2,1,0:T(8,128)(2,1)S(1)}, u32[]{:S(2)}, u32[]{:S(2)}) async-start(bf16[32,16,128]{2,1,0:T(8,128)(2,1)} %reduce_sum.82), calls=%async_computation.6 | async-start | bytes 262144 | tf_op jit(solution)/shard_map/all_to_all | solution.py:220
where the time goes:
time: 280 us; the launch traced here: 279 us
  waiting for transfers between devices  110 us (39%)
  blocking collectives  57.3 us (20%)
  starting transfers between devices  47.4 us (17%)
  local copies, waits for them, and re-layouts  27.3 us (10%)
  between operations  14 us (5%)
  other arithmetic  11.3 us (4%)
  matrix products  11.1 us (4%)
    all_to_all x3, waiting for transfers between devices, sum_at_owner(): lax.all_to_all(blocks, axis, split_axis=0, concat_axis=0, tiled=True)  75.3 us
    all_to_all x1, blocking collectives, body(): lax.all_to_all(outgoing, 'sp', split_axis=0, concat_axis=0, tiled=True)  57.3 us
    all_to_all x3, waiting for transfers between devices, copy_for_each(): return lax.all_to_all(copies, axis, split_axis=0, concat_axis=0, tiled=True)  25.4 us
    all_to_all x3, starting transfers between devices, copy_for_each(): return lax.all_to_all(copies, axis, split_axis=0, concat_axis=0, tiled=True)  21.1 us
    all_to_all x3, starting transfers between devices, sum_at_owner(): lax.all_to_all(blocks, axis, split_axis=0, concat_axis=0, tiled=True)  18 us
    all_to_all x1, waiting for transfers between devices, body(): lax.all_to_all(routed_sum.astype(jnp.bfloat16), 'sp', split_axis=0, conca...  8.96 us
    slice x44, local copies, waits for them, and re-layouts, folded_in_pairs(): part[side::2]  5.8 us
  transfers between devices with their start and end apart: 8, of which 8 were waited for; matrix products, arithmetic and copies ran while one was open for 5% of the time, Pallas kernels for 0%

commit v1 on v0

v1 whole, which is shorter than its diff:
```python
import jax
import jax.numpy as jnp
from jax import lax
from jax.experimental import pallas as pl
from jax.experimental.pallas import tpu as pltpu
from jax.sharding import Mesh
from jax.sharding import PartitionSpec as P

F32 = jnp.float32
BF16 = jnp.bfloat16
SUM_LANE = 64
W_LANE = 80
META_LANE = 88


def exchanged(value, axis):
    return lax.all_to_all(value, axis, split_axis=0, concat_axis=0, tiled=True)


def three_parts(value):
    first = value.astype(BF16).astype(F32)
    second = (value - first).astype(BF16).astype(F32)
    third = (value - first - second).astype(BF16).astype(F32)
    return first, second, third


def iota(shape, dim):
    return lax.broadcasted_iota(jnp.int32, shape, dim)


def matmul(a, b):
    return jnp.dot(a, b, preferred_element_type=F32)


def opening(pool_ref, docs_ref, routes_ref, weights_ref, message_ref, slots_ref):
    rows, channels = pool_ref.shape
    square = (rows, rows)
    across = iota((channels, 128), 0)
    lane = iota((channels, 128), 1)
    spread = (lane == across) | ((across % 4 == 3) & (lane == SUM_LANE + across // 4))
    wide = matmul(pool_ref[...], spread.astype(F32).astype(BF16))
    docs = docs_ref[...].astype(F32)
    last_doc = docs[:, rows - 1 :]
    trailing = (docs == last_doc).astype(F32)
    sums = matmul(jnp.broadcast_to(trailing, (8, rows)).astype(BF16), wide.astype(BF16))[0:1]
    count = jnp.sum(trailing, axis=1, keepdims=True)

    columns = [jnp.broadcast_to(routes_ref[:, k : k + 1].astype(F32), square) for k in (0, 1)]
    lines = [column.T for column in columns]
    before = iota(square, 0) < iota(square, 1)

    def counted(mask):
        return jnp.sum(mask.astype(F32), axis=0, keepdims=True)

    first_rank = counted((columns[0] == lines[0]) & before)
    second_rank = counted(columns[0] == lines[1]) + counted((columns[1] == lines[1]) & before)
    first_slot = lines[0][0:1] * 16.0 + first_rank
    second_slot = lines[1][0:1] * 16.0 + second_rank
    slots_ref[...] = jnp.concatenate(
        [first_slot, second_slot, jnp.zeros((6, rows), F32)], axis=0
    )
    share = [
        jnp.broadcast_to(weights_ref[:, k : k + 1], square).T[0:1] for k in (0, 1)
    ]
    slot = iota((512, rows), 0).astype(F32)
    is_first = slot == first_slot
    is_second = slot == second_slot
    weight = jnp.sum(
        jnp.where(is_first, share[0], 0.0) + jnp.where(is_second, share[1], 0.0),
        axis=1,
        keepdims=True,
    )
    chosen_first = jnp.sum(is_first.astype(F32), axis=1, keepdims=True)

    row = iota((16, 128), 0)
    at = iota((16, 128), 1)
    parts = three_parts(sums)
    shared = jnp.where(at < channels, wide[rows - 16 :], 0.0)
    in_sums = (at >= SUM_LANE) & (at < SUM_LANE + 16)
    for k in range(3):
        shared = jnp.where(in_sums & (row == k), parts[k], shared)
    doc_high = jnp.floor(last_doc * (1.0 / 128.0))
    doc_low = last_doc - doc_high * 128.0
    for k, value in enumerate((count, doc_high, doc_low)):
        shared = jnp.where(at == META_LANE + k, value, shared)
    place = iota((512, 128), 1)
    message = jnp.broadcast_to(shared[None], (32, 16, 128)).reshape(512, 128)
    for k, value in enumerate((*three_parts(weight), chosen_first)):
        message = jnp.where(place == W_LANE + k, value, message)
    message_ref[...] = message.reshape(32, 16, 128).astype(BF16)


def pooling(
    index_ref, arrived_ref, pool_ref, docs_ref, gain_ref, project_ref, norm_ref, out_ref
):
    rows, channels = pool_ref.shape
    own = index_ref[0]
    docs = docs_ref[...].astype(F32)
    first_doc = docs[:, 0:1]
    arrived = arrived_ref[...].astype(F32)
    meta = arrived[:, 0:1]
    their_count = meta[:, :, META_LANE : META_LANE + 1]
    their_doc = (
        meta[:, :, META_LANE + 1 : META_LANE + 2] * 128.0
        + meta[:, :, META_LANE + 2 : META_LANE + 3]
    )
    block = iota((32, 1, 1), 0)
    joins = (block < own) & (their_doc == first_doc.reshape(1, 1, 1))
    carry_length = jnp.sum(jnp.where(joins, their_count, 0.0), axis=0)
    sums = jnp.sum(jnp.where(joins, arrived[:, 0:8], 0.0), axis=0)
    sums = jnp.where(iota((8, 128), 0) < 3, sums, 0.0)
    back = (iota((128, channels), 0) == SUM_LANE + iota((128, channels), 1) // 4) & (
        iota((128, channels), 1) % 4 == 3
    )
    total = jnp.sum(sums, axis=0, keepdims=True)
    carry = sum(
        matmul(jnp.broadcast_to(part, (8, 128)).astype(BF16), back.astype(F32).astype(BF16))
        for part in three_parts(total)
    )[0:1]

    behind = block == own - 1
    rim = jnp.sum(jnp.where(behind, arrived, 0.0), axis=0)[:, :channels]
    rim_joins = jnp.where(behind & joins, their_count, 0.0)
    rim_rows = jnp.sum(rim_joins, axis=0)

    square = (rows, rows)
    line = jnp.broadcast_to(docs, square)
    column = line.T
    here = iota(square, 0)
    there = iota(square, 1)
    together = (line == column) & (there <= here)
    opens = column[:, 0:1] == first_doc
    length = jnp.sum(together.astype(F32), axis=1, keepdims=True) + jnp.where(
        opens, carry_length, 0.0
    )
    values = pool_ref[...]
    rim = rim.astype(BF16)
    position = iota((rows, 16), 0)
    back_by = 16 - iota((rows, 16), 1)
    rim_open = (
        jnp.broadcast_to(opens, (rows, 16))
        & (back_by.astype(F32) <= rim_rows)
    )
    scale = iota((rows, channels), 1) % 4
    total = matmul(together.astype(F32).astype(BF16), values) + jnp.where(opens, carry, 0.0)
    amount = jnp.broadcast_to(length, (rows, channels))
    for k, window in ((0, 2), (1, 8), (2, 16)):
        mask = (together & (there > here - window)).astype(F32).astype(BF16)
        rim_mask = (rim_open & (position + back_by < window)).astype(F32).astype(BF16)
        part = matmul(mask, values) + matmul(rim_mask, rim)
        total = jnp.where(scale == k, part, total)
        amount = jnp.where(scale == k, jnp.minimum(length, float(window)), amount)
    pooled = ((total / amount - values.astype(F32)) * gain_ref[...]).astype(BF16)
    parts = three_parts(norm_ref[...])
    tail = jnp.concatenate([*parts, jnp.zeros((5, 128), F32)], axis=0).astype(BF16)
    for k in range(8):
        both = matmul(pooled, project_ref[:, 256 * k : 256 * (k + 1)])
        for side in (0, 1):
            out_ref[2 * k + side, 0:128] = both[:, 128 * side : 128 * (side + 1)].astype(BF16)
            out_ref[2 * k + side, 128:136] = tail


def sending(arrived_ref, residual_ref, slots_ref, hidden_ref, out_ref, gain_ref):
    projected = jnp.zeros((128, 128), F32)
    for k in range(16):
        projected = projected + arrived_ref[k, 0:128].astype(F32)
        tail = arrived_ref[k, 128:136].astype(F32)
        gain_ref[k : k + 1] = tail[0:1] + tail[1:2] + tail[2:3]
    hidden = residual_ref[...].astype(F32) + projected.astype(BF16).astype(F32)
    hidden_ref[...] = hidden
    slot = iota((512, 128), 0).astype(F32)
    chosen = (slot == slots_ref[0:1]) | (slot == slots_ref[1:2])
    picked = matmul(chosen.astype(F32).astype(BF16), hidden.astype(BF16))
    out_ref[...] = picked.reshape(64, 8, 128).astype(BF16)


def experts(
    core_ref,
    x_ref,
    message_ref,
    gain_ref,
    gate0,
    gate1,
    up0,
    up1,
    down0,
    down1,
    sgate0,
    sgate1,
    sup0,
    sup1,
    sdown0,
    sdown1,
    out_ref,
    normed_ref,
):
    squares = jnp.zeros((256, 128), F32)
    for k in range(16):
        part = x_ref[k // 2, :, k % 2].astype(F32).reshape(256, 128)
        squares = squares + part * part
    scaling = lax.rsqrt(jnp.sum(squares, axis=1, keepdims=True) * (1.0 / 2048.0) + 1e-06)
    for k in range(16):
        part = x_ref[k // 2, :, k % 2].astype(F32).reshape(256, 128)
        normed_ref[:, 128 * k : 128 * (k + 1)] = (part * scaling * gain_ref[k : k + 1]).astype(
            BF16
        )
    message = message_ref[...].astype(F32)
    side = jnp.where(core_ref[0] == 0, message[:, 0:8], message[:, 8:16])
    side = side.reshape(256, 128)
    weight = side[:, W_LANE : W_LANE + 1] + (
        side[:, W_LANE + 1 : W_LANE + 2] + side[:, W_LANE + 2 : W_LANE + 3]
    )
    first = side[:, W_LANE + 3 : W_LANE + 4]
    normed = normed_ref[...]

    def hidden(gate, up, factor):
        upper = matmul(normed, up[...])
        lower = matmul(normed, gate[...])
        return (jax.nn.silu(lower) * upper * factor).astype(BF16)

    pieces = (
        (hidden(gate0, up0, weight), down0),
        (hidden(gate1, up1, weight), down1),
        (hidden(sgate0, sup0, first), sdown0),
        (hidden(sgate1, sup1, first), sdown1),
    )
    for k in range(8):
        cut = slice(256 * k, 256 * (k + 1))
        total = sum(matmul(value, down[:, cut]) for value, down in pieces)
        out_ref[k, :, 0] = total[:, :128].reshape(32, 8, 128).astype(BF16)
        out_ref[k, :, 1] = total[:, 128:].reshape(32, 8, 128).astype(BF16)


def adding(arrived_ref, out_ref):
    total = arrived_ref[0].astype(F32)
    for k in range(1, 8):
        total = total + arrived_ref[k].astype(F32)
    out_ref[...] = total.astype(BF16)


def closing(arrived_ref, slots_ref, hidden_ref, out_ref):
    slot = iota((128, 512), 1).astype(F32)
    first = jnp.broadcast_to(slots_ref[0:1], (128, 128)).T[:, 0:1]
    second = jnp.broadcast_to(slots_ref[1:2], (128, 128)).T[:, 0:1]
    chosen = (slot == first) | (slot == second)
    arrived = arrived_ref[...].astype(F32).reshape(512, 128).astype(BF16)
    routed = matmul(chosen.astype(F32).astype(BF16), arrived)
    out_ref[...] = (hidden_ref[...] + routed).astype(BF16)


VMEM = pl.BlockSpec(memory_space=pltpu.VMEM)
SMEM = pl.BlockSpec(memory_space=pltpu.SMEM)


def kernel(body, name, outs, operands, scalars=0, scratch=()):
    return pl.pallas_call(
        body,
        name=name,
        out_shape=outs,
        in_specs=[SMEM] * scalars + [VMEM] * (len(operands) - scalars),
        out_specs=jax.tree.map(lambda _: VMEM, outs),
        scratch_shapes=scratch,
        compiler_params=pltpu.CompilerParams(vmem_limit_bytes=56 * 2**20),
    )(*operands)


def array(shape, kind):
    return jax.ShapeDtypeStruct(shape, kind)


def body(
    pool_input,
    doc_ids,
    residual,
    pool_gain,
    out_proj,
    norm_gain,
    routes,
    route_weights,
    expert_gate,
    expert_up,
    expert_down,
    shared_gate,
    shared_up,
    shared_down,
):
    docs = doc_ids.reshape(1, 128)
    message, slots = kernel(
        opening,
        "opening",
        (array((32, 16, 128), BF16), array((8, 128), F32)),
        (pool_input, docs, routes, route_weights),
    )
    swap = ((0, 1), (1, 0))
    own = (
        expert_gate[0],
        expert_up[0],
        expert_down[0],
        shared_gate,
        shared_up,
        shared_down,
    )
    other = [lax.ppermute(value, "c", swap) for value in own]
    arrived = exchanged(message, "sp")
    index = lax.axis_index("sp").astype(jnp.int32).reshape(1)
    core = lax.axis_index("c").astype(jnp.int32).reshape(1)
    terms = kernel(
        pooling,
        "pooling",
        array((16, 136, 128), BF16),
        (
            index,
            arrived,
            pool_input,
            docs,
            pool_gain.reshape(1, 64),
            out_proj,
            norm_gain.reshape(1, 128),
        ),
        scalars=1,
    )
    terms = exchanged(terms, ("y", "c"))
    hidden_state, outgoing, gains = kernel(
        sending,
        "sending",
        (array((128, 128), F32), array((64, 8, 128), BF16), array((16, 128), F32)),
        (terms, residual, slots),
    )
    rows = exchanged(outgoing, ("sp", "c"))
    rows = exchanged(jnp.broadcast_to(rows, (8, *rows.shape)), "y")
    pairs = [part for both in zip(own, other) for part in both]
    parts = kernel(
        experts,
        "experts",
        array((8, 32, 2, 8, 128), BF16),
        (core, rows.reshape(8, 32, 2, 8, 128), arrived, gains, *pairs),
        scalars=1,
        scratch=[pltpu.VMEM((256, 2048), BF16)],
    )
    parts = exchanged(parts.reshape(8, 64, 8, 128), "y")
    summed = kernel(adding, "adding", array((64, 8, 128), BF16), (parts,))
    returned = exchanged(summed, ("sp", "c"))
    return kernel(
        closing, "closing", array((128, 128), BF16), (returned, slots, hidden_state)
    )


def solution(mesh):
    split = Mesh(mesh.devices.reshape(32, 8, 2), ("sp", "y", "c"))
    tp = ("y", "c")
    placed = (
        P("sp", tp),
        P("sp"),
        P("sp", tp),
        P(tp),
        P(tp, None),
        P(tp),
        P("sp", None),
        P("sp", None),
        P("sp", None, tp),
        P("sp", None, tp),
        P("sp", tp, None),
        P(None, tp),
        P(None, tp),
        P(tp, None),
    )
    return jax.shard_map(
        body, mesh=split, in_specs=placed, out_specs=P("sp", tp), check_vma=False
    )
```

time: 280 us -> 175 us (0.62)
  waiting for transfers between devices: 110 us -> 24.7 us
  blocking collectives: 57.3 us -> 93.5 us
  local copies, waits for them, and re-layouts: 27.3 us -> 6.26 us
  Pallas kernels: 0 us -> 19.1 us
  starting transfers between devices: 47.4 us -> 30.5 us
  between operations: 14 us -> 0.17 us
  other arithmetic: 11.3 us -> 0 us
  matrix products: 11.1 us -> 0 us
    all_to_all x7 -> x2, waiting for transfers between devices: 110 us -> 22.8 us  [exchanged(): return lax.all_to_all(value, axis, split_axis=0, concat_axis=0, tiled=True)]
    all_to_all x1 -> x4, blocking collectives: 57.3 us -> 93.5 us  [exchanged(): return lax.all_to_all(value, axis, split_axis=0, concat_axis=0, tiled=True)]
    all_to_all x7 -> x2, starting transfers between devices: 44.3 us -> 17.4 us  [exchanged(): return lax.all_to_all(value, axis, split_axis=0, concat_axis=0, tiled=True)]
    pallas_call x0 -> x6, Pallas kernels: none -> 19.1 us  [kernel(): pl.pallas_call(body, name=name, out_shape=outs, in_specs=[SMEM] * scalars...]
    dot_general x5 -> x0, matrix products: 11.1 us -> none  [the longest x1 5.02 us: expert_terms(): jnp.einsum('secf,efd->secd', hidden, down_weight, preferred_element_type=...]
    ppermute x1 -> x6, starting transfers between devices: 3.12 us -> 13.1 us  [body(): other = [lax.ppermute(value, 'c', swap) for value in own]]
    slice x54 -> x0, local copies, waits for them, and re-layouts: 9.41 us -> none  [the longest x44 5.8 us: folded_in_pairs(): part[side::2]]
    gather x4 -> x0, local copies, waits for them, and re-layouts: 4.89 us -> none  [the longest x1 3.35 us: body(): jnp.take(with_blank, slot_token, axis=0)]
  transfers between devices with their start and end apart: 8 -> 8, of which waited for: 8 -> 3; matrix products, arithmetic and copies ran while one was open for 5% -> 0% of each run, Pallas kernels for 0% -> 0%
where the time goes in v1:
time: 175 us; the launch traced here: 174 us
  blocking collectives  93.5 us (53%)
  starting transfers between devices  30.5 us (17%)
  waiting for transfers between devices  24.7 us (14%)
  Pallas kernels  19.1 us (11%)
  local copies, waits for them, and re-layouts  6.26 us (4%)
    all_to_all x4, blocking collectives, exchanged(): return lax.all_to_all(value, axis, split_axis=0, concat_axis=0, tiled=True)  93.5 us
    all_to_all x2, waiting for transfers between devices, exchanged(): return lax.all_to_all(value, axis, split_axis=0, concat_axis=0, tiled=True)  22.8 us
    pallas_call x6, Pallas kernels, kernel(): pl.pallas_call(body, name=name, out_shape=outs, in_specs=[SMEM] * scalars...  19.1 us
    all_to_all x2, starting transfers between devices, exchanged(): return lax.all_to_all(value, axis, split_axis=0, concat_axis=0, tiled=True)  17.4 us
    ppermute x6, starting transfers between devices, body(): other = [lax.ppermute(value, 'c', swap) for value in own]  13.1 us
    unnamed x23, local copies, waits for them, and re-layouts  5.14 us
  transfers between devices with their start and end apart: 8, of which 3 were waited for; matrix products, arithmetic and copies ran while one was open for 0% of the time, Pallas kernels for 0%

profile of v1, /device:TPU:1, one launch (start us, length us, event | category | flops | bytes accessed | tf_op | source)
XLA Modules:
  0.0 174.3 jit_solution(16123638997151644)
XLA Ops:
  0.0 1.4 copy.15.pool_ref
  2.9 2.1 %opening.1 = (bf16[32,16,128]{2,1,0:T(8,128)(2,1)}, f32[8,128]{1,0:T(8,128)}) custom-call(bf16[128,64]{1,0:T(8,128)(2,1)} %copy.15.pool_ref, s32[1,128]{1,0:T(1,128)} %bitcast.14, s32[128,2]{1,0:T(8,128)} %copy.16.routes_ref, f32[128,2]{1,0:T(8,128)} %copy.17.weights_ref), custom_call_target="tpu_custom_call" | custom-call | tf_op jit(solution)/shard_map/opening/pallas_call | solution.py:256
  5.0 13.7 %all-to-all-start = ((bf16[32,16,128]{2,1,0:T(8,128)(2,1)}), bf16[32,16,128]{2,1,0:T(8,128)(2,1)S(1)}, u32[]{:S(2)}, u32[]{:S(2)}) async-start(bf16[32,16,128]{2,1,0:T(8,128)(2,1)} %get-tuple-element.10), calls=%async_computation | async-start | bytes 262144 | tf_op jit(solution)/shard_map/all_to_all | solution.py:17
  18.7 9.3 %all-to-all-done.arrived_ref.message_ref = bf16[32,16,128]{2,1,0:T(8,128)(2,1)S(1)} async-done(((bf16[32,16,128]{2,1,0:T(8,128)(2,1)}), bf16[32,16,128]{2,1,0:T(8,128)(2,1)S(1)}, u32[]{:S(2)}, u32[]{:S(2)}) %all-to-all-start) | async-done | bytes 131104 | tf_op jit(solution)/shard_map/all_to_all | solution.py:17
  28.7 2.7 %pooling.1 = bf16[16,136,128]{2,1,0:T(8,128)(2,1)} custom-call(s32[1]{0:T(128)} %bitcast.1.index_ref, bf16[32,16,128]{2,1,0:T(8,128)(2,1)} %copy-done.3, bf16[128,64]{1,0:T(8,128)(2,1)} %copy.15.pool_ref, s32[1,128]{1,0:T(1,128)} %bitcast.15, f32[1,64]{1,0:T(1,128)} %bitcast.16, bf16[64,2048]{1,0:T(8,128)(2,1)} %project_ref.1, f32[1,128]{1,0:T(1,128)} %bitcast.17), custom_call_target="tpu_custom_call" | custom-call | tf_op jit(solution)/shard_map/pooling/pallas_call | solution.py:256
  31.4 27.6 %all_to_all.30.arrived_ref = bf16[16,136,128]{2,1,0:T(8,128)(2,1)} all-to-all(bf16[16,136,128]{2,1,0:T(8,128)(2,1)} %pooling.1), channel_id=1, replica_groups=mesh['sp'=32,'y'=8,'c'=2] {'y','c'}, dimensions={0} | all-to-all | bytes 1114112 | tf_op jit(solution)/shard_map/all_to_all | solution.py:17
  59.0 2.0 %sending.1 = (f32[128,128]{1,0:T(8,128)}, bf16[64,8,128]{2,1,0:T(8,128)(2,1)}, f32[16,128]{1,0:T(8,128)}) custom-call(bf16[16,136,128]{2,1,0:T(8,128)(2,1)} %all_to_all.30.arrived_ref, bf16[128,128]{1,0:T(8,128)(2,1)} %residual_ref.1, f32[8,128]{1,0:T(8,128)} %get-tuple-element.11.slots_ref), custom_call_target="tpu_custom_call" | custom-call | tf_op jit(solution)/shard_map/sending/pallas_call | solution.py:256
  61.0 15.8 %all_to_all.31 = bf16[64,8,128]{2,1,0:T(8,128)(2,1)S(1)} all-to-all(bf16[64,8,128]{2,1,0:T(8,128)(2,1)} %get-tuple-element.12), channel_id=1, replica_groups=mesh['sp'=32,'y'=8,'c'=2] {'sp','c'}, dimensions={0} | all-to-all | bytes 262144 | tf_op jit(solution)/shard_map/all_to_all | solution.py:17
  76.8 1.1 broadcast_in_dim.3
  78.0 3.7 %all-to-all-start.3 = ((bf16[8,64,8,128]{3,2,1,0:T(8,128)(2,1)}), bf16[8,64,8,128]{3,2,1,0:T(8,128)(2,1)S(1)}, u32[]{:S(2)}, u32[]{:S(2)}) async-start(bf16[8,64,8,128]{3,2,1,0:T(8,128)(2,1)} %broadcast_in_dim.3), calls=%async_computation.3 | async-start | bytes 2097152 | tf_op jit(solution)/shard_map/all_to_all | solution.py:17
  81.7 2.3 %collective-permute-start = (bf16[2048,256]{1,0:T(8,128)(2,1)S(1)}, bf16[2048,256]{1,0:T(8,128)(2,1)}, u32[]{:S(2)}, u32[]{:S(2)}) collective-permute-start(bf16[2048,256]{1,0:T(8,128)(2,1)S(1)} %bitcast.13), channel_id=1, source_target_pairs={{0,1},{1,0},{2,3},{3,2},{4,5},{5,4},{6,7},{7,6},{8,9},{9,8},{10,11... | collective-permute-start | bytes 3145736 | tf_op jit(solution)/shard_map/ppermute | solution.py:303
  84.0 2.0 %collective-permute-start.1 = (bf16[2048,256]{1,0:T(8,128)(2,1)}, bf16[2048,256]{1,0:T(8,128)(2,1)}, u32[]{:S(2)}, u32[]{:S(2)}) collective-permute-start(bf16[2048,256]{1,0:T(8,128)(2,1)} %bitcast.7.up0), channel_id=1, source_target_pairs={{0,1},{1,0},{2,3},{3,2},{4,5},{5,4},{6,7},{7,6},{8,9},{9,8},{10,11... | collective-permute-start | bytes 3145736 | tf_op jit(solution)/shard_map/ppermute | solution.py:303
  86.0 2.4 %collective-permute-start.2 = (bf16[256,2048]{1,0:T(8,128)(2,1)}, bf16[256,2048]{1,0:T(8,128)(2,1)}, u32[]{:S(2)}, u32[]{:S(2)}) collective-permute-start(bf16[256,2048]{1,0:T(8,128)(2,1)} %bitcast.8.down0), channel_id=1, source_target_pairs={{0,1},{1,0},{2,3},{3,2},{4,5},{5,4},{6,7},{7,6},{8,9},{9,8},{10,11... | collective-permute-start | bytes 3145736 | tf_op jit(solution)/shard_map/ppermute | solution.py:303
  88.5 2.0 %collective-permute-start.5 = (bf16[64,2048]{1,0:T(8,128)(2,1)}, bf16[64,2048]{1,0:T(8,128)(2,1)}, u32[]{:S(2)}, u32[]{:S(2)}) collective-permute-start(bf16[64,2048]{1,0:T(8,128)(2,1)} %sdown0.1), channel_id=1, source_target_pairs={{0,1},{1,0},{2,3},{3,2},{4,5},{5,4},{6,7},{7,6},{8,9},{9,8},{10,11... | collective-permute-start | bytes 786440 | tf_op jit(solution)/shard_map/ppermute | solution.py:303
  90.8 2.3 %collective-permute-start.4 = (bf16[2048,64]{1,0:T(8,128)(2,1)S(1)}, bf16[2048,64]{1,0:T(8,128)(2,1)}, u32[]{:S(2)}, u32[]{:S(2)}) collective-permute-start(bf16[2048,64]{1,0:T(8,128)(2,1)S(1)} %copy.22.sup0), channel_id=1, source_target_pairs={{0,1},{1,0},{2,3},{3,2},{4,5},{5,4},{6,7},{7,6},{8,9},{9,8},{10,11... | collective-permute-start | bytes 786440 | tf_op jit(solution)/shard_map/ppermute | solution.py:303
  93.4 2.0 %collective-permute-start.3 = (bf16[2048,64]{1,0:T(8,128)(2,1)S(1)}, bf16[2048,64]{1,0:T(8,128)(2,1)}, u32[]{:S(2)}, u32[]{:S(2)}) collective-permute-start(bf16[2048,64]{1,0:T(8,128)(2,1)S(1)} %copy.21.sgate0), channel_id=1, source_target_pairs={{0,1},{1,0},{2,3},{3,2},{4,5},{5,4},{6,7},{7,6},{8,9},{9,8},{10,11... | collective-permute-start | bytes 786440 | tf_op jit(solution)/shard_map/ppermute | solution.py:303
  95.5 1.9 %collective-permute-done.3.sgate1 = bf16[2048,64]{1,0:T(8,128)(2,1)} collective-permute-done((bf16[2048,64]{1,0:T(8,128)(2,1)S(1)}, bf16[2048,64]{1,0:T(8,128)(2,1)}, u32[]{:S(2)}, u32[]{:S(2)}) %collective-permute-start.3) | collective-permute-done | bytes 262176 | tf_op jit(solution)/shard_map/ppermute | solution.py:303
  97.4 13.5 %all-to-all-done.3 = bf16[8,64,8,128]{3,2,1,0:T(8,128)(2,1)S(1)} async-done(((bf16[8,64,8,128]{3,2,1,0:T(8,128)(2,1)}), bf16[8,64,8,128]{3,2,1,0:T(8,128)(2,1)S(1)}, u32[]{:S(2)}, u32[]{:S(2)}) %all-to-all-start.3) | async-done | bytes 1048608 | tf_op jit(solution)/shard_map/all_to_all | solution.py:17
  110.9 1.0 copy-done
  111.9 8.5 %experts.1 = bf16[8,32,2,8,128]{4,3,2,1,0:T(8,128)(2,1)} custom-call(s32[1]{0:T(128)} %bitcast.core_ref, bf16[8,32,2,8,128]{4,3,2,1,0:T(8,128)(2,1)} %bitcast.10, bf16[32,16,128]{2,1,0:T(8,128)(2,1)} %copy-done.3, f32[16,128]{1,0:T(8,128)} %get-tuple-element.13.gain_ref, bf16[2048,256]{1,0:T(8,128)(2,1)} %bitcast.12, ...), custom_call_target="tpu_custom_call" | custom-call | tf_op jit(solution)/shard_map/experts/pallas_call | solution.py:256
  120.4 33.3 %all_to_all.32.arrived_ref = bf16[8,64,8,128]{3,2,1,0:T(8,128)(2,1)} all-to-all(bf16[8,64,8,128]{3,2,1,0:T(8,128)(2,1)} %bitcast.11), channel_id=1, replica_groups=mesh['sp'=32,'y'=8,'c'=2] {'y'}, dimensions={0} | all-to-all | bytes 2097152 | tf_op jit(solution)/shard_map/all_to_all | solution.py:17
  153.7 2.0 %adding.1 = bf16[64,8,128]{2,1,0:T(8,128)(2,1)} custom-call(bf16[8,64,8,128]{3,2,1,0:T(8,128)(2,1)} %all_to_all.32.arrived_ref), custom_call_target="tpu_custom_call" | custom-call | tf_op jit(solution)/shard_map/adding/pallas_call | solution.py:256
  155.7 16.7 %all_to_all.33.arrived_ref = bf16[64,8,128]{2,1,0:T(8,128)(2,1)} all-to-all(bf16[64,8,128]{2,1,0:T(8,128)(2,1)} %adding.1), channel_id=1, replica_groups=mesh['sp'=32,'y'=8,'c'=2] {'sp','c'}, dimensions={0} | all-to-all | bytes 262144 | tf_op jit(solution)/shard_map/all_to_all | solution.py:17
  172.4 1.8 %closing.1 = bf16[128,128]{1,0:T(8,128)(2,1)} custom-call(bf16[64,8,128]{2,1,0:T(8,128)(2,1)} %all_to_all.33.arrived_ref, f32[8,128]{1,0:T(8,128)} %get-tuple-element.11.slots_ref, f32[128,128]{1,0:T(8,128)} %get-tuple-element.14.hidden_ref), custom_call_target="tpu_custom_call" | custom-call | tf_op jit(solution)/shard_map/closing/pallas_call | solution.py:256
  (26 shorter events, 2.7 us)
Async XLA Ops:
  0.0 1.5 copy-start.7
  1.5 0.7 copy-start.8
  5.0 23.1 %all-to-all-start = ((bf16[32,16,128]{2,1,0:T(8,128)(2,1)}), bf16[32,16,128]{2,1,0:T(8,128)(2,1)S(1)}, u32[]{:S(2)}, u32[]{:S(2)}) async-start(bf16[32,16,128]{2,1,0:T(8,128)(2,1)} %get-tuple-element.10), calls=%async_computation | async-start | bytes 262144 | tf_op jit(solution)/shard_map/all_to_all | solution.py:17
  28.1 0.7 copy-start.3
  78.0 3.7 %copy-start.4 = (bf16[1,2048,256]{2,1,0:T(8,128)(2,1)S(1)}, bf16[1,2048,256]{2,1,0:T(8,128)(2,1)}, u32[]{:S(2)}) copy-start(bf16[1,2048,256]{2,1,0:T(8,128)(2,1)} %param.22) | copy-start | bytes 3145732
  78.0 12.5 %copy-start.5 = (bf16[2048,64]{0,1:T(8,128)(2,1)S(1)}, bf16[2048,64]{0,1:T(8,128)(2,1)}, u32[]{:S(2)}) copy-start(bf16[2048,64]{0,1:T(8,128)(2,1)} %param.26) | copy-start | bytes 786436
  78.0 32.9 %all-to-all-start.3 = ((bf16[8,64,8,128]{3,2,1,0:T(8,128)(2,1)}), bf16[8,64,8,128]{3,2,1,0:T(8,128)(2,1)S(1)}, u32[]{:S(2)}, u32[]{:S(2)}) async-start(bf16[8,64,8,128]{3,2,1,0:T(8,128)(2,1)} %broadcast_in_dim.3), calls=%async_computation.3 | async-start | bytes 2097152 | tf_op jit(solution)/shard_map/all_to_all | solution.py:17
  81.7 15.7 %collective-permute-start = (bf16[2048,256]{1,0:T(8,128)(2,1)S(1)}, bf16[2048,256]{1,0:T(8,128)(2,1)}, u32[]{:S(2)}, u32[]{:S(2)}) collective-permute-start(bf16[2048,256]{1,0:T(8,128)(2,1)S(1)} %bitcast.13), channel_id=1, source_target_pairs={{0,1},{1,0},{2,3},{3,2},{4,5},{5,4},{6,7},{7,6},{8,9},{9,8},{10,11... | collective-permute-start | bytes 3145736 | tf_op jit(solution)/shard_map/ppermute | solution.py:303
  84.0 13.4 %collective-permute-start.1 = (bf16[2048,256]{1,0:T(8,128)(2,1)}, bf16[2048,256]{1,0:T(8,128)(2,1)}, u32[]{:S(2)}, u32[]{:S(2)}) collective-permute-start(bf16[2048,256]{1,0:T(8,128)(2,1)} %bitcast.7.up0), channel_id=1, source_target_pairs={{0,1},{1,0},{2,3},{3,2},{4,5},{5,4},{6,7},{7,6},{8,9},{9,8},{10,11... | collective-permute-start | bytes 3145736 | tf_op jit(solution)/shard_map/ppermute | solution.py:303
  86.0 7.1 %copy-start.6 = (bf16[2048,64]{0,1:T(8,128)(2,1)S(1)}, bf16[2048,64]{0,1:T(8,128)(2,1)}, u32[]{:S(2)}) copy-start(bf16[2048,64]{0,1:T(8,128)(2,1)} %param.25) | copy-start | bytes 786436
  86.0 11.3 %collective-permute-start.2 = (bf16[256,2048]{1,0:T(8,128)(2,1)}, bf16[256,2048]{1,0:T(8,128)(2,1)}, u32[]{:S(2)}, u32[]{:S(2)}) collective-permute-start(bf16[256,2048]{1,0:T(8,128)(2,1)} %bitcast.8.down0), channel_id=1, source_target_pairs={{0,1},{1,0},{2,3},{3,2},{4,5},{5,4},{6,7},{7,6},{8,9},{9,8},{10,11... | collective-permute-start | bytes 3145736 | tf_op jit(solution)/shard_map/ppermute | solution.py:303
  88.5 4.9 %collective-permute-start.5 = (bf16[64,2048]{1,0:T(8,128)(2,1)}, bf16[64,2048]{1,0:T(8,128)(2,1)}, u32[]{:S(2)}, u32[]{:S(2)}) collective-permute-start(bf16[64,2048]{1,0:T(8,128)(2,1)} %sdown0.1), channel_id=1, source_target_pairs={{0,1},{1,0},{2,3},{3,2},{4,5},{5,4},{6,7},{7,6},{8,9},{9,8},{10,11... | collective-permute-start | bytes 786440 | tf_op jit(solution)/shard_map/ppermute | solution.py:303
  90.8 20.1 %copy-start.1 = (bf16[2048,64]{1,0:T(8,128)(2,1)}, bf16[2048,64]{1,0:T(8,128)(2,1)S(1)}, u32[]{:S(2)}) copy-start(bf16[2048,64]{1,0:T(8,128)(2,1)S(1)} %copy.22.sup0) | copy-start | bytes 786436
  90.8 4.7 %collective-permute-start.4 = (bf16[2048,64]{1,0:T(8,128)(2,1)S(1)}, bf16[2048,64]{1,0:T(8,128)(2,1)}, u32[]{:S(2)}, u32[]{:S(2)}) collective-permute-start(bf16[2048,64]{1,0:T(8,128)(2,1)S(1)} %copy.22.sup0), channel_id=1, source_target_pairs={{0,1},{1,0},{2,3},{3,2},{4,5},{5,4},{6,7},{7,6},{8,9},{9,8},{10,11... | collective-permute-start | bytes 786440 | tf_op jit(solution)/shard_map/ppermute | solution.py:303
  93.4 17.5 %copy-start.2 = (bf16[2048,64]{1,0:T(8,128)(2,1)}, bf16[2048,64]{1,0:T(8,128)(2,1)S(1)}, u32[]{:S(2)}) copy-start(bf16[2048,64]{1,0:T(8,128)(2,1)S(1)} %copy.21.sgate0) | copy-start | bytes 786436
  93.4 3.9 %collective-permute-start.3 = (bf16[2048,64]{1,0:T(8,128)(2,1)S(1)}, bf16[2048,64]{1,0:T(8,128)(2,1)}, u32[]{:S(2)}, u32[]{:S(2)}) collective-permute-start(bf16[2048,64]{1,0:T(8,128)(2,1)S(1)} %copy.21.sgate0), channel_id=1, source_target_pairs={{0,1},{1,0},{2,3},{3,2},{4,5},{5,4},{6,7},{7,6},{8,9},{9,8},{10,11... | collective-permute-start | bytes 786440 | tf_op jit(solution)/shard_map/ppermute | solution.py:303
  110.9 1.0 copy-start

commit v2 on v1

--- a/solution.py
+++ b/solution.py
@@ -32,21 +32,23 @@
     return jnp.dot(a, b, preferred_element_type=F32)
 
 
-def opening(pool_ref, docs_ref, routes_ref, weights_ref, message_ref, slots_ref):
-    rows, channels = pool_ref.shape
+def opening(pool_ref, docs_ref, routes_ref, weights_ref, message_ref, slots_ref, values_ref):
+    channels, rows = pool_ref.shape
     square = (rows, rows)
+    values = pool_ref[...].astype(F32).T.astype(BF16)
+    values_ref[...] = values
     across = iota((channels, 128), 0)
     lane = iota((channels, 128), 1)
     spread = (lane == across) | ((across % 4 == 3) & (lane == SUM_LANE + across // 4))
-    wide = matmul(pool_ref[...], spread.astype(F32).astype(BF16))
+    wide = matmul(values, spread.astype(F32).astype(BF16))
     docs = docs_ref[...].astype(F32)
     last_doc = docs[:, rows - 1 :]
     trailing = (docs == last_doc).astype(F32)
     sums = matmul(jnp.broadcast_to(trailing, (8, rows)).astype(BF16), wide.astype(BF16))[0:1]
     count = jnp.sum(trailing, axis=1, keepdims=True)
 
-    columns = [jnp.broadcast_to(routes_ref[:, k : k + 1].astype(F32), square) for k in (0, 1)]
-    lines = [column.T for column in columns]
+    lines = [jnp.broadcast_to(routes_ref[k : k + 1].astype(F32), square) for k in (0, 1)]
+    columns = [line.T for line in lines]
     before = iota(square, 0) < iota(square, 1)
 
     def counted(mask):
@@ -59,9 +61,7 @@
     slots_ref[...] = jnp.concatenate(
         [first_slot, second_slot, jnp.zeros((6, rows), F32)], axis=0
     )
-    share = [
-        jnp.broadcast_to(weights_ref[:, k : k + 1], square).T[0:1] for k in (0, 1)
-    ]
+    share = [weights_ref[k : k + 1] for k in (0, 1)]
     slot = iota((512, rows), 0).astype(F32)
     is_first = slot == first_slot
     is_second = slot == second_slot
@@ -160,7 +160,7 @@
             out_ref[2 * k + side, 128:136] = tail
 
 
-def sending(arrived_ref, residual_ref, slots_ref, hidden_ref, out_ref, gain_ref):
+def sending(arrived_ref, slots_ref, residual_ref, hidden_ref, out_ref, gain_ref):
     projected = jnp.zeros((128, 128), F32)
     for k in range(16):
         projected = projected + arrived_ref[k, 0:128].astype(F32)
@@ -174,26 +174,23 @@
     out_ref[...] = picked.reshape(64, 8, 128).astype(BF16)
 
 
-def experts(
-    core_ref,
-    x_ref,
-    message_ref,
-    gain_ref,
-    gate0,
-    gate1,
-    up0,
-    up1,
-    down0,
-    down1,
-    sgate0,
-    sgate1,
-    sup0,
-    sup1,
-    sdown0,
-    sdown1,
-    out_ref,
-    normed_ref,
-):
+def spreading(arrived_ref, out_ref):
+    for k in range(8):
+        out_ref[k] = arrived_ref[...]
+
+
+def experts(core_ref, x_ref, message_ref, gain_ref, *refs):
+    sources, out_ref, normed_ref = refs[:12], refs[12], refs[13]
+    near, landed = refs[14:26], refs[26]
+    copies = [
+        pltpu.make_async_copy(source, target, landed.at[k])
+        for k, (source, target) in enumerate(zip(sources, near))
+    ]
+    order = (0, 2, 1, 3, 6, 7, 8, 9, 4, 5, 10, 11)
+    for k in order:
+        copies[k].start()
+    gate0, gate1, up0, up1, down0, down1, sgate0, sgate1, sup0, sup1, sdown0, sdown1 = near
+
     squares = jnp.zeros((256, 128), F32)
     for k in range(16):
         part = x_ref[k // 2, :, k % 2].astype(F32).reshape(256, 128)
@@ -218,15 +215,26 @@
         lower = matmul(normed, gate[...])
         return (jax.nn.silu(lower) * upper * factor).astype(BF16)
 
-    pieces = (
-        (hidden(gate0, up0, weight), down0),
-        (hidden(gate1, up1, weight), down1),
-        (hidden(sgate0, sup0, first), sdown0),
-        (hidden(sgate1, sup1, first), sdown1),
-    )
+    copies[0].wait()
+    copies[2].wait()
+    left = hidden(gate0, up0, weight)
+    copies[1].wait()
+    copies[3].wait()
+    right = hidden(gate1, up1, weight)
+    for k in (6, 7, 8, 9):
+        copies[k].wait()
+    across = jnp.concatenate([sgate0[...], sgate1[...], sup0[...], sup1[...]], axis=0)
+    both = lax.dot_general(
+        normed, across, (((1,), (1,)), ((), ())), preferred_element_type=F32
+    )
+    shared = (jax.nn.silu(both[:, :128]) * both[:, 128:] * first).astype(BF16)
+    for k in (4, 5, 10, 11):
+        copies[k].wait()
+    sdown = jnp.concatenate([sdown0[...], sdown1[...]], axis=0)
     for k in range(8):
         cut = slice(256 * k, 256 * (k + 1))
-        total = sum(matmul(value, down[:, cut]) for value, down in pieces)
+        total = matmul(left, down0[:, cut]) + matmul(right, down1[:, cut])
+        total = total + matmul(shared, sdown[:, cut])
         out_ref[k, :, 0] = total[:, :128].reshape(32, 8, 128).astype(BF16)
         out_ref[k, :, 1] = total[:, 128:].reshape(32, 8, 128).astype(BF16)
 
@@ -252,20 +260,31 @@
 SMEM = pl.BlockSpec(memory_space=pltpu.SMEM)
 
 
-def kernel(body, name, outs, operands, scalars=0, scratch=()):
+HBM = pl.BlockSpec(memory_space=pl.ANY)
+
+
+def kernel(body, name, outs, operands, near=(), far=(), scalars=0, scratch=(), room=16):
+    near = [pltpu.with_memory_space_constraint(value, pltpu.VMEM) for value in near]
+    far = [pltpu.with_memory_space_constraint(value, pltpu.HBM) for value in far]
+    scalar = operands[:scalars]
+    plain = [
+        pltpu.with_memory_space_constraint(value, pltpu.HBM) for value in operands[scalars:]
+    ]
     return pl.pallas_call(
         body,
         name=name,
         out_shape=outs,
-        in_specs=[SMEM] * scalars + [VMEM] * (len(operands) - scalars),
+        in_specs=[SMEM] * scalars
+        + [VMEM] * (len(near) + len(plain))
+        + [HBM] * len(far),
         out_specs=jax.tree.map(lambda _: VMEM, outs),
         scratch_shapes=scratch,
-        compiler_params=pltpu.CompilerParams(vmem_limit_bytes=56 * 2**20),
-    )(*operands)
+        compiler_params=pltpu.CompilerParams(vmem_limit_bytes=room * 2**20),
+    )(*scalar, *near, *plain, *far)
 
 
 def array(shape, kind):
-    return jax.ShapeDtypeStruct(shape, kind)
+    return pltpu.VMEM(shape, kind)
 
 
 def body(
@@ -285,19 +304,19 @@
     shared_down,
 ):
     docs = doc_ids.reshape(1, 128)
-    message, slots = kernel(
+    message, slots, values = kernel(
         opening,
         "opening",
-        (array((32, 16, 128), BF16), array((8, 128), F32)),
-        (pool_input, docs, routes, route_weights),
+        (array((32, 16, 128), BF16), array((8, 128), F32), array((128, 64), BF16)),
+        (pool_input.T, docs, routes.T, route_weights.T),
     )
     swap = ((0, 1), (1, 0))
     own = (
         expert_gate[0],
         expert_up[0],
         expert_down[0],
-        shared_gate,
-        shared_up,
+        shared_gate.T,
+        shared_up.T,
         shared_down,
     )
     other = [lax.ppermute(value, "c", swap) for value in own]
@@ -308,15 +327,8 @@
         pooling,
         "pooling",
         array((16, 136, 128), BF16),
-        (
-            index,
-            arrived,
-            pool_input,
-            docs,
-            pool_gain.reshape(1, 64),
-            out_proj,
-            norm_gain.reshape(1, 128),
-        ),
+        (index, docs, pool_gain.reshape(1, 64), out_proj, norm_gain.reshape(1, 128)),
+        near=(arrived, values),
         scalars=1,
     )
     terms = exchanged(terms, ("y", "c"))
@@ -324,24 +336,35 @@
         sending,
         "sending",
         (array((128, 128), F32), array((64, 8, 128), BF16), array((16, 128), F32)),
-        (terms, residual, slots),
+        (residual,),
+        near=(terms, slots),
     )
     rows = exchanged(outgoing, ("sp", "c"))
-    rows = exchanged(jnp.broadcast_to(rows, (8, *rows.shape)), "y")
+    rows = kernel(spreading, "spreading", array((8, 64, 8, 128), BF16), (), near=(rows,))
+    rows = exchanged(rows, "y")
     pairs = [part for both in zip(own, other) for part in both]
     parts = kernel(
         experts,
         "experts",
         array((8, 32, 2, 8, 128), BF16),
-        (core, rows.reshape(8, 32, 2, 8, 128), arrived, gains, *pairs),
+        (core,),
+        near=(rows.reshape(8, 32, 2, 8, 128), arrived, gains),
+        far=pairs,
         scalars=1,
-        scratch=[pltpu.VMEM((256, 2048), BF16)],
+        scratch=[pltpu.VMEM((256, 2048), BF16)]
+        + [pltpu.VMEM(value.shape, BF16) for value in pairs]
+        + [pltpu.SemaphoreType.DMA((len(pairs),))],
+        room=24,
     )
     parts = exchanged(parts.reshape(8, 64, 8, 128), "y")
-    summed = kernel(adding, "adding", array((64, 8, 128), BF16), (parts,))
+    summed = kernel(adding, "adding", array((64, 8, 128), BF16), (), near=(parts,))
     returned = exchanged(summed, ("sp", "c"))
     return kernel(
-        closing, "closing", array((128, 128), BF16), (returned, slots, hidden_state)
+        closing,
+        "closing",
+        jax.ShapeDtypeStruct((128, 128), BF16),
+        (),
+        near=(returned, slots, hidden_state),
     )
 
 

time: 175 us -> 158 us (0.903)
  Pallas kernels: 19.1 us -> 12.5 us
  local copies, waits for them, and re-layouts: 6.26 us -> 0.01 us
  blocking collectives: 93.5 us -> 88.9 us
    pallas_call x6 -> x7, Pallas kernels: 19.1 us -> 12.5 us  [kernel(): pl.pallas_call(body, name=name, out_shape=outs, in_specs=[SMEM] * scalars...]
    unnamed x23 -> x4, local copies, waits for them, and re-layouts: 5.14 us -> 0.01 us
    all_to_all x4, blocking collectives: 93.5 us -> 88.9 us  [exchanged(): return lax.all_to_all(value, axis, split_axis=0, concat_axis=0, tiled=True)]
where the time goes in v2:
time: 158 us; the launch traced here: 157 us
  blocking collectives  88.9 us (56%)
  starting transfers between devices  30.4 us (19%)
  waiting for transfers between devices  25.5 us (16%)
  Pallas kernels  12.5 us (8%)
    all_to_all x4, blocking collectives, exchanged(): return lax.all_to_all(value, axis, split_axis=0, concat_axis=0, tiled=True)  88.9 us
    all_to_all x2, waiting for transfers between devices, exchanged(): return lax.all_to_all(value, axis, split_axis=0, concat_axis=0, tiled=True)  23.7 us
    all_to_all x2, starting transfers between devices, exchanged(): return lax.all_to_all(value, axis, split_axis=0, concat_axis=0, tiled=True)  17.4 us
    ppermute x6, starting transfers between devices, body(): other = [lax.ppermute(value, 'c', swap) for value in own]  13 us
    pallas_call x7, Pallas kernels, kernel(): pl.pallas_call(body, name=name, out_shape=outs, in_specs=[SMEM] * scalars...  12.5 us
  transfers between devices with their start and end apart: 8, of which 3 were waited for; matrix products, arithmetic and copies ran while one was open for 0% of the time, Pallas kernels for 0%

profile of v2, /device:TPU:1, one launch (start us, length us, event | category | flops | bytes accessed | tf_op | source)
XLA Modules:
  0.0 157.4 jit_solution(12061432087266614966)
XLA Ops:
  0.0 1.8 %opening.1 = (bf16[32,16,128]{2,1,0:T(8,128)(2,1)}, f32[8,128]{1,0:T(8,128)S(1)}, bf16[128,64]{1,0:T(8,128)(2,1)S(1)}) custom-call(bf16[64,128]{1,0:T(8,128)(2,1)} %bitcast.27, s32[1,128]{1,0:T(1,128)} %bitcast.28, s32[2,128]{1,0:T(2,128)} %bitcast.30, f32[2,128]{1,0:T(2,128)} %bitcast.31), custom_call_target="tpu_custom_call" | custom-call | tf_op jit(solution)/shard_map/opening/pallas_call | solution.py:273
  1.8 13.7 %all-to-all-start = ((bf16[32,16,128]{2,1,0:T(8,128)(2,1)}), bf16[32,16,128]{2,1,0:T(8,128)(2,1)S(1)}, u32[]{:S(2)}, u32[]{:S(2)}) async-start(bf16[32,16,128]{2,1,0:T(8,128)(2,1)} %get-tuple-element.11), calls=%async_computation | async-start | bytes 262144 | tf_op jit(solution)/shard_map/all_to_all | solution.py:17
  15.5 9.3 %all-to-all-done.arrived_ref.message_ref = bf16[32,16,128]{2,1,0:T(8,128)(2,1)S(1)} async-done(((bf16[32,16,128]{2,1,0:T(8,128)(2,1)}), bf16[32,16,128]{2,1,0:T(8,128)(2,1)S(1)}, u32[]{:S(2)}, u32[]{:S(2)}) %all-to-all-start) | async-done | bytes 131104 | tf_op jit(solution)/shard_map/all_to_all | solution.py:17
  24.9 1.8 %pooling.1 = bf16[16,136,128]{2,1,0:T(8,128)(2,1)S(1)} custom-call(s32[1]{0:T(128)} %bitcast.1.index_ref, bf16[32,16,128]{2,1,0:T(8,128)(2,1)S(1)} %all-to-all-done.arrived_ref.message_ref, bf16[128,64]{1,0:T(8,128)(2,1)S(1)} %get-tuple-element.12.pool_ref, s32[1,128]{1,0:T(1,128)} %bitcast.29, f32[1,64]{1,0:T(1,128)} %bitcast.32, ...), custom_call_target="tpu_custom_call" | custom-call | tf_op jit(solution)/shard_map/pooling/pallas_call | solution.py:273
  26.7 27.3 %all_to_all.30.arrived_ref = bf16[16,136,128]{2,1,0:T(8,128)(2,1)S(1)} all-to-all(bf16[16,136,128]{2,1,0:T(8,128)(2,1)S(1)} %pooling.1), channel_id=1, replica_groups=mesh['sp'=32,'y'=8,'c'=2] {'y','c'}, dimensions={0} | all-to-all | bytes 1114112 | tf_op jit(solution)/shard_map/all_to_all | solution.py:17
  54.0 1.0 sending.1
  55.0 15.0 %all_to_all.31.arrived_ref = bf16[64,8,128]{2,1,0:T(8,128)(2,1)S(1)} all-to-all(bf16[64,8,128]{2,1,0:T(8,128)(2,1)S(1)} %get-tuple-element.14), channel_id=1, replica_groups=mesh['sp'=32,'y'=8,'c'=2] {'sp','c'}, dimensions={0} | all-to-all | bytes 262144 | tf_op jit(solution)/shard_map/all_to_all | solution.py:17
  70.0 1.1 spreading.1
  71.1 3.7 %all-to-all-start.3 = ((bf16[8,64,8,128]{3,2,1,0:T(8,128)(2,1)}), bf16[8,64,8,128]{3,2,1,0:T(8,128)(2,1)S(1)}, u32[]{:S(2)}, u32[]{:S(2)}) async-start(bf16[8,64,8,128]{3,2,1,0:T(8,128)(2,1)} %spreading.1), calls=%async_computation.3 | async-start | bytes 2097152 | tf_op jit(solution)/shard_map/all_to_all | solution.py:17
  74.8 2.3 %collective-permute-start = (bf16[2048,256]{1,0:T(8,128)(2,1)S(1)}, bf16[2048,256]{1,0:T(8,128)(2,1)}, u32[]{:S(2)}, u32[]{:S(2)}) collective-permute-start(bf16[2048,256]{1,0:T(8,128)(2,1)S(1)} %bitcast.18), channel_id=1, source_target_pairs={{0,1},{1,0},{2,3},{3,2},{4,5},{5,4},{6,7},{7,6},{8,9},{9,8},{10,11... | collective-permute-start | bytes 3145736 | tf_op jit(solution)/shard_map/ppermute | solution.py:322
  77.1 2.0 %collective-permute-start.1 = (bf16[2048,256]{1,0:T(8,128)(2,1)S(1)}, bf16[2048,256]{1,0:T(8,128)(2,1)}, u32[]{:S(2)}, u32[]{:S(2)}) collective-permute-start(bf16[2048,256]{1,0:T(8,128)(2,1)S(1)} %bitcast.20), channel_id=1, source_target_pairs={{0,1},{1,0},{2,3},{3,2},{4,5},{5,4},{6,7},{7,6},{8,9},{9,8},{10,11... | collective-permute-start | bytes 3145736 | tf_op jit(solution)/shard_map/ppermute | solution.py:322
  79.2 2.3 %collective-permute-start.2 = (bf16[256,2048]{1,0:T(8,128)(2,1)}, bf16[256,2048]{1,0:T(8,128)(2,1)}, u32[]{:S(2)}, u32[]{:S(2)}) collective-permute-start(bf16[256,2048]{1,0:T(8,128)(2,1)} %bitcast.21), channel_id=1, source_target_pairs={{0,1},{1,0},{2,3},{3,2},{4,5},{5,4},{6,7},{7,6},{8,9},{9,8},{10,11... | collective-permute-start | bytes 3145736 | tf_op jit(solution)/shard_map/ppermute | solution.py:322
  81.5 2.0 %collective-permute-start.3 = (bf16[64,2048]{1,0:T(8,128)(2,1)}, bf16[64,2048]{1,0:T(8,128)(2,1)}, u32[]{:S(2)}, u32[]{:S(2)}) collective-permute-start(bf16[64,2048]{1,0:T(8,128)(2,1)} %bitcast.23), channel_id=1, source_target_pairs={{0,1},{1,0},{2,3},{3,2},{4,5},{5,4},{6,7},{7,6},{8,9},{9,8},{10,11... | collective-permute-start | bytes 786440 | tf_op jit(solution)/shard_map/ppermute | solution.py:322
  83.5 2.3 %collective-permute-start.4 = (bf16[64,2048]{1,0:T(8,128)(2,1)}, bf16[64,2048]{1,0:T(8,128)(2,1)}, u32[]{:S(2)}, u32[]{:S(2)}) collective-permute-start(bf16[64,2048]{1,0:T(8,128)(2,1)} %bitcast.25), channel_id=1, source_target_pairs={{0,1},{1,0},{2,3},{3,2},{4,5},{5,4},{6,7},{7,6},{8,9},{9,8},{10,11... | collective-permute-start | bytes 786440 | tf_op jit(solution)/shard_map/ppermute | solution.py:322
  85.8 0.0 collective-permute-done.3.refs_7_
  85.8 2.0 %collective-permute-start.5 = (bf16[64,2048]{1,0:T(8,128)(2,1)}, bf16[64,2048]{1,0:T(8,128)(2,1)}, u32[]{:S(2)}, u32[]{:S(2)}) collective-permute-start(bf16[64,2048]{1,0:T(8,128)(2,1)} %refs_10_.1), channel_id=1, source_target_pairs={{0,1},{1,0},{2,3},{3,2},{4,5},{5,4},{6,7},{7,6},{8,9},{9,8},{10,11... | collective-permute-start | bytes 786440 | tf_op jit(solution)/shard_map/ppermute | solution.py:322
  87.9 1.7 %collective-permute-done.5.refs_11_ = bf16[64,2048]{1,0:T(8,128)(2,1)} collective-permute-done((bf16[64,2048]{1,0:T(8,128)(2,1)}, bf16[64,2048]{1,0:T(8,128)(2,1)}, u32[]{:S(2)}, u32[]{:S(2)}) %collective-permute-start.5) | collective-permute-done | bytes 262176 | tf_op jit(solution)/shard_map/ppermute | solution.py:322
  89.6 0.0 collective-permute-done.2.refs_5_
  89.6 14.4 %all-to-all-done.3 = bf16[8,64,8,128]{3,2,1,0:T(8,128)(2,1)S(1)} async-done(((bf16[8,64,8,128]{3,2,1,0:T(8,128)(2,1)}), bf16[8,64,8,128]{3,2,1,0:T(8,128)(2,1)S(1)}, u32[]{:S(2)}, u32[]{:S(2)}) %all-to-all-start.3) | async-done | bytes 1048608 | tf_op jit(solution)/shard_map/all_to_all | solution.py:17
  104.0 5.7 %experts.1 = bf16[8,32,2,8,128]{4,3,2,1,0:T(8,128)(2,1)S(1)} custom-call(s32[1]{0:T(128)} %bitcast.core_ref, bf16[8,32,2,8,128]{4,3,2,1,0:T(8,128)(2,1)S(1)} %bitcast.15, bf16[32,16,128]{2,1,0:T(8,128)(2,1)S(1)} %all-to-all-done.arrived_ref.message_ref, f32[16,128]{1,0:T(8,128)S(1)} %get-tuple-element.15.gain_ref, bf16[2048,256]{1,0:T(8,128)(2,1)} %bitcast.17, ...), custom_call_target="tpu_custom_call" | custom-call | tf_op jit(solution)/shard_map/experts/pallas_call | solution.py:273
  109.7 31.5 %all_to_all.32.arrived_ref = bf16[8,64,8,128]{3,2,1,0:T(8,128)(2,1)S(1)} all-to-all(bf16[8,64,8,128]{3,2,1,0:T(8,128)(2,1)S(1)} %bitcast.16), channel_id=1, replica_groups=mesh['sp'=32,'y'=8,'c'=2] {'y'}, dimensions={0} | all-to-all | bytes 2097152 | tf_op jit(solution)/shard_map/all_to_all | solution.py:17
  141.2 0.1 adding.1
  141.4 15.1 %all_to_all.33.arrived_ref = bf16[64,8,128]{2,1,0:T(8,128)(2,1)S(1)} all-to-all(bf16[64,8,128]{2,1,0:T(8,128)(2,1)S(1)} %adding.1), channel_id=1, replica_groups=mesh['sp'=32,'y'=8,'c'=2] {'sp','c'}, dimensions={0} | all-to-all | bytes 262144 | tf_op jit(solution)/shard_map/all_to_all | solution.py:17
  156.5 0.9 closing.1
  (7 shorter events, 0.0 us)
Async XLA Ops:
  1.8 23.1 %all-to-all-start = ((bf16[32,16,128]{2,1,0:T(8,128)(2,1)}), bf16[32,16,128]{2,1,0:T(8,128)(2,1)S(1)}, u32[]{:S(2)}, u32[]{:S(2)}) async-start(bf16[32,16,128]{2,1,0:T(8,128)(2,1)} %get-tuple-element.11), calls=%async_computation | async-start | bytes 262144 | tf_op jit(solution)/shard_map/all_to_all | solution.py:17
  71.1 3.7 %copy-start = (bf16[1,2048,256]{2,1,0:T(8,128)(2,1)S(1)}, bf16[1,2048,256]{2,1,0:T(8,128)(2,1)}, u32[]{:S(2)}) copy-start(bf16[1,2048,256]{2,1,0:T(8,128)(2,1)} %param.22) | copy-start | bytes 3145732
  71.1 6.0 %copy-start.1 = (bf16[1,2048,256]{2,1,0:T(8,128)(2,1)S(1)}, bf16[1,2048,256]{2,1,0:T(8,128)(2,1)}, u32[]{:S(2)}) copy-start(bf16[1,2048,256]{2,1,0:T(8,128)(2,1)} %param.23) | copy-start | bytes 3145732
  71.1 32.9 %all-to-all-start.3 = ((bf16[8,64,8,128]{3,2,1,0:T(8,128)(2,1)}), bf16[8,64,8,128]{3,2,1,0:T(8,128)(2,1)S(1)}, u32[]{:S(2)}, u32[]{:S(2)}) async-start(bf16[8,64,8,128]{3,2,1,0:T(8,128)(2,1)} %spreading.1), calls=%async_computation.3 | async-start | bytes 2097152 | tf_op jit(solution)/shard_map/all_to_all | solution.py:17
  74.8 14.8 %collective-permute-start = (bf16[2048,256]{1,0:T(8,128)(2,1)S(1)}, bf16[2048,256]{1,0:T(8,128)(2,1)}, u32[]{:S(2)}, u32[]{:S(2)}) collective-permute-start(bf16[2048,256]{1,0:T(8,128)(2,1)S(1)} %bitcast.18), channel_id=1, source_target_pairs={{0,1},{1,0},{2,3},{3,2},{4,5},{5,4},{6,7},{7,6},{8,9},{9,8},{10,11... | collective-permute-start | bytes 3145736 | tf_op jit(solution)/shard_map/ppermute | solution.py:322
  77.1 12.5 %collective-permute-start.1 = (bf16[2048,256]{1,0:T(8,128)(2,1)S(1)}, bf16[2048,256]{1,0:T(8,128)(2,1)}, u32[]{:S(2)}, u32[]{:S(2)}) collective-permute-start(bf16[2048,256]{1,0:T(8,128)(2,1)S(1)} %bitcast.20), channel_id=1, source_target_pairs={{0,1},{1,0},{2,3},{3,2},{4,5},{5,4},{6,7},{7,6},{8,9},{9,8},{10,11... | collective-permute-start | bytes 3145736 | tf_op jit(solution)/shard_map/ppermute | solution.py:322
  79.2 10.5 %collective-permute-start.2 = (bf16[256,2048]{1,0:T(8,128)(2,1)}, bf16[256,2048]{1,0:T(8,128)(2,1)}, u32[]{:S(2)}, u32[]{:S(2)}) collective-permute-start(bf16[256,2048]{1,0:T(8,128)(2,1)} %bitcast.21), channel_id=1, source_target_pairs={{0,1},{1,0},{2,3},{3,2},{4,5},{5,4},{6,7},{7,6},{8,9},{9,8},{10,11... | collective-permute-start | bytes 3145736 | tf_op jit(solution)/shard_map/ppermute | solution.py:322
  81.5 4.4 %collective-permute-start.3 = (bf16[64,2048]{1,0:T(8,128)(2,1)}, bf16[64,2048]{1,0:T(8,128)(2,1)}, u32[]{:S(2)}, u32[]{:S(2)}) collective-permute-start(bf16[64,2048]{1,0:T(8,128)(2,1)} %bitcast.23), channel_id=1, source_target_pairs={{0,1},{1,0},{2,3},{3,2},{4,5},{5,4},{6,7},{7,6},{8,9},{9,8},{10,11... | collective-permute-start | bytes 786440 | tf_op jit(solution)/shard_map/ppermute | solution.py:322
  83.5 4.4 %collective-permute-start.4 = (bf16[64,2048]{1,0:T(8,128)(2,1)}, bf16[64,2048]{1,0:T(8,128)(2,1)}, u32[]{:S(2)}, u32[]{:S(2)}) collective-permute-start(bf16[64,2048]{1,0:T(8,128)(2,1)} %bitcast.25), channel_id=1, source_target_pairs={{0,1},{1,0},{2,3},{3,2},{4,5},{5,4},{6,7},{7,6},{8,9},{9,8},{10,11... | collective-permute-start | bytes 786440 | tf_op jit(solution)/shard_map/ppermute | solution.py:322
  85.8 3.8 %collective-permute-start.5 = (bf16[64,2048]{1,0:T(8,128)(2,1)}, bf16[64,2048]{1,0:T(8,128)(2,1)}, u32[]{:S(2)}, u32[]{:S(2)}) collective-permute-start(bf16[64,2048]{1,0:T(8,128)(2,1)} %refs_10_.1), channel_id=1, source_target_pairs={{0,1},{1,0},{2,3},{3,2},{4,5},{5,4},{6,7},{7,6},{8,9},{9,8},{10,11... | collective-permute-start | bytes 786440 | tf_op jit(solution)/shard_map/ppermute | solution.py:322

commit v3 on v2

--- a/solution.py
+++ b/solution.py
@@ -6,11 +6,18 @@
 from jax.sharding import Mesh
 from jax.sharding import PartitionSpec as P
 
+
 F32 = jnp.float32
 BF16 = jnp.bfloat16
 SUM_LANE = 64
 W_LANE = 80
 META_LANE = 88
+
+
+SWAP = ((0, 1), (1, 0))
+AROUND = tuple(
+    (2 * y + c, 2 * ((y + (1 if c else -1)) % 8) + c) for y in range(8) for c in range(2)
+)
 
 
 def exchanged(value, axis):
@@ -176,74 +183,76 @@
 
 def spreading(arrived_ref, out_ref):
     for k in range(8):
-        out_ref[k] = arrived_ref[...]
-
-
-def experts(core_ref, x_ref, message_ref, gain_ref, *refs):
-    sources, out_ref, normed_ref = refs[:12], refs[12], refs[13]
-    near, landed = refs[14:26], refs[26]
+        out_ref[k] = arrived_ref[:, k % 2]
+
+
+def experts(place_ref, x_ref, message_ref, gain_ref, *refs):
+    sources, out_ref, normed_ref = refs[:16], refs[16], refs[17]
+    near, landed = refs[18:34], refs[34]
     copies = [
         pltpu.make_async_copy(source, target, landed.at[k])
         for k, (source, target) in enumerate(zip(sources, near))
     ]
-    order = (0, 2, 1, 3, 6, 7, 8, 9, 4, 5, 10, 11)
-    for k in order:
+    gates, ups, downs, packs = (near[4 * k : 4 * k + 4] for k in range(4))
+    for k in range(4):
         copies[k].start()
-    gate0, gate1, up0, up1, down0, down1, sgate0, sgate1, sup0, sup1, sdown0, sdown1 = near
-
-    squares = jnp.zeros((256, 128), F32)
+        copies[4 + k].start()
+    for k in (12, 13, 14, 15, 8, 9, 10, 11):
+        copies[k].start()
+
+    squares = jnp.zeros((128, 128), F32)
     for k in range(16):
-        part = x_ref[k // 2, :, k % 2].astype(F32).reshape(256, 128)
+        part = x_ref[k // 2, :, k % 2].astype(F32).reshape(128, 128)
         squares = squares + part * part
     scaling = lax.rsqrt(jnp.sum(squares, axis=1, keepdims=True) * (1.0 / 2048.0) + 1e-06)
     for k in range(16):
-        part = x_ref[k // 2, :, k % 2].astype(F32).reshape(256, 128)
+        part = x_ref[k // 2, :, k % 2].astype(F32).reshape(128, 128)
         normed_ref[:, 128 * k : 128 * (k + 1)] = (part * scaling * gain_ref[k : k + 1]).astype(
             BF16
         )
-    message = message_ref[...].astype(F32)
-    side = jnp.where(core_ref[0] == 0, message[:, 0:8], message[:, 8:16])
-    side = side.reshape(256, 128)
+    message = message_ref[...].astype(F32).reshape(16, 2, 16, 128)
+    message = jnp.where(place_ref[1] == 0, message[:, 0], message[:, 1])
+    side = jnp.where(place_ref[0] == 0, message[:, 0:8], message[:, 8:16])
+    side = side.reshape(128, 128)
     weight = side[:, W_LANE : W_LANE + 1] + (
         side[:, W_LANE + 1 : W_LANE + 2] + side[:, W_LANE + 2 : W_LANE + 3]
     )
     first = side[:, W_LANE + 3 : W_LANE + 4]
     normed = normed_ref[...]
-
-    def hidden(gate, up, factor):
-        upper = matmul(normed, up[...])
-        lower = matmul(normed, gate[...])
-        return (jax.nn.silu(lower) * upper * factor).astype(BF16)
-
-    copies[0].wait()
-    copies[2].wait()
-    left = hidden(gate0, up0, weight)
-    copies[1].wait()
-    copies[3].wait()
-    right = hidden(gate1, up1, weight)
-    for k in (6, 7, 8, 9):
+    hidden = []
+    for k in range(4):
         copies[k].wait()
-    across = jnp.concatenate([sgate0[...], sgate1[...], sup0[...], sup1[...]], axis=0)
+        copies[4 + k].wait()
+        lower = matmul(normed, gates[k][...])
+        upper = matmul(normed, ups[k][...])
+        hidden.append((jax.nn.silu(lower) * upper * weight).astype(BF16))
+    for k in range(12, 16):
+        copies[k].wait()
+    across = jnp.concatenate(
+        [pack[0:64] for pack in packs] + [pack[64:128] for pack in packs], axis=0
+    )
     both = lax.dot_general(
         normed, across, (((1,), (1,)), ((), ())), preferred_element_type=F32
     )
-    shared = (jax.nn.silu(both[:, :128]) * both[:, 128:] * first).astype(BF16)
-    for k in (4, 5, 10, 11):
+    shared = (jax.nn.silu(both[:, :256]) * both[:, 256:] * first).astype(BF16)
+    for k in range(8, 12):
         copies[k].wait()
-    sdown = jnp.concatenate([sdown0[...], sdown1[...]], axis=0)
+    shared_down = jnp.concatenate([pack[128:192] for pack in packs], axis=0)
     for k in range(8):
         cut = slice(256 * k, 256 * (k + 1))
-        total = matmul(left, down0[:, cut]) + matmul(right, down1[:, cut])
-        total = total + matmul(shared, sdown[:, cut])
-        out_ref[k, :, 0] = total[:, :128].reshape(32, 8, 128).astype(BF16)
-        out_ref[k, :, 1] = total[:, 128:].reshape(32, 8, 128).astype(BF16)
+        total = matmul(shared, shared_down[:, cut])
+        for value, down in zip(hidden, downs):
+            total = total + matmul(value, down[:, cut])
+        out_ref[k, :, 0] = total[:, :128].reshape(16, 8, 128).astype(BF16)
+        out_ref[k, :, 1] = total[:, 128:].reshape(16, 8, 128).astype(BF16)
 
 
 def adding(arrived_ref, out_ref):
-    total = arrived_ref[0].astype(F32)
-    for k in range(1, 8):
-        total = total + arrived_ref[k].astype(F32)
-    out_ref[...] = total.astype(BF16)
+    for side in (0, 1):
+        total = arrived_ref[side].astype(F32)
+        for k in range(2 + side, 8, 2):
+            total = total + arrived_ref[k].astype(F32)
+        out_ref[:, side] = total.astype(BF16)
 
 
 def closing(arrived_ref, slots_ref, hidden_ref, out_ref):
@@ -263,7 +272,7 @@
 HBM = pl.BlockSpec(memory_space=pl.ANY)
 
 
-def kernel(body, name, outs, operands, near=(), far=(), scalars=0, scratch=(), room=16):
+def kernel(body, outs, operands, near=(), far=(), scalars=0, scratch=(), room=16):
     near = [pltpu.with_memory_space_constraint(value, pltpu.VMEM) for value in near]
     far = [pltpu.with_memory_space_constraint(value, pltpu.HBM) for value in far]
     scalar = operands[:scalars]
@@ -272,7 +281,6 @@
     ]
     return pl.pallas_call(
         body,
-        name=name,
         out_shape=outs,
         in_specs=[SMEM] * scalars
         + [VMEM] * (len(near) + len(plain))
@@ -304,28 +312,27 @@
     shared_down,
 ):
     docs = doc_ids.reshape(1, 128)
+    own = {
+        "gate": expert_gate[0],
+        "up": expert_up[0],
+        "down": expert_down[0],
+    }
+    own["shared"] = jnp.concatenate([shared_gate.T, shared_up.T, shared_down], axis=0)
+    ring, own_other, ring_other = {}, {}, {}
+    for name, value in own.items():
+        ring[name] = lax.ppermute(value, ("y", "c"), AROUND)
+        own_other[name] = lax.ppermute(value, "c", SWAP)
+        ring_other[name] = lax.ppermute(ring[name], "c", SWAP)
+
     message, slots, values = kernel(
         opening,
-        "opening",
         (array((32, 16, 128), BF16), array((8, 128), F32), array((128, 64), BF16)),
         (pool_input.T, docs, routes.T, route_weights.T),
     )
-    swap = ((0, 1), (1, 0))
-    own = (
-        expert_gate[0],
-        expert_up[0],
-        expert_down[0],
-        shared_gate.T,
-        shared_up.T,
-        shared_down,
-    )
-    other = [lax.ppermute(value, "c", swap) for value in own]
     arrived = exchanged(message, "sp")
     index = lax.axis_index("sp").astype(jnp.int32).reshape(1)
-    core = lax.axis_index("c").astype(jnp.int32).reshape(1)
     terms = kernel(
         pooling,
-        "pooling",
         array((16, 136, 128), BF16),
         (index, docs, pool_gain.reshape(1, 64), out_proj, norm_gain.reshape(1, 128)),
         near=(arrived, values),
@@ -334,37 +341,38 @@
     terms = exchanged(terms, ("y", "c"))
     hidden_state, outgoing, gains = kernel(
         sending,
-        "sending",
         (array((128, 128), F32), array((64, 8, 128), BF16), array((16, 128), F32)),
         (residual,),
         near=(terms, slots),
     )
     rows = exchanged(outgoing, ("sp", "c"))
-    rows = kernel(spreading, "spreading", array((8, 64, 8, 128), BF16), (), near=(rows,))
+    rows = kernel(
+        spreading, array((8, 16, 2, 8, 128), BF16), (), near=(rows.reshape(16, 2, 2, 8, 128),)
+    )
     rows = exchanged(rows, "y")
-    pairs = [part for both in zip(own, other) for part in both]
+    place = jnp.stack([lax.axis_index("c"), lax.axis_index("y") & 1]).astype(jnp.int32)
+    groups = [
+        part
+        for name in own
+        for part in (own[name], own_other[name], ring[name], ring_other[name])
+    ]
     parts = kernel(
         experts,
-        "experts",
-        array((8, 32, 2, 8, 128), BF16),
-        (core,),
-        near=(rows.reshape(8, 32, 2, 8, 128), arrived, gains),
-        far=pairs,
+        array((8, 16, 2, 8, 128), BF16),
+        (place,),
+        near=(rows, arrived, gains),
+        far=groups,
         scalars=1,
-        scratch=[pltpu.VMEM((256, 2048), BF16)]
-        + [pltpu.VMEM(value.shape, BF16) for value in pairs]
-        + [pltpu.SemaphoreType.DMA((len(pairs),))],
-        room=24,
-    )
-    parts = exchanged(parts.reshape(8, 64, 8, 128), "y")
-    summed = kernel(adding, "adding", array((64, 8, 128), BF16), (), near=(parts,))
-    returned = exchanged(summed, ("sp", "c"))
+        scratch=[pltpu.VMEM((128, 2048), BF16)]
+        + [pltpu.VMEM(value.shape, BF16) for value in groups]
+        + [pltpu.SemaphoreType.DMA((len(groups),))],
+        room=32,
+    )
+    parts = exchanged(parts, "y")
+    summed = kernel(adding, array((16, 2, 2, 8, 128), BF16), (), near=(parts,))
+    returned = exchanged(summed.reshape(64, 8, 128), ("sp", "c"))
     return kernel(
-        closing,
-        "closing",
-        jax.ShapeDtypeStruct((128, 128), BF16),
-        (),
-        near=(returned, slots, hidden_state),
+        closing, jax.ShapeDtypeStruct((128, 128), BF16), (), near=(returned, slots, hidden_state)
     )
 
 
@@ -387,6 +395,4 @@
         P(None, tp),
         P(tp, None),
     )
-    return jax.shard_map(
-        body, mesh=split, in_specs=placed, out_specs=P("sp", tp), check_vma=False
-    )
+    return jax.shard_map(body, mesh=split, in_specs=placed, out_specs=P("sp", tp), check_vma=False)

time: 158 us -> 163 us (1.032)
  blocking collectives: 88.9 us -> 35.5 us
  starting transfers between devices: 30.4 us -> 62.5 us
  waiting for transfers between devices: 25.5 us -> 47.2 us
  Pallas kernels: 12.5 us -> 15.2 us
    all_to_all x4 -> x2, blocking collectives: 88.9 us -> 35.5 us  [exchanged(): return lax.all_to_all(value, axis, split_axis=0, concat_axis=0, tiled=True)]
    ppermute x6 -> x12, starting transfers between devices: 13 us -> 36.7 us  [the longest x4 16.7 us: body(): own_other[name] = lax.ppermute(value, 'c', SWAP)]
    ppermute x6 -> x12, waiting for transfers between devices: 1.74 us -> 21.5 us  [the longest x4 19.3 us: body(): ring[name] = lax.ppermute(value, ('y', 'c'), AROUND)]
    all_to_all x2 -> x4, starting transfers between devices: 17.4 us -> 25.8 us  [exchanged(): return lax.all_to_all(value, axis, split_axis=0, concat_axis=0, tiled=True)]
    pallas_call x7, Pallas kernels: 12.5 us -> 15.2 us  [kernel(): pl.pallas_call(body, out_shape=outs, in_specs=[SMEM] * scalars + [VMEM] *...]
    all_to_all x2 -> x4, waiting for transfers between devices: 23.7 us -> 25.6 us  [exchanged(): return lax.all_to_all(value, axis, split_axis=0, concat_axis=0, tiled=True)]
  transfers between devices with their start and end apart: 8 -> 16, of which waited for: 3 -> 7; matrix products, arithmetic and copies ran while one was open for 0% -> 0% of each run, Pallas kernels for 0% -> 4%
where the time goes in v3:
time: 163 us; the launch traced here: 162 us
  starting transfers between devices  62.5 us (38%)
  waiting for transfers between devices  47.2 us (29%)
  blocking collectives  35.5 us (22%)
  Pallas kernels  15.2 us (9%)
    all_to_all x2, blocking collectives, exchanged(): return lax.all_to_all(value, axis, split_axis=0, concat_axis=0, tiled=True)  35.5 us
    all_to_all x4, starting transfers between devices, exchanged(): return lax.all_to_all(value, axis, split_axis=0, concat_axis=0, tiled=True)  25.8 us
    all_to_all x4, waiting for transfers between devices, exchanged(): return lax.all_to_all(value, axis, split_axis=0, concat_axis=0, tiled=True)  25.6 us
    ppermute x4, waiting for transfers between devices, body(): ring[name] = lax.ppermute(value, ('y', 'c'), AROUND)  19.3 us
    ppermute x4, starting transfers between devices, body(): own_other[name] = lax.ppermute(value, 'c', SWAP)  16.7 us
    pallas_call x7, Pallas kernels, kernel(): pl.pallas_call(body, out_shape=outs, in_specs=[SMEM] * scalars + [VMEM] *...  15.2 us
    ppermute x4, starting transfers between devices, body(): ring[name] = lax.ppermute(value, ('y', 'c'), AROUND)  11.6 us
    ppermute x4, starting transfers between devices, body(): ring_other[name] = lax.ppermute(ring[name], 'c', SWAP)  8.43 us
  transfers between devices with their start and end apart: 16, of which 7 were waited for; matrix products, arithmetic and copies ran while one was open for 0% of the time, Pallas kernels for 4%

profile of v3, /device:TPU:1, one launch (start us, length us, event | category | flops | bytes accessed | tf_op | source)
XLA Modules:
  0.0 161.8 jit_solution(2095017801759043473)
XLA Ops:
  1.2 4.0 %collective-permute-start.10 = (bf16[192,2048]{1,0:T(8,128)(2,1)S(1)}, bf16[192,2048]{1,0:T(8,128)(2,1)}, u32[]{:S(2)}, u32[]{:S(2)}) collective-permute-start(bf16[192,2048]{1,0:T(8,128)(2,1)S(1)} %pad_maximum_fusion.refs_12_), channel_id=1, source_target_pairs={{0,14},{1,3},{2,0},{3,5},{4,2},{5,7},{6,4},{7,9},{8,6},{9,11},{10,... | collective-permute-start | bytes 2359304 | tf_op jit(solution)/shard_map/ppermute | solution.py:323
  5.2 6.6 %collective-permute-start.9 = (bf16[192,2048]{1,0:T(8,128)(2,1)S(1)}, bf16[192,2048]{1,0:T(8,128)(2,1)}, u32[]{:S(2)}, u32[]{:S(2)}) collective-permute-start(bf16[192,2048]{1,0:T(8,128)(2,1)S(1)} %pad_maximum_fusion.refs_12_), channel_id=1, source_target_pairs={{0,1},{1,0},{2,3},{3,2},{4,5},{5,4},{6,7},{7,6},{8,9},{9,8},{10,11... | collective-permute-start | bytes 2359304 | tf_op jit(solution)/shard_map/ppermute | solution.py:324
  13.7 11.0 %all-to-all-start = ((bf16[32,16,128]{2,1,0:T(8,128)(2,1)}), bf16[32,16,128]{2,1,0:T(8,128)(2,1)S(1)}, u32[]{:S(2)}, u32[]{:S(2)}) async-start(bf16[32,16,128]{2,1,0:T(8,128)(2,1)} %get-tuple-element.11), calls=%async_computation | async-start | bytes 262144 | tf_op jit(solution)/shard_map/all_to_all | solution.py:24
  24.7 9.9 %all-to-all-done.arrived_ref.message_ref = bf16[32,16,128]{2,1,0:T(8,128)(2,1)S(1)} async-done(((bf16[32,16,128]{2,1,0:T(8,128)(2,1)}), bf16[32,16,128]{2,1,0:T(8,128)(2,1)S(1)}, u32[]{:S(2)}, u32[]{:S(2)}) %all-to-all-start) | async-done | bytes 131104 | tf_op jit(solution)/shard_map/all_to_all | solution.py:24
  34.6 2.7 %shard_map.137 = bf16[16,136,128]{2,1,0:T(8,128)(2,1)} custom-call(s32[1]{0:T(128)} %bitcast.2.index_ref, bf16[32,16,128]{2,1,0:T(8,128)(2,1)S(1)} %all-to-all-done.arrived_ref.message_ref, bf16[128,64]{1,0:T(8,128)(2,1)S(1)} %get-tuple-element.12.pool_ref, s32[1,128]{1,0:T(1,128)} %bitcast.31, f32[1,64]{1,0:T(1,128)} %bitcast.34, ...), custom_call_target="tpu_custom_call" | custom-call | tf_op jit(solution)/shard_map/pallas_call | solution.py:282
  37.3 5.6 %all-to-all-start.1 = ((bf16[16,136,128]{2,1,0:T(8,128)(2,1)}), bf16[16,136,128]{2,1,0:T(8,128)(2,1)S(1)}, u32[]{:S(2)}, u32[]{:S(2)}) async-start(bf16[16,136,128]{2,1,0:T(8,128)(2,1)} %shard_map.137), calls=%async_computation.1 | async-start | bytes 1114112 | tf_op jit(solution)/shard_map/all_to_all | solution.py:24
  42.9 3.3 %collective-permute-start.1 = (bf16[2048,256]{1,0:T(8,128)(2,1)S(1)}, bf16[2048,256]{1,0:T(8,128)(2,1)}, u32[]{:S(2)}, u32[]{:S(2)}) collective-permute-start(bf16[2048,256]{1,0:T(8,128)(2,1)S(1)} %bitcast.19), channel_id=1, source_target_pairs={{0,14},{1,3},{2,0},{3,5},{4,2},{5,7},{6,4},{7,9},{8,6},{9,11},{10,... | collective-permute-start | bytes 3145736 | tf_op jit(solution)/shard_map/ppermute | solution.py:323
  46.2 3.8 %collective-permute-start = (bf16[2048,256]{1,0:T(8,128)(2,1)S(1)}, bf16[2048,256]{1,0:T(8,128)(2,1)}, u32[]{:S(2)}, u32[]{:S(2)}) collective-permute-start(bf16[2048,256]{1,0:T(8,128)(2,1)S(1)} %bitcast.20), channel_id=1, source_target_pairs={{0,1},{1,0},{2,3},{3,2},{4,5},{5,4},{6,7},{7,6},{8,9},{9,8},{10,11... | collective-permute-start | bytes 3145736 | tf_op jit(solution)/shard_map/ppermute | solution.py:324
  50.0 1.9 %collective-permute-start.4 = (bf16[2048,256]{1,0:T(8,128)(2,1)}, bf16[2048,256]{1,0:T(8,128)(2,1)}, u32[]{:S(2)}, u32[]{:S(2)}) collective-permute-start(bf16[2048,256]{1,0:T(8,128)(2,1)} %bitcast.21), channel_id=1, source_target_pairs={{0,14},{1,3},{2,0},{3,5},{4,2},{5,7},{6,4},{7,9},{8,6},{9,11},{10,... | collective-permute-start | bytes 3145736 | tf_op jit(solution)/shard_map/ppermute | solution.py:323
  51.9 2.4 %collective-permute-start.7 = (bf16[256,2048]{1,0:T(8,128)(2,1)}, bf16[256,2048]{1,0:T(8,128)(2,1)}, u32[]{:S(2)}, u32[]{:S(2)}) collective-permute-start(bf16[256,2048]{1,0:T(8,128)(2,1)} %bitcast.24), channel_id=1, source_target_pairs={{0,14},{1,3},{2,0},{3,5},{4,2},{5,7},{6,4},{7,9},{8,6},{9,11},{10,... | collective-permute-start | bytes 3145736 | tf_op jit(solution)/shard_map/ppermute | solution.py:323
  54.4 4.4 %collective-permute-start.3 = (bf16[2048,256]{1,0:T(8,128)(2,1)}, bf16[2048,256]{1,0:T(8,128)(2,1)}, u32[]{:S(2)}, u32[]{:S(2)}) collective-permute-start(bf16[2048,256]{1,0:T(8,128)(2,1)} %bitcast.22), channel_id=1, source_target_pairs={{0,1},{1,0},{2,3},{3,2},{4,5},{5,4},{6,7},{7,6},{8,9},{9,8},{10,11... | collective-permute-start | bytes 3145736 | tf_op jit(solution)/shard_map/ppermute | solution.py:324
  58.7 2.3 %all-to-all-done.1.arrived_ref = bf16[16,136,128]{2,1,0:T(8,128)(2,1)S(1)} async-done(((bf16[16,136,128]{2,1,0:T(8,128)(2,1)}), bf16[16,136,128]{2,1,0:T(8,128)(2,1)S(1)}, u32[]{:S(2)}, u32[]{:S(2)}) %all-to-all-start.1) | async-done | bytes 557088 | tf_op jit(solution)/shard_map/all_to_all | solution.py:24
  62.6 4.2 %all-to-all-start.2 = ((bf16[64,8,128]{2,1,0:T(8,128)(2,1)}), bf16[64,8,128]{2,1,0:T(8,128)(2,1)S(1)}, u32[]{:S(2)}, u32[]{:S(2)}) async-start(bf16[64,8,128]{2,1,0:T(8,128)(2,1)} %get-tuple-element.14), calls=%async_computation.2 | async-start | bytes 262144 | tf_op jit(solution)/shard_map/all_to_all | solution.py:24
  66.8 3.3 %collective-permute-done.1.refs_2_ = bf16[2048,256]{1,0:T(8,128)(2,1)} collective-permute-done((bf16[2048,256]{1,0:T(8,128)(2,1)S(1)}, bf16[2048,256]{1,0:T(8,128)(2,1)}, u32[]{:S(2)}, u32[]{:S(2)}) %collective-permute-start.1) | collective-permute-done | bytes 1048608 | tf_op jit(solution)/shard_map/ppermute | solution.py:323
  72.0 2.4 %collective-permute-start.2 = (bf16[2048,256]{1,0:T(8,128)(2,1)}, bf16[2048,256]{1,0:T(8,128)(2,1)S(1)}, u32[]{:S(2)}, u32[]{:S(2)}) collective-permute-start(bf16[2048,256]{1,0:T(8,128)(2,1)} %collective-permute-done.1.refs_2_), channel_id=1, source_target_pairs={{0,1},{1,0},{2,3},{3,2},{4,5},{5,4},{6,7},{7,6},{8,9},{9,8},{10,11... | collective-permute-start | bytes 3145736 | tf_op jit(solution)/shard_map/ppermute | solution.py:325
  74.5 6.7 %collective-permute-done.4.refs_6_ = bf16[2048,256]{1,0:T(8,128)(2,1)} collective-permute-done((bf16[2048,256]{1,0:T(8,128)(2,1)}, bf16[2048,256]{1,0:T(8,128)(2,1)}, u32[]{:S(2)}, u32[]{:S(2)}) %collective-permute-start.4) | collective-permute-done | bytes 1048608 | tf_op jit(solution)/shard_map/ppermute | solution.py:323
  83.1 9.3 %collective-permute-done.7.refs_10_ = bf16[256,2048]{1,0:T(8,128)(2,1)} collective-permute-done((bf16[256,2048]{1,0:T(8,128)(2,1)}, bf16[256,2048]{1,0:T(8,128)(2,1)}, u32[]{:S(2)}, u32[]{:S(2)}) %collective-permute-start.7) | collective-permute-done | bytes 1048608 | tf_op jit(solution)/shard_map/ppermute | solution.py:323
  95.2 4.9 %all-to-all-start.3 = ((bf16[8,16,2,8,128]{4,3,2,1,0:T(8,128)(2,1)}), bf16[8,16,2,8,128]{4,3,2,1,0:T(8,128)(2,1)S(1)}, u32[]{:S(2)}, u32[]{:S(2)}) async-start(bf16[8,16,2,8,128]{4,3,2,1,0:T(8,128)(2,1)} %shard_map.139), calls=%async_computation.3 | async-start | bytes 1048576 | tf_op jit(solution)/shard_map/all_to_all | solution.py:24
  100.2 2.2 %collective-permute-start.11 = (bf16[192,2048]{1,0:T(8,128)(2,1)}, bf16[192,2048]{1,0:T(8,128)(2,1)}, u32[]{:S(2)}, u32[]{:S(2)}) collective-permute-start(bf16[192,2048]{1,0:T(8,128)(2,1)} %collective-permute-done.10.refs_14_), channel_id=1, source_target_pairs={{0,1},{1,0},{2,3},{3,2},{4,5},{5,4},{6,7},{7,6},{8,9},{9,8},{10,11... | collective-permute-start | bytes 2359304 | tf_op jit(solution)/shard_map/ppermute | solution.py:325
  102.5 2.2 %collective-permute-done.11.refs_15_ = bf16[192,2048]{1,0:T(8,128)(2,1)} collective-permute-done((bf16[192,2048]{1,0:T(8,128)(2,1)}, bf16[192,2048]{1,0:T(8,128)(2,1)}, u32[]{:S(2)}, u32[]{:S(2)}) %collective-permute-start.11) | collective-permute-done | bytes 786464 | tf_op jit(solution)/shard_map/ppermute | solution.py:325
  104.7 13.5 %all-to-all-done.3.x_ref = bf16[8,16,2,8,128]{4,3,2,1,0:T(8,128)(2,1)S(1)} async-done(((bf16[8,16,2,8,128]{4,3,2,1,0:T(8,128)(2,1)}), bf16[8,16,2,8,128]{4,3,2,1,0:T(8,128)(2,1)S(1)}, u32[]{:S(2)}, u32[]{:S(2)}) %all-to-all-start.3) | async-done | bytes 524320 | tf_op jit(solution)/shard_map/all_to_all | solution.py:24
  118.2 7.1 %shard_map.140 = bf16[8,16,2,8,128]{4,3,2,1,0:T(8,128)(2,1)S(1)} custom-call(s32[2]{0:T(128)S(1)} %pad_add_fusion.place_ref, bf16[8,16,2,8,128]{4,3,2,1,0:T(8,128)(2,1)S(1)} %all-to-all-done.3.x_ref, bf16[32,16,128]{2,1,0:T(8,128)(2,1)S(1)} %all-to-all-done.arrived_ref.message_ref, f32[16,128]{1,0:T(8,128)S(1)} %get-tuple-element.15.gain_ref, ...), custom_call_target="tpu_custom_call" | custom-call | tf_op jit(solution)/shard_map/pallas_call | solution.py:282
  125.3 20.3 %all_to_all.30.arrived_ref = bf16[8,16,2,8,128]{4,3,2,1,0:T(8,128)(2,1)S(1)} all-to-all(bf16[8,16,2,8,128]{4,3,2,1,0:T(8,128)(2,1)S(1)} %shard_map.140), channel_id=1, replica_groups=mesh['sp'=32,'y'=8,'c'=2] {'y'}, dimensions={0} | all-to-all | bytes 1048576 | tf_op jit(solution)/shard_map/all_to_all | solution.py:24
  145.6 15.2 %all_to_all.31.arrived_ref = bf16[64,8,128]{2,1,0:T(8,128)(2,1)S(1)} all-to-all(bf16[64,8,128]{2,1,0:T(8,128)(2,1)S(1)} %bitcast.17), channel_id=1, replica_groups=mesh['sp'=32,'y'=8,'c'=2] {'sp','c'}, dimensions={0} | all-to-all | bytes 262144 | tf_op jit(solution)/shard_map/all_to_all | solution.py:24
  (27 shorter events, 12.4 us)
Async XLA Ops:
  1.2 36.1 %copy-start = (bf16[192,2048]{1,0:T(8,128)(2,1)}, bf16[192,2048]{1,0:T(8,128)(2,1)S(1)}, u32[]{:S(2)}) copy-start(bf16[192,2048]{1,0:T(8,128)(2,1)S(1)} %pad_maximum_fusion.refs_12_) | copy-start | bytes 2359300
  1.2 50.8 %collective-permute-start.10 = (bf16[192,2048]{1,0:T(8,128)(2,1)S(1)}, bf16[192,2048]{1,0:T(8,128)(2,1)}, u32[]{:S(2)}, u32[]{:S(2)}) collective-permute-start(bf16[192,2048]{1,0:T(8,128)(2,1)S(1)} %pad_maximum_fusion.refs_12_), channel_id=1, source_target_pairs={{0,14},{1,3},{2,0},{3,5},{4,2},{5,7},{6,4},{7,9},{8,6},{9,11},{10,... | collective-permute-start | bytes 2359304 | tf_op jit(solution)/shard_map/ppermute | solution.py:323
  5.2 49.1 %collective-permute-start.9 = (bf16[192,2048]{1,0:T(8,128)(2,1)S(1)}, bf16[192,2048]{1,0:T(8,128)(2,1)}, u32[]{:S(2)}, u32[]{:S(2)}) collective-permute-start(bf16[192,2048]{1,0:T(8,128)(2,1)S(1)} %pad_maximum_fusion.refs_12_), channel_id=1, source_target_pairs={{0,1},{1,0},{2,3},{3,2},{4,5},{5,4},{6,7},{7,6},{8,9},{9,8},{10,11... | collective-permute-start | bytes 2359304 | tf_op jit(solution)/shard_map/ppermute | solution.py:324
  13.7 20.9 %all-to-all-start = ((bf16[32,16,128]{2,1,0:T(8,128)(2,1)}), bf16[32,16,128]{2,1,0:T(8,128)(2,1)S(1)}, u32[]{:S(2)}, u32[]{:S(2)}) async-start(bf16[32,16,128]{2,1,0:T(8,128)(2,1)} %get-tuple-element.11), calls=%async_computation | async-start | bytes 262144 | tf_op jit(solution)/shard_map/all_to_all | solution.py:24
  34.6 8.3 %copy-start.1 = (bf16[1,2048,256]{2,1,0:T(8,128)(2,1)S(1)}, bf16[1,2048,256]{2,1,0:T(8,128)(2,1)}, u32[]{:S(2)}) copy-start(bf16[1,2048,256]{2,1,0:T(8,128)(2,1)} %param.22) | copy-start | bytes 3145732
  37.3 23.7 %all-to-all-start.1 = ((bf16[16,136,128]{2,1,0:T(8,128)(2,1)}), bf16[16,136,128]{2,1,0:T(8,128)(2,1)S(1)}, u32[]{:S(2)}, u32[]{:S(2)}) async-start(bf16[16,136,128]{2,1,0:T(8,128)(2,1)} %shard_map.137), calls=%async_computation.1 | async-start | bytes 1114112 | tf_op jit(solution)/shard_map/all_to_all | solution.py:24
  42.9 27.2 %collective-permute-start.1 = (bf16[2048,256]{1,0:T(8,128)(2,1)S(1)}, bf16[2048,256]{1,0:T(8,128)(2,1)}, u32[]{:S(2)}, u32[]{:S(2)}) collective-permute-start(bf16[2048,256]{1,0:T(8,128)(2,1)S(1)} %bitcast.19), channel_id=1, source_target_pairs={{0,14},{1,3},{2,0},{3,5},{4,2},{5,7},{6,4},{7,9},{8,6},{9,11},{10,... | collective-permute-start | bytes 3145736 | tf_op jit(solution)/shard_map/ppermute | solution.py:323
  46.2 25.8 %collective-permute-start = (bf16[2048,256]{1,0:T(8,128)(2,1)S(1)}, bf16[2048,256]{1,0:T(8,128)(2,1)}, u32[]{:S(2)}, u32[]{:S(2)}) collective-permute-start(bf16[2048,256]{1,0:T(8,128)(2,1)S(1)} %bitcast.20), channel_id=1, source_target_pairs={{0,1},{1,0},{2,3},{3,2},{4,5},{5,4},{6,7},{7,6},{8,9},{9,8},{10,11... | collective-permute-start | bytes 3145736 | tf_op jit(solution)/shard_map/ppermute | solution.py:324
  50.0 31.1 %collective-permute-start.4 = (bf16[2048,256]{1,0:T(8,128)(2,1)}, bf16[2048,256]{1,0:T(8,128)(2,1)}, u32[]{:S(2)}, u32[]{:S(2)}) collective-permute-start(bf16[2048,256]{1,0:T(8,128)(2,1)} %bitcast.21), channel_id=1, source_target_pairs={{0,14},{1,3},{2,0},{3,5},{4,2},{5,7},{6,4},{7,9},{8,6},{9,11},{10,... | collective-permute-start | bytes 3145736 | tf_op jit(solution)/shard_map/ppermute | solution.py:323
  51.9 40.4 %collective-permute-start.7 = (bf16[256,2048]{1,0:T(8,128)(2,1)}, bf16[256,2048]{1,0:T(8,128)(2,1)}, u32[]{:S(2)}, u32[]{:S(2)}) collective-permute-start(bf16[256,2048]{1,0:T(8,128)(2,1)} %bitcast.24), channel_id=1, source_target_pairs={{0,14},{1,3},{2,0},{3,5},{4,2},{5,7},{6,4},{7,9},{8,6},{9,11},{10,... | collective-permute-start | bytes 3145736 | tf_op jit(solution)/shard_map/ppermute | solution.py:323
  54.4 45.8 %collective-permute-start.3 = (bf16[2048,256]{1,0:T(8,128)(2,1)}, bf16[2048,256]{1,0:T(8,128)(2,1)}, u32[]{:S(2)}, u32[]{:S(2)}) collective-permute-start(bf16[2048,256]{1,0:T(8,128)(2,1)} %bitcast.22), channel_id=1, source_target_pairs={{0,1},{1,0},{2,3},{3,2},{4,5},{5,4},{6,7},{7,6},{8,9},{9,8},{10,11... | collective-permute-start | bytes 3145736 | tf_op jit(solution)/shard_map/ppermute | solution.py:324
  62.6 31.7 %all-to-all-start.2 = ((bf16[64,8,128]{2,1,0:T(8,128)(2,1)}), bf16[64,8,128]{2,1,0:T(8,128)(2,1)S(1)}, u32[]{:S(2)}, u32[]{:S(2)}) async-start(bf16[64,8,128]{2,1,0:T(8,128)(2,1)} %get-tuple-element.14), calls=%async_computation.2 | async-start | bytes 262144 | tf_op jit(solution)/shard_map/all_to_all | solution.py:24
  70.1 32.4 %collective-permute-start.6 = (bf16[256,2048]{1,0:T(8,128)(2,1)}, bf16[256,2048]{1,0:T(8,128)(2,1)S(1)}, u32[]{:S(2)}, u32[]{:S(2)}) collective-permute-start(bf16[256,2048]{1,0:T(8,128)(2,1)} %bitcast.25), channel_id=1, source_target_pairs={{0,1},{1,0},{2,3},{3,2},{4,5},{5,4},{6,7},{7,6},{8,9},{9,8},{10,11... | collective-permute-start | bytes 3145736 | tf_op jit(solution)/shard_map/ppermute | solution.py:324
  72.0 32.7 %collective-permute-start.2 = (bf16[2048,256]{1,0:T(8,128)(2,1)}, bf16[2048,256]{1,0:T(8,128)(2,1)S(1)}, u32[]{:S(2)}, u32[]{:S(2)}) collective-permute-start(bf16[2048,256]{1,0:T(8,128)(2,1)} %collective-permute-done.1.refs_2_), channel_id=1, source_target_pairs={{0,1},{1,0},{2,3},{3,2},{4,5},{5,4},{6,7},{7,6},{8,9},{9,8},{10,11... | collective-permute-start | bytes 3145736 | tf_op jit(solution)/shard_map/ppermute | solution.py:325
  81.2 23.6 %collective-permute-start.5 = (bf16[2048,256]{1,0:T(8,128)(2,1)}, bf16[2048,256]{1,0:T(8,128)(2,1)}, u32[]{:S(2)}, u32[]{:S(2)}) collective-permute-start(bf16[2048,256]{1,0:T(8,128)(2,1)} %collective-permute-done.4.refs_6_), channel_id=1, source_target_pairs={{0,1},{1,0},{2,3},{3,2},{4,5},{5,4},{6,7},{7,6},{8,9},{9,8},{10,11... | collective-permute-start | bytes 3145736 | tf_op jit(solution)/shard_map/ppermute | solution.py:325
  92.4 12.3 %collective-permute-start.8 = (bf16[256,2048]{1,0:T(8,128)(2,1)}, bf16[256,2048]{1,0:T(8,128)(2,1)}, u32[]{:S(2)}, u32[]{:S(2)}) collective-permute-start(bf16[256,2048]{1,0:T(8,128)(2,1)} %collective-permute-done.7.refs_10_), channel_id=1, source_target_pairs={{0,1},{1,0},{2,3},{3,2},{4,5},{5,4},{6,7},{7,6},{8,9},{9,8},{10,11... | collective-permute-start | bytes 3145736 | tf_op jit(solution)/shard_map/ppermute | solution.py:325
  95.2 23.0 %all-to-all-start.3 = ((bf16[8,16,2,8,128]{4,3,2,1,0:T(8,128)(2,1)}), bf16[8,16,2,8,128]{4,3,2,1,0:T(8,128)(2,1)S(1)}, u32[]{:S(2)}, u32[]{:S(2)}) async-start(bf16[8,16,2,8,128]{4,3,2,1,0:T(8,128)(2,1)} %shard_map.139), calls=%async_computation.3 | async-start | bytes 1048576 | tf_op jit(solution)/shard_map/all_to_all | solution.py:24
  100.2 4.5 %collective-permute-start.11 = (bf16[192,2048]{1,0:T(8,128)(2,1)}, bf16[192,2048]{1,0:T(8,128)(2,1)}, u32[]{:S(2)}, u32[]{:S(2)}) collective-permute-start(bf16[192,2048]{1,0:T(8,128)(2,1)} %collective-permute-done.10.refs_14_), channel_id=1, source_target_pairs={{0,1},{1,0},{2,3},{3,2},{4,5},{5,4},{6,7},{7,6},{8,9},{9,8},{10,11... | collective-permute-start | bytes 2359304 | tf_op jit(solution)/shard_map/ppermute | solution.py:325
  102.5 15.7 %copy-start.2 = (bf16[256,2048]{1,0:T(8,128)(2,1)}, bf16[256,2048]{1,0:T(8,128)(2,1)S(1)}, u32[]{:S(2)}) copy-start(bf16[256,2048]{1,0:T(8,128)(2,1)S(1)} %collective-permute-done.6.refs_9_) | copy-start | bytes 3145732
  104.7 13.5 %copy-start.3 = (bf16[2048,256]{1,0:T(8,128)(2,1)}, bf16[2048,256]{1,0:T(8,128)(2,1)S(1)}, u32[]{:S(2)}) copy-start(bf16[2048,256]{1,0:T(8,128)(2,1)S(1)} %collective-permute-done.2.refs_3_) | copy-start | bytes 3145732

commit v4 on v3

--- a/solution.py
+++ b/solution.py
@@ -39,7 +39,25 @@
     return jnp.dot(a, b, preferred_element_type=F32)
 
 
-def opening(pool_ref, docs_ref, routes_ref, weights_ref, message_ref, slots_ref, values_ref):
+def opening(
+    pool_ref,
+    docs_ref,
+    routes_ref,
+    weights_ref,
+    gate_ref,
+    up_ref,
+    message_ref,
+    slots_ref,
+    values_ref,
+    pack_ref,
+    packed,
+):
+    copies = [
+        pltpu.make_async_copy(source, pack_ref.at[k], packed.at[k])
+        for k, source in enumerate((gate_ref, up_ref))
+    ]
+    for copy in copies:
+        copy.start()
     channels, rows = pool_ref.shape
     square = (rows, rows)
     values = pool_ref[...].astype(F32).T.astype(BF16)
@@ -95,6 +113,22 @@
     for k, value in enumerate((*three_parts(weight), chosen_first)):
         message = jnp.where(place == W_LANE + k, value, message)
     message_ref[...] = message.reshape(32, 16, 128).astype(BF16)
+    for copy in copies:
+        copy.wait()
+
+
+def packing(*refs):
+    sources, pack_ref, packed = refs[:4], refs[4], refs[5]
+    copies, start = [], 0
+    for k, source in enumerate(sources):
+        rows = source.shape[0]
+        copies.append(
+            pltpu.make_async_copy(source, pack_ref.at[start : start + rows], packed.at[k])
+        )
+        copies[-1].start()
+        start += rows
+    for copy in copies:
+        copy.wait()
 
 
 def pooling(
@@ -187,18 +221,15 @@
 
 
 def experts(place_ref, x_ref, message_ref, gain_ref, *refs):
-    sources, out_ref, normed_ref = refs[:16], refs[16], refs[17]
-    near, landed = refs[18:34], refs[34]
+    sources, out_ref, normed_ref = refs[:8], refs[8], refs[9]
+    near, landed = refs[10:18], refs[18]
     copies = [
         pltpu.make_async_copy(source, target, landed.at[k])
         for k, (source, target) in enumerate(zip(sources, near))
     ]
-    gates, ups, downs, packs = (near[4 * k : 4 * k + 4] for k in range(4))
-    for k in range(4):
-        copies[k].start()
-        copies[4 + k].start()
-    for k in (12, 13, 14, 15, 8, 9, 10, 11):
-        copies[k].start()
+    for copy in copies[:2]:
+        copy.start()
+    uppers, lowers = near[:4], near[4:]
 
     squares = jnp.zeros((128, 128), F32)
     for k in range(16):
@@ -222,27 +253,28 @@
     hidden = []
     for k in range(4):
         copies[k].wait()
-        copies[4 + k].wait()
-        lower = matmul(normed, gates[k][...])
-        upper = matmul(normed, ups[k][...])
+        copies[k + 2].start()
+        if k == 3:
+            copies[6].start()
+            copies[7].start()
+        lower = matmul(normed, uppers[k][0])
+        upper = matmul(normed, uppers[k][1])
         hidden.append((jax.nn.silu(lower) * upper * weight).astype(BF16))
-    for k in range(12, 16):
-        copies[k].wait()
+    for copy in copies[4:]:
+        copy.wait()
     across = jnp.concatenate(
-        [pack[0:64] for pack in packs] + [pack[64:128] for pack in packs], axis=0
+        [pack[256:320] for pack in lowers] + [pack[320:384] for pack in lowers], axis=0
     )
     both = lax.dot_general(
         normed, across, (((1,), (1,)), ((), ())), preferred_element_type=F32
     )
     shared = (jax.nn.silu(both[:, :256]) * both[:, 256:] * first).astype(BF16)
-    for k in range(8, 12):
-        copies[k].wait()
-    shared_down = jnp.concatenate([pack[128:192] for pack in packs], axis=0)
+    shared_down = jnp.concatenate([pack[384:448] for pack in lowers], axis=0)
     for k in range(8):
         cut = slice(256 * k, 256 * (k + 1))
         total = matmul(shared, shared_down[:, cut])
-        for value, down in zip(hidden, downs):
-            total = total + matmul(value, down[:, cut])
+        for value, pack in zip(hidden, lowers):
+            total = total + matmul(value, pack[0:256, cut])
         out_ref[k, :, 0] = total[:, :128].reshape(16, 8, 128).astype(BF16)
         out_ref[k, :, 1] = total[:, 128:].reshape(16, 8, 128).astype(BF16)
 
@@ -270,6 +302,15 @@
 
 
 HBM = pl.BlockSpec(memory_space=pl.ANY)
+
+
+def is_array(value):
+    return not isinstance(value, tuple)
+
+
+def spec_of(value):
+    far = getattr(value, "memory_space", None) == pltpu.HBM
+    return HBM if far else VMEM
 
 
 def kernel(body, outs, operands, near=(), far=(), scalars=0, scratch=(), room=16):
@@ -285,7 +326,7 @@
         in_specs=[SMEM] * scalars
         + [VMEM] * (len(near) + len(plain))
         + [HBM] * len(far),
-        out_specs=jax.tree.map(lambda _: VMEM, outs),
+        out_specs=jax.tree.map(spec_of, outs, is_leaf=is_array),
         scratch_shapes=scratch,
         compiler_params=pltpu.CompilerParams(vmem_limit_bytes=room * 2**20),
     )(*scalar, *near, *plain, *far)
@@ -312,23 +353,32 @@
     shared_down,
 ):
     docs = doc_ids.reshape(1, 128)
-    own = {
-        "gate": expert_gate[0],
-        "up": expert_up[0],
-        "down": expert_down[0],
-    }
-    own["shared"] = jnp.concatenate([shared_gate.T, shared_up.T, shared_down], axis=0)
-    ring, own_other, ring_other = {}, {}, {}
-    for name, value in own.items():
-        ring[name] = lax.ppermute(value, ("y", "c"), AROUND)
-        own_other[name] = lax.ppermute(value, "c", SWAP)
-        ring_other[name] = lax.ppermute(ring[name], "c", SWAP)
-
-    message, slots, values = kernel(
+    message, slots, values, upper = kernel(
         opening,
-        (array((32, 16, 128), BF16), array((8, 128), F32), array((128, 64), BF16)),
+        (
+            array((32, 16, 128), BF16),
+            array((8, 128), F32),
+            array((128, 64), BF16),
+            pltpu.HBM((2, 2048, 256), BF16),
+        ),
         (pool_input.T, docs, routes.T, route_weights.T),
-    )
+        far=(expert_gate[0], expert_up[0]),
+        scratch=[pltpu.SemaphoreType.DMA((2,))],
+    )
+    lower = kernel(
+        packing,
+        pltpu.HBM((448, 2048), BF16),
+        (),
+        far=(expert_down[0], shared_gate.T, shared_up.T, shared_down),
+        scratch=[pltpu.SemaphoreType.DMA((4,))],
+    )
+    uppers, lowers = [upper], [lower]
+    for group in (uppers, lowers):
+        value = group[0]
+        ring = lax.ppermute(value, ("y", "c"), AROUND)
+        own_other = lax.ppermute(value, "c", SWAP)
+        ring_other = lax.ppermute(ring, "c", SWAP)
+        group += [own_other, ring, ring_other]
     arrived = exchanged(message, "sp")
     index = lax.axis_index("sp").astype(jnp.int32).reshape(1)
     terms = kernel(
@@ -351,11 +401,7 @@
     )
     rows = exchanged(rows, "y")
     place = jnp.stack([lax.axis_index("c"), lax.axis_index("y") & 1]).astype(jnp.int32)
-    groups = [
-        part
-        for name in own
-        for part in (own[name], own_other[name], ring[name], ring_other[name])
-    ]
+    groups = uppers + lowers
     parts = kernel(
         experts,
         array((8, 16, 2, 8, 128), BF16),
@@ -365,8 +411,8 @@
         scalars=1,
         scratch=[pltpu.VMEM((128, 2048), BF16)]
         + [pltpu.VMEM(value.shape, BF16) for value in groups]
-        + [pltpu.SemaphoreType.DMA((len(groups),))],
-        room=32,
+        + [pltpu.SemaphoreType.DMA((8,))],
+        room=24,
     )
     parts = exchanged(parts, "y")
     summed = kernel(adding, array((16, 2, 2, 8, 128), BF16), (), near=(parts,))

time: 163 us -> 265 us (1.63)
  Pallas kernels: 15.2 us -> 137 us
  starting transfers between devices: 62.5 us -> 40.2 us
  blocking collectives: 35.5 us -> 50 us
  waiting for transfers between devices: 47.2 us -> 36.3 us
    pallas_call x7 -> x8, Pallas kernels: 15.2 us -> 137 us  [kernel(): pl.pallas_call(body, out_shape=outs, in_specs=[SMEM] * scalars + [VMEM] *...]
    ppermute x12 -> x6, waiting for transfers between devices: 21.5 us -> 0.02 us  [the longest x2 0.01 us: body(): ring = lax.ppermute(value, ('y', 'c'), AROUND)]
    ppermute x12 -> x6, starting transfers between devices: 36.7 us -> 16 us  [the longest x2 7.36 us: body(): ring = lax.ppermute(value, ('y', 'c'), AROUND)]
    all_to_all x2 -> x3, blocking collectives: 35.5 us -> 50 us  [exchanged(): return lax.all_to_all(value, axis, split_axis=0, concat_axis=0, tiled=True)]
    all_to_all x4 -> x3, waiting for transfers between devices: 25.6 us -> 36.3 us  [exchanged(): return lax.all_to_all(value, axis, split_axis=0, concat_axis=0, tiled=True)]
    all_to_all x4 -> x3, starting transfers between devices: 25.8 us -> 24.2 us  [exchanged(): return lax.all_to_all(value, axis, split_axis=0, concat_axis=0, tiled=True)]
  transfers between devices with their start and end apart: 16 -> 9, of which waited for: 7 -> 3; matrix products, arithmetic and copies ran while one was open for 0% -> 0% of each run, Pallas kernels for 4% -> 23%
where the time goes in v4:
time: 265 us; the launch traced here: 264 us
  Pallas kernels  137 us (52%)
  blocking collectives  50 us (19%)
  starting transfers between devices  40.2 us (15%)
  waiting for transfers between devices  36.3 us (14%)
    pallas_call x8, Pallas kernels, kernel(): pl.pallas_call(body, out_shape=outs, in_specs=[SMEM] * scalars + [VMEM] *...  137 us
    all_to_all x3, blocking collectives, exchanged(): return lax.all_to_all(value, axis, split_axis=0, concat_axis=0, tiled=True)  50 us
    all_to_all x3, waiting for transfers between devices, exchanged(): return lax.all_to_all(value, axis, split_axis=0, concat_axis=0, tiled=True)  36.3 us
    all_to_all x3, starting transfers between devices, exchanged(): return lax.all_to_all(value, axis, split_axis=0, concat_axis=0, tiled=True)  24.2 us
    ppermute x2, starting transfers between devices, body(): ring = lax.ppermute(value, ('y', 'c'), AROUND)  7.36 us
  transfers between devices with their start and end apart: 9, of which 3 were waited for; matrix products, arithmetic and copies ran while one was open for 0% of the time, Pallas kernels for 23%

profile of v4, /device:TPU:1, one launch (start us, length us, event | category | flops | bytes accessed | tf_op | source)
XLA Modules:
  0.0 263.8 jit_solution(4953402479710426446)
XLA Ops:
  0.0 66.0 %shard_map.136 = (bf16[32,16,128]{2,1,0:T(8,128)(2,1)}, f32[8,128]{1,0:T(8,128)S(1)}, bf16[128,64]{1,0:T(8,128)(2,1)S(1)}, bf16[2,2048,256]{2,1,0:T(8,128)(2,1)}) custom-call(bf16[64,128]{1,0:T(8,128)(2,1)} %bitcast.23, s32[1,128]{1,0:T(1,128)} %bitcast.24, s32[2,128]{1,0:T(2,128)} %bitcast.26, f32[2,128]{1,0:T(2,128)} %bitcast.27, ...), custom_call_target="tpu_custom_call" | custom-call | tf_op jit(solution)/shard_map/pallas_call | solution.py:323
  66.0 4.0 %collective-permute-start.1 = (bf16[2,2048,256]{2,1,0:T(8,128)(2,1)}, bf16[2,2048,256]{2,1,0:T(8,128)(2,1)}, u32[]{:S(2)}, u32[]{:S(2)}) collective-permute-start(bf16[2,2048,256]{2,1,0:T(8,128)(2,1)} %get-tuple-element.17.refs_0_), channel_id=1, source_target_pairs={{0,14},{1,3},{2,0},{3,5},{4,2},{5,7},{6,4},{7,9},{8,6},{9,11},{10,... | collective-permute-start | bytes 6291464 | tf_op jit(solution)/shard_map/ppermute | solution.py:378
  70.1 56.7 %shard_map.140.refs_4_ = bf16[448,2048]{1,0:T(8,128)(2,1)} custom-call(bf16[256,2048]{1,0:T(8,128)(2,1)} %bitcast.18, bf16[64,2048]{1,0:T(8,128)(2,1)} %bitcast.21, bf16[64,2048]{1,0:T(8,128)(2,1)} %bitcast.22, bf16[64,2048]{1,0:T(8,128)(2,1)} %refs_3_.1), custom_call_target="tpu_custom_call" | custom-call | tf_op jit(solution)/shard_map/pallas_call | solution.py:323
  126.8 3.3 %collective-permute-start.4 = (bf16[448,2048]{1,0:T(8,128)(2,1)}, bf16[448,2048]{1,0:T(8,128)(2,1)}, u32[]{:S(2)}, u32[]{:S(2)}) collective-permute-start(bf16[448,2048]{1,0:T(8,128)(2,1)} %shard_map.140.refs_4_), channel_id=1, source_target_pairs={{0,14},{1,3},{2,0},{3,5},{4,2},{5,7},{6,4},{7,9},{8,6},{9,11},{10,... | collective-permute-start | bytes 5505032 | tf_op jit(solution)/shard_map/ppermute | solution.py:378
  130.2 12.9 %all-to-all-start = ((bf16[32,16,128]{2,1,0:T(8,128)(2,1)}), bf16[32,16,128]{2,1,0:T(8,128)(2,1)S(1)}, u32[]{:S(2)}, u32[]{:S(2)}) async-start(bf16[32,16,128]{2,1,0:T(8,128)(2,1)} %get-tuple-element.12), calls=%async_computation | async-start | bytes 262144 | tf_op jit(solution)/shard_map/all_to_all | solution.py:24
  143.1 9.3 %all-to-all-done.arrived_ref.message_ref = bf16[32,16,128]{2,1,0:T(8,128)(2,1)S(1)} async-done(((bf16[32,16,128]{2,1,0:T(8,128)(2,1)}), bf16[32,16,128]{2,1,0:T(8,128)(2,1)S(1)}, u32[]{:S(2)}, u32[]{:S(2)}) %all-to-all-start) | async-done | bytes 131104 | tf_op jit(solution)/shard_map/all_to_all | solution.py:24
  152.4 2.6 shard_map.137
  155.0 7.8 %all-to-all-start.1 = ((bf16[16,136,128]{2,1,0:T(8,128)(2,1)}), bf16[16,136,128]{2,1,0:T(8,128)(2,1)S(1)}, u32[]{:S(2)}, u32[]{:S(2)}) async-start(bf16[16,136,128]{2,1,0:T(8,128)(2,1)} %shard_map.137), calls=%async_computation.1 | async-start | bytes 1114112 | tf_op jit(solution)/shard_map/all_to_all | solution.py:24
  162.8 2.0 collective-permute-start
  164.8 2.3 collective-permute-start.2
  167.2 2.0 collective-permute-start.3
  169.2 2.3 collective-permute-start.5
  171.5 9.1 %all-to-all-done.1.arrived_ref = bf16[16,136,128]{2,1,0:T(8,128)(2,1)S(1)} async-done(((bf16[16,136,128]{2,1,0:T(8,128)(2,1)}), bf16[16,136,128]{2,1,0:T(8,128)(2,1)S(1)}, u32[]{:S(2)}, u32[]{:S(2)}) %all-to-all-start.1) | async-done | bytes 557088 | tf_op jit(solution)/shard_map/all_to_all | solution.py:24
  180.7 1.0 shard_map.138
  181.7 14.6 %all_to_all.30 = bf16[64,8,128]{2,1,0:T(8,128)(2,1)S(1)} all-to-all(bf16[64,8,128]{2,1,0:T(8,128)(2,1)S(1)} %get-tuple-element.15), channel_id=1, replica_groups=mesh['sp'=32,'y'=8,'c'=2] {'sp','c'}, dimensions={0} | all-to-all | bytes 262144 | tf_op jit(solution)/shard_map/all_to_all | solution.py:24
  196.3 0.9 shard_map.139
  197.2 3.5 %all-to-all-start.3 = ((bf16[8,16,2,8,128]{4,3,2,1,0:T(8,128)(2,1)}), bf16[8,16,2,8,128]{4,3,2,1,0:T(8,128)(2,1)S(1)}, u32[]{:S(2)}, u32[]{:S(2)}) async-start(bf16[8,16,2,8,128]{4,3,2,1,0:T(8,128)(2,1)} %shard_map.139), calls=%async_computation.3 | async-start | bytes 1048576 | tf_op jit(solution)/shard_map/all_to_all | solution.py:24
  200.7 0.1 pad_add_fusion.place_ref
  200.8 17.8 %all-to-all-done.3.x_ref = bf16[8,16,2,8,128]{4,3,2,1,0:T(8,128)(2,1)S(1)} async-done(((bf16[8,16,2,8,128]{4,3,2,1,0:T(8,128)(2,1)}), bf16[8,16,2,8,128]{4,3,2,1,0:T(8,128)(2,1)S(1)}, u32[]{:S(2)}, u32[]{:S(2)}) %all-to-all-start.3) | async-done | bytes 524320 | tf_op jit(solution)/shard_map/all_to_all | solution.py:24
  218.6 8.9 %shard_map.141 = bf16[8,16,2,8,128]{4,3,2,1,0:T(8,128)(2,1)S(1)} custom-call(s32[2]{0:T(128)S(1)} %pad_add_fusion.place_ref, bf16[8,16,2,8,128]{4,3,2,1,0:T(8,128)(2,1)S(1)} %all-to-all-done.3.x_ref, bf16[32,16,128]{2,1,0:T(8,128)(2,1)S(1)} %all-to-all-done.arrived_ref.message_ref, f32[16,128]{1,0:T(8,128)S(1)} %get-tuple-element.16.gain_ref, ...), custom_call_target="tpu_custom_call" | custom-call | tf_op jit(solution)/shard_map/pallas_call | solution.py:323
  227.5 20.2 %all_to_all.31.arrived_ref = bf16[8,16,2,8,128]{4,3,2,1,0:T(8,128)(2,1)S(1)} all-to-all(bf16[8,16,2,8,128]{4,3,2,1,0:T(8,128)(2,1)S(1)} %shard_map.141), channel_id=1, replica_groups=mesh['sp'=32,'y'=8,'c'=2] {'y'}, dimensions={0} | all-to-all | bytes 1048576 | tf_op jit(solution)/shard_map/all_to_all | solution.py:24
  247.7 0.1 shard_map.142
  247.8 15.1 %all_to_all.32.arrived_ref = bf16[64,8,128]{2,1,0:T(8,128)(2,1)S(1)} all-to-all(bf16[64,8,128]{2,1,0:T(8,128)(2,1)S(1)} %bitcast.17), channel_id=1, replica_groups=mesh['sp'=32,'y'=8,'c'=2] {'sp','c'}, dimensions={0} | all-to-all | bytes 262144 | tf_op jit(solution)/shard_map/all_to_all | solution.py:24
  262.9 0.9 shard_map.143
  (8 shorter events, 0.0 us)
Async XLA Ops:
  66.0 98.8 %collective-permute-start.1 = (bf16[2,2048,256]{2,1,0:T(8,128)(2,1)}, bf16[2,2048,256]{2,1,0:T(8,128)(2,1)}, u32[]{:S(2)}, u32[]{:S(2)}) collective-permute-start(bf16[2,2048,256]{2,1,0:T(8,128)(2,1)} %get-tuple-element.17.refs_0_), channel_id=1, source_target_pairs={{0,14},{1,3},{2,0},{3,5},{4,2},{5,7},{6,4},{7,9},{8,6},{9,11},{10,... | collective-permute-start | bytes 6291464 | tf_op jit(solution)/shard_map/ppermute | solution.py:378
  126.8 40.3 %copy-start = (bf16[448,2048]{1,0:T(8,128)(2,1)S(1)}, bf16[448,2048]{1,0:T(8,128)(2,1)}, u32[]{:S(2)}) copy-start(bf16[448,2048]{1,0:T(8,128)(2,1)} %shard_map.140.refs_4_) | copy-start | bytes 5505028
  126.8 42.4 %collective-permute-start.4 = (bf16[448,2048]{1,0:T(8,128)(2,1)}, bf16[448,2048]{1,0:T(8,128)(2,1)}, u32[]{:S(2)}, u32[]{:S(2)}) collective-permute-start(bf16[448,2048]{1,0:T(8,128)(2,1)} %shard_map.140.refs_4_), channel_id=1, source_target_pairs={{0,14},{1,3},{2,0},{3,5},{4,2},{5,7},{6,4},{7,9},{8,6},{9,11},{10,... | collective-permute-start | bytes 5505032 | tf_op jit(solution)/shard_map/ppermute | solution.py:378
  130.2 22.3 %all-to-all-start = ((bf16[32,16,128]{2,1,0:T(8,128)(2,1)}), bf16[32,16,128]{2,1,0:T(8,128)(2,1)S(1)}, u32[]{:S(2)}, u32[]{:S(2)}) async-start(bf16[32,16,128]{2,1,0:T(8,128)(2,1)} %get-tuple-element.12), calls=%async_computation | async-start | bytes 262144 | tf_op jit(solution)/shard_map/all_to_all | solution.py:24
  155.0 25.6 %all-to-all-start.1 = ((bf16[16,136,128]{2,1,0:T(8,128)(2,1)}), bf16[16,136,128]{2,1,0:T(8,128)(2,1)S(1)}, u32[]{:S(2)}, u32[]{:S(2)}) async-start(bf16[16,136,128]{2,1,0:T(8,128)(2,1)} %shard_map.137), calls=%async_computation.1 | async-start | bytes 1114112 | tf_op jit(solution)/shard_map/all_to_all | solution.py:24
  162.8 38.0 %collective-permute-start = (bf16[2,2048,256]{2,1,0:T(8,128)(2,1)}, bf16[2,2048,256]{2,1,0:T(8,128)(2,1)}, u32[]{:S(2)}, u32[]{:S(2)}) collective-permute-start(bf16[2,2048,256]{2,1,0:T(8,128)(2,1)} %get-tuple-element.17.refs_0_), channel_id=1, source_target_pairs={{0,1},{1,0},{2,3},{3,2},{4,5},{5,4},{6,7},{7,6},{8,9},{9,8},{10,11... | collective-permute-start | bytes 6291464 | tf_op jit(solution)/shard_map/ppermute | solution.py:379
  164.8 53.8 %collective-permute-start.2 = (bf16[2,2048,256]{2,1,0:T(8,128)(2,1)}, bf16[2,2048,256]{2,1,0:T(8,128)(2,1)}, u32[]{:S(2)}, u32[]{:S(2)}) collective-permute-start(bf16[2,2048,256]{2,1,0:T(8,128)(2,1)} %collective-permute-done.1.refs_2_), channel_id=1, source_target_pairs={{0,1},{1,0},{2,3},{3,2},{4,5},{5,4},{6,7},{7,6},{8,9},{9,8},{10,11... | collective-permute-start | bytes 6291464 | tf_op jit(solution)/shard_map/ppermute | solution.py:380
  167.2 33.7 %collective-permute-start.3 = (bf16[448,2048]{1,0:T(8,128)(2,1)S(1)}, bf16[448,2048]{1,0:T(8,128)(2,1)}, u32[]{:S(2)}, u32[]{:S(2)}) collective-permute-start(bf16[448,2048]{1,0:T(8,128)(2,1)S(1)} %copy-done), channel_id=1, source_target_pairs={{0,1},{1,0},{2,3},{3,2},{4,5},{5,4},{6,7},{7,6},{8,9},{9,8},{10,11... | collective-permute-start | bytes 5505032 | tf_op jit(solution)/shard_map/ppermute | solution.py:379
  169.2 49.4 %collective-permute-start.5 = (bf16[448,2048]{1,0:T(8,128)(2,1)}, bf16[448,2048]{1,0:T(8,128)(2,1)}, u32[]{:S(2)}, u32[]{:S(2)}) collective-permute-start(bf16[448,2048]{1,0:T(8,128)(2,1)} %collective-permute-done.4.refs_6_), channel_id=1, source_target_pairs={{0,1},{1,0},{2,3},{3,2},{4,5},{5,4},{6,7},{7,6},{8,9},{9,8},{10,11... | collective-permute-start | bytes 5505032 | tf_op jit(solution)/shard_map/ppermute | solution.py:380
  197.2 21.4 %all-to-all-start.3 = ((bf16[8,16,2,8,128]{4,3,2,1,0:T(8,128)(2,1)}), bf16[8,16,2,8,128]{4,3,2,1,0:T(8,128)(2,1)S(1)}, u32[]{:S(2)}, u32[]{:S(2)}) async-start(bf16[8,16,2,8,128]{4,3,2,1,0:T(8,128)(2,1)} %shard_map.139), calls=%async_computation.3 | async-start | bytes 1048576 | tf_op jit(solution)/shard_map/all_to_all | solution.py:24

commit v5 on v4

--- a/solution.py
+++ b/solution.py
@@ -132,7 +132,15 @@
 
 
 def pooling(
-    index_ref, arrived_ref, pool_ref, docs_ref, gain_ref, project_ref, norm_ref, out_ref
+    index_ref,
+    arrived_ref,
+    pool_ref,
+    docs_ref,
+    gain_ref,
+    project_ref,
+    norm_ref,
+    kept_ref,
+    out_ref,
 ):
     rows, channels = pool_ref.shape
     own = index_ref[0]
@@ -196,17 +204,37 @@
     tail = jnp.concatenate([*parts, jnp.zeros((5, 128), F32)], axis=0).astype(BF16)
     for k in range(8):
         both = matmul(pooled, project_ref[:, 256 * k : 256 * (k + 1)])
-        for side in (0, 1):
-            out_ref[2 * k + side, 0:128] = both[:, 128 * side : 128 * (side + 1)].astype(BF16)
-            out_ref[2 * k + side, 128:136] = tail
+        left, right = both[:, :128], both[:, 128:]
+        kept_ref[k] = jnp.where(index_ref[1] == 0, left, right)
+        out_ref[k, 0:128] = jnp.where(index_ref[1] == 0, right, left).astype(BF16)
+        out_ref[k, 128:136] = tail
+
+
+def pairing(core_ref, kept_ref, arrived_ref, norm_ref, out_ref):
+    own = jnp.concatenate([*three_parts(norm_ref[...]), jnp.zeros((5, 128), F32)], axis=0)
+    other = arrived_ref[0, 128:136].astype(F32)
+    first = core_ref[0] == 0
+    tail = jnp.concatenate(
+        [
+            jnp.where(first, own, other)[0:3],
+            jnp.where(first, other, own)[0:3],
+            jnp.zeros((2, 128), F32),
+        ],
+        axis=0,
+    ).astype(BF16)
+    for k in range(8):
+        out_ref[k, 0:128] = (kept_ref[k] + arrived_ref[k, 0:128].astype(F32)).astype(BF16)
+        out_ref[k, 128:136] = tail
 
 
 def sending(arrived_ref, slots_ref, residual_ref, hidden_ref, out_ref, gain_ref):
     projected = jnp.zeros((128, 128), F32)
-    for k in range(16):
+    for k in range(8):
         projected = projected + arrived_ref[k, 0:128].astype(F32)
         tail = arrived_ref[k, 128:136].astype(F32)
-        gain_ref[k : k + 1] = tail[0:1] + tail[1:2] + tail[2:3]
+        for side in (0, 1):
+            part = tail[3 * side : 3 * side + 3]
+            gain_ref[2 * k + side : 2 * k + side + 1] = part[0:1] + part[1:2] + part[2:3]
     hidden = residual_ref[...].astype(F32) + projected.astype(BF16).astype(F32)
     hidden_ref[...] = hidden
     slot = iota((512, 128), 0).astype(F32)
@@ -227,7 +255,7 @@
         pltpu.make_async_copy(source, target, landed.at[k])
         for k, (source, target) in enumerate(zip(sources, near))
     ]
-    for copy in copies[:2]:
+    for copy in copies:
         copy.start()
     uppers, lowers = near[:4], near[4:]
 
@@ -253,10 +281,6 @@
     hidden = []
     for k in range(4):
         copies[k].wait()
-        copies[k + 2].start()
-        if k == 3:
-            copies[6].start()
-            copies[7].start()
         lower = matmul(normed, uppers[k][0])
         upper = matmul(normed, uppers[k][1])
         hidden.append((jax.nn.silu(lower) * upper * weight).astype(BF16))
@@ -359,7 +383,7 @@
             array((32, 16, 128), BF16),
             array((8, 128), F32),
             array((128, 64), BF16),
-            pltpu.HBM((2, 2048, 256), BF16),
+            array((2, 2048, 256), BF16),
         ),
         (pool_input.T, docs, routes.T, route_weights.T),
         far=(expert_gate[0], expert_up[0]),
@@ -367,7 +391,7 @@
     )
     lower = kernel(
         packing,
-        pltpu.HBM((448, 2048), BF16),
+        array((448, 2048), BF16),
         (),
         far=(expert_down[0], shared_gate.T, shared_up.T, shared_down),
         scratch=[pltpu.SemaphoreType.DMA((4,))],
@@ -380,15 +404,24 @@
         ring_other = lax.ppermute(ring, "c", SWAP)
         group += [own_other, ring, ring_other]
     arrived = exchanged(message, "sp")
-    index = lax.axis_index("sp").astype(jnp.int32).reshape(1)
-    terms = kernel(
+    core = lax.axis_index("c").astype(jnp.int32)
+    index = jnp.stack([lax.axis_index("sp").astype(jnp.int32), core])
+    kept, terms = kernel(
         pooling,
-        array((16, 136, 128), BF16),
+        (array((8, 128, 128), F32), array((8, 136, 128), BF16)),
         (index, docs, pool_gain.reshape(1, 64), out_proj, norm_gain.reshape(1, 128)),
         near=(arrived, values),
         scalars=1,
     )
-    terms = exchanged(terms, ("y", "c"))
+    terms = lax.ppermute(terms, "c", SWAP)
+    terms = kernel(
+        pairing,
+        array((8, 136, 128), BF16),
+        (core.reshape(1), norm_gain.reshape(1, 128)),
+        near=(kept, terms),
+        scalars=1,
+    )
+    terms = exchanged(terms, "y")
     hidden_state, outgoing, gains = kernel(
         sending,
         (array((128, 128), F32), array((64, 8, 128), BF16), array((16, 128), F32)),
@@ -400,7 +433,7 @@
         spreading, array((8, 16, 2, 8, 128), BF16), (), near=(rows.reshape(16, 2, 2, 8, 128),)
     )
     rows = exchanged(rows, "y")
-    place = jnp.stack([lax.axis_index("c"), lax.axis_index("y") & 1]).astype(jnp.int32)
+    place = jnp.stack([core, lax.axis_index("y").astype(jnp.int32) & 1])
     groups = uppers + lowers
     parts = kernel(
         experts,

time: 265 us -> 168 us (0.63)
  Pallas kernels: 137 us -> 18.5 us
  blocking collectives: 50 us -> 74 us
  waiting for transfers between devices: 36.3 us -> 27 us
  starting transfers between devices: 40.2 us -> 47.5 us
    pallas_call x8 -> x9, Pallas kernels: 137 us -> 18.5 us  [kernel(): pl.pallas_call(body, out_shape=outs, in_specs=[SMEM] * scalars + [VMEM] *...]
    all_to_all x3 -> x4, blocking collectives: 50 us -> 74 us  [exchanged(): return lax.all_to_all(value, axis, split_axis=0, concat_axis=0, tiled=True)]
    all_to_all x3 -> x2, waiting for transfers between devices: 36.3 us -> 17.8 us  [exchanged(): return lax.all_to_all(value, axis, split_axis=0, concat_axis=0, tiled=True)]
    ppermute x2, starting transfers between devices: 4.61 us -> 14.5 us  [body(): ring_other = lax.ppermute(ring, 'c', SWAP)]
    ppermute x2, waiting for transfers between devices: 0.01 us -> 9.21 us  [body(): ring = lax.ppermute(value, ('y', 'c'), AROUND)]
    all_to_all x3 -> x2, starting transfers between devices: 24.2 us -> 16.4 us  [exchanged(): return lax.all_to_all(value, axis, split_axis=0, concat_axis=0, tiled=True)]
    ppermute x2, starting transfers between devices: 4.03 us -> 7.5 us  [body(): own_other = lax.ppermute(value, 'c', SWAP)]
  transfers between devices with their start and end apart: 9 -> 9, of which waited for: 3 -> 3; matrix products, arithmetic and copies ran while one was open for 0% -> 0% of each run, Pallas kernels for 23% -> 3%
where the time goes in v5:
time: 168 us; the launch traced here: 167 us
  blocking collectives  74 us (44%)
  starting transfers between devices  47.5 us (28%)
  waiting for transfers between devices  27 us (16%)
  Pallas kernels  18.5 us (11%)
    all_to_all x4, blocking collectives, exchanged(): return lax.all_to_all(value, axis, split_axis=0, concat_axis=0, tiled=True)  74 us
    pallas_call x9, Pallas kernels, kernel(): pl.pallas_call(body, out_shape=outs, in_specs=[SMEM] * scalars + [VMEM] *...  18.5 us
    all_to_all x2, waiting for transfers between devices, exchanged(): return lax.all_to_all(value, axis, split_axis=0, concat_axis=0, tiled=True)  17.8 us
    all_to_all x2, starting transfers between devices, exchanged(): return lax.all_to_all(value, axis, split_axis=0, concat_axis=0, tiled=True)  16.4 us
    ppermute x2, starting transfers between devices, body(): ring_other = lax.ppermute(ring, 'c', SWAP)  14.5 us
    ppermute x2, waiting for transfers between devices, body(): ring = lax.ppermute(value, ('y', 'c'), AROUND)  9.21 us
    ppermute x2, starting transfers between devices, body(): own_other = lax.ppermute(value, 'c', SWAP)  7.5 us
    ppermute x2, starting transfers between devices, body(): ring = lax.ppermute(value, ('y', 'c'), AROUND)  7.23 us
  transfers between devices with their start and end apart: 9, of which 3 were waited for; matrix products, arithmetic and copies ran while one was open for 0% of the time, Pallas kernels for 3%

profile of v5, /device:TPU:1, one launch (start us, length us, event | category | flops | bytes accessed | tf_op | source)
XLA Modules:
  0.0 167.3 jit_solution(12854037404030891262)
XLA Ops:
  0.0 3.8 %shard_map.136 = (bf16[32,16,128]{2,1,0:T(8,128)(2,1)}, f32[8,128]{1,0:T(8,128)S(1)}, bf16[128,64]{1,0:T(8,128)(2,1)S(1)}, bf16[2,2048,256]{2,1,0:T(8,128)(2,1)}) custom-call(bf16[64,128]{1,0:T(8,128)(2,1)} %bitcast.23, s32[1,128]{1,0:T(1,128)} %bitcast.26, s32[2,128]{1,0:T(2,128)} %bitcast.28, f32[2,128]{1,0:T(2,128)} %bitcast.29, ...), custom_call_target="tpu_custom_call" | custom-call | tf_op jit(solution)/shard_map/pallas_call | solution.py:347
  3.8 4.0 %collective-permute-start.2 = (bf16[2,2048,256]{2,1,0:T(8,128)(2,1)}, bf16[2,2048,256]{2,1,0:T(8,128)(2,1)}, u32[]{:S(2)}, u32[]{:S(2)}) collective-permute-start(bf16[2,2048,256]{2,1,0:T(8,128)(2,1)} %get-tuple-element.21.refs_0_), channel_id=1, source_target_pairs={{0,14},{1,3},{2,0},{3,5},{4,2},{5,7},{6,4},{7,9},{8,6},{9,11},{10,... | collective-permute-start | bytes 6291464 | tf_op jit(solution)/shard_map/ppermute | solution.py:402
  7.9 1.5 shard_map.141.refs_4_
  9.3 3.2 %collective-permute-start.5 = (bf16[448,2048]{1,0:T(8,128)(2,1)S(1)}, bf16[448,2048]{1,0:T(8,128)(2,1)}, u32[]{:S(2)}, u32[]{:S(2)}) collective-permute-start(bf16[448,2048]{1,0:T(8,128)(2,1)S(1)} %shard_map.141.refs_4_), channel_id=1, source_target_pairs={{0,14},{1,3},{2,0},{3,5},{4,2},{5,7},{6,4},{7,9},{8,6},{9,11},{10,... | collective-permute-start | bytes 5505032 | tf_op jit(solution)/shard_map/ppermute | solution.py:402
  12.6 12.9 %all-to-all-start = ((bf16[32,16,128]{2,1,0:T(8,128)(2,1)}), bf16[32,16,128]{2,1,0:T(8,128)(2,1)S(1)}, u32[]{:S(2)}, u32[]{:S(2)}) async-start(bf16[32,16,128]{2,1,0:T(8,128)(2,1)} %get-tuple-element.14), calls=%async_computation | async-start | bytes 262144 | tf_op jit(solution)/shard_map/all_to_all | solution.py:24
  25.5 5.1 %collective-permute-start.1 = (bf16[2,2048,256]{2,1,0:T(8,128)(2,1)}, bf16[2,2048,256]{2,1,0:T(8,128)(2,1)}, u32[]{:S(2)}, u32[]{:S(2)}) collective-permute-start(bf16[2,2048,256]{2,1,0:T(8,128)(2,1)} %get-tuple-element.21.refs_0_), channel_id=1, source_target_pairs={{0,1},{1,0},{2,3},{3,2},{4,5},{5,4},{6,7},{7,6},{8,9},{9,8},{10,11... | collective-permute-start | bytes 6291464 | tf_op jit(solution)/shard_map/ppermute | solution.py:403
  30.6 3.1 %collective-permute-done.2.refs_2_ = bf16[2,2048,256]{2,1,0:T(8,128)(2,1)} collective-permute-done((bf16[2,2048,256]{2,1,0:T(8,128)(2,1)}, bf16[2,2048,256]{2,1,0:T(8,128)(2,1)}, u32[]{:S(2)}, u32[]{:S(2)}) %collective-permute-start.2) | collective-permute-done | bytes 2097184 | tf_op jit(solution)/shard_map/ppermute | solution.py:402
  33.7 7.1 %collective-permute-start.3 = (bf16[2,2048,256]{2,1,0:T(8,128)(2,1)}, bf16[2,2048,256]{2,1,0:T(8,128)(2,1)}, u32[]{:S(2)}, u32[]{:S(2)}) collective-permute-start(bf16[2,2048,256]{2,1,0:T(8,128)(2,1)} %collective-permute-done.2.refs_2_), channel_id=1, source_target_pairs={{0,1},{1,0},{2,3},{3,2},{4,5},{5,4},{6,7},{7,6},{8,9},{9,8},{10,11... | collective-permute-start | bytes 6291464 | tf_op jit(solution)/shard_map/ppermute | solution.py:404
  40.9 1.8 %shard_map.137 = (f32[8,128,128]{2,1,0:T(8,128)S(1)}, bf16[8,136,128]{2,1,0:T(8,128)(2,1)S(1)}) custom-call(s32[2]{0:T(128)S(1)} %pad_add_fusion.1.index_ref, bf16[32,16,128]{2,1,0:T(8,128)(2,1)S(1)} %all-to-all-done.arrived_ref.message_ref, bf16[128,64]{1,0:T(8,128)(2,1)S(1)} %get-tuple-element.15.pool_ref, s32[1,128]{1,0:T(1,128)} %bitcast.27, ...), custom_call_target="tpu_custom_call" | custom-call | tf_op jit(solution)/shard_map/pallas_call | solution.py:347
  42.7 1.9 %collective-permute-start = (bf16[8,136,128]{2,1,0:T(8,128)(2,1)S(1)}, bf16[8,136,128]{2,1,0:T(8,128)(2,1)S(1)}, u32[]{:S(2)}, u32[]{:S(2)}) collective-permute-start(bf16[8,136,128]{2,1,0:T(8,128)(2,1)S(1)} %get-tuple-element.17), channel_id=1, source_target_pairs={{0,1},{1,0},{2,3},{3,2},{4,5},{5,4},{6,7},{7,6},{8,9},{9,8},{10,11... | collective-permute-start | bytes 835592 | tf_op jit(solution)/shard_map/ppermute | solution.py:416
  44.6 2.4 %collective-permute-start.4 = (bf16[448,2048]{1,0:T(8,128)(2,1)S(1)}, bf16[448,2048]{1,0:T(8,128)(2,1)}, u32[]{:S(2)}, u32[]{:S(2)}) collective-permute-start(bf16[448,2048]{1,0:T(8,128)(2,1)S(1)} %shard_map.141.refs_4_), channel_id=1, source_target_pairs={{0,1},{1,0},{2,3},{3,2},{4,5},{5,4},{6,7},{7,6},{8,9},{9,8},{10,11... | collective-permute-start | bytes 5505032 | tf_op jit(solution)/shard_map/ppermute | solution.py:403
  47.0 6.1 %collective-permute-done.5.refs_6_ = bf16[448,2048]{1,0:T(8,128)(2,1)} collective-permute-done((bf16[448,2048]{1,0:T(8,128)(2,1)S(1)}, bf16[448,2048]{1,0:T(8,128)(2,1)}, u32[]{:S(2)}, u32[]{:S(2)}) %collective-permute-start.5) | collective-permute-done | bytes 1835040 | tf_op jit(solution)/shard_map/ppermute | solution.py:402
  53.1 7.3 %collective-permute-start.6 = (bf16[448,2048]{1,0:T(8,128)(2,1)}, bf16[448,2048]{1,0:T(8,128)(2,1)}, u32[]{:S(2)}, u32[]{:S(2)}) collective-permute-start(bf16[448,2048]{1,0:T(8,128)(2,1)} %collective-permute-done.5.refs_6_), channel_id=1, source_target_pairs={{0,1},{1,0},{2,3},{3,2},{4,5},{5,4},{6,7},{7,6},{8,9},{9,8},{10,11... | collective-permute-start | bytes 5505032 | tf_op jit(solution)/shard_map/ppermute | solution.py:404
  60.5 0.7 shard_map.138
  61.2 15.0 %all_to_all.30.arrived_ref = bf16[8,136,128]{2,1,0:T(8,128)(2,1)S(1)} all-to-all(bf16[8,136,128]{2,1,0:T(8,128)(2,1)S(1)} %shard_map.138), channel_id=1, replica_groups=mesh['sp'=32,'y'=8,'c'=2] {'y'}, dimensions={0} | all-to-all | bytes 557056 | tf_op jit(solution)/shard_map/all_to_all | solution.py:24
  76.2 1.0 shard_map.139
  77.2 23.7 %all_to_all.31 = bf16[64,8,128]{2,1,0:T(8,128)(2,1)S(1)} all-to-all(bf16[64,8,128]{2,1,0:T(8,128)(2,1)S(1)} %get-tuple-element.19), channel_id=1, replica_groups=mesh['sp'=32,'y'=8,'c'=2] {'sp','c'}, dimensions={0} | all-to-all | bytes 262144 | tf_op jit(solution)/shard_map/all_to_all | solution.py:24
  100.9 0.9 shard_map.140
  101.8 3.5 %all-to-all-start.3 = ((bf16[8,16,2,8,128]{4,3,2,1,0:T(8,128)(2,1)}), bf16[8,16,2,8,128]{4,3,2,1,0:T(8,128)(2,1)S(1)}, u32[]{:S(2)}, u32[]{:S(2)}) async-start(bf16[8,16,2,8,128]{4,3,2,1,0:T(8,128)(2,1)} %shard_map.140), calls=%async_computation.3 | async-start | bytes 1048576 | tf_op jit(solution)/shard_map/all_to_all | solution.py:24
  105.4 17.8 %all-to-all-done.3.x_ref = bf16[8,16,2,8,128]{4,3,2,1,0:T(8,128)(2,1)S(1)} async-done(((bf16[8,16,2,8,128]{4,3,2,1,0:T(8,128)(2,1)}), bf16[8,16,2,8,128]{4,3,2,1,0:T(8,128)(2,1)S(1)}, u32[]{:S(2)}, u32[]{:S(2)}) %all-to-all-start.3) | async-done | bytes 524320 | tf_op jit(solution)/shard_map/all_to_all | solution.py:24
  123.2 7.8 %shard_map.142 = bf16[8,16,2,8,128]{4,3,2,1,0:T(8,128)(2,1)S(1)} custom-call(s32[2]{0:T(128)S(1)} %pad_add_fusion.place_ref, bf16[8,16,2,8,128]{4,3,2,1,0:T(8,128)(2,1)S(1)} %all-to-all-done.3.x_ref, bf16[32,16,128]{2,1,0:T(8,128)(2,1)S(1)} %all-to-all-done.arrived_ref.message_ref, f32[16,128]{1,0:T(8,128)S(1)} %get-tuple-element.20.gain_ref, ...), custom_call_target="tpu_custom_call" | custom-call | tf_op jit(solution)/shard_map/pallas_call | solution.py:347
  131.0 20.3 %all_to_all.32.arrived_ref = bf16[8,16,2,8,128]{4,3,2,1,0:T(8,128)(2,1)S(1)} all-to-all(bf16[8,16,2,8,128]{4,3,2,1,0:T(8,128)(2,1)S(1)} %shard_map.142), channel_id=1, replica_groups=mesh['sp'=32,'y'=8,'c'=2] {'y'}, dimensions={0} | all-to-all | bytes 1048576 | tf_op jit(solution)/shard_map/all_to_all | solution.py:24
  151.3 15.1 %all_to_all.33.arrived_ref = bf16[64,8,128]{2,1,0:T(8,128)(2,1)S(1)} all-to-all(bf16[64,8,128]{2,1,0:T(8,128)(2,1)S(1)} %bitcast.17), channel_id=1, replica_groups=mesh['sp'=32,'y'=8,'c'=2] {'sp','c'}, dimensions={0} | all-to-all | bytes 262144 | tf_op jit(solution)/shard_map/all_to_all | solution.py:24
  166.4 0.9 shard_map.144
  (11 shorter events, 0.2 us)
Async XLA Ops:
  3.8 29.8 %collective-permute-start.2 = (bf16[2,2048,256]{2,1,0:T(8,128)(2,1)}, bf16[2,2048,256]{2,1,0:T(8,128)(2,1)}, u32[]{:S(2)}, u32[]{:S(2)}) collective-permute-start(bf16[2,2048,256]{2,1,0:T(8,128)(2,1)} %get-tuple-element.21.refs_0_), channel_id=1, source_target_pairs={{0,14},{1,3},{2,0},{3,5},{4,2},{5,7},{6,4},{7,9},{8,6},{9,11},{10,... | collective-permute-start | bytes 6291464 | tf_op jit(solution)/shard_map/ppermute | solution.py:402
  9.3 92.5 %copy-start = (bf16[448,2048]{1,0:T(8,128)(2,1)}, bf16[448,2048]{1,0:T(8,128)(2,1)S(1)}, u32[]{:S(2)}) copy-start(bf16[448,2048]{1,0:T(8,128)(2,1)S(1)} %shard_map.141.refs_4_) | copy-start | bytes 5505028
  9.3 43.8 %collective-permute-start.5 = (bf16[448,2048]{1,0:T(8,128)(2,1)S(1)}, bf16[448,2048]{1,0:T(8,128)(2,1)}, u32[]{:S(2)}, u32[]{:S(2)}) collective-permute-start(bf16[448,2048]{1,0:T(8,128)(2,1)S(1)} %shard_map.141.refs_4_), channel_id=1, source_target_pairs={{0,14},{1,3},{2,0},{3,5},{4,2},{5,7},{6,4},{7,9},{8,6},{9,11},{10,... | collective-permute-start | bytes 5505032 | tf_op jit(solution)/shard_map/ppermute | solution.py:402
  12.6 28.3 %all-to-all-start = ((bf16[32,16,128]{2,1,0:T(8,128)(2,1)}), bf16[32,16,128]{2,1,0:T(8,128)(2,1)S(1)}, u32[]{:S(2)}, u32[]{:S(2)}) async-start(bf16[32,16,128]{2,1,0:T(8,128)(2,1)} %get-tuple-element.14), calls=%async_computation | async-start | bytes 262144 | tf_op jit(solution)/shard_map/all_to_all | solution.py:24
  25.5 79.9 %collective-permute-start.1 = (bf16[2,2048,256]{2,1,0:T(8,128)(2,1)}, bf16[2,2048,256]{2,1,0:T(8,128)(2,1)}, u32[]{:S(2)}, u32[]{:S(2)}) collective-permute-start(bf16[2,2048,256]{2,1,0:T(8,128)(2,1)} %get-tuple-element.21.refs_0_), channel_id=1, source_target_pairs={{0,1},{1,0},{2,3},{3,2},{4,5},{5,4},{6,7},{7,6},{8,9},{9,8},{10,11... | collective-permute-start | bytes 6291464 | tf_op jit(solution)/shard_map/ppermute | solution.py:403
  33.7 89.5 %collective-permute-start.3 = (bf16[2,2048,256]{2,1,0:T(8,128)(2,1)}, bf16[2,2048,256]{2,1,0:T(8,128)(2,1)}, u32[]{:S(2)}, u32[]{:S(2)}) collective-permute-start(bf16[2,2048,256]{2,1,0:T(8,128)(2,1)} %collective-permute-done.2.refs_2_), channel_id=1, source_target_pairs={{0,1},{1,0},{2,3},{3,2},{4,5},{5,4},{6,7},{7,6},{8,9},{9,8},{10,11... | collective-permute-start | bytes 6291464 | tf_op jit(solution)/shard_map/ppermute | solution.py:404
  42.7 17.8 %collective-permute-start = (bf16[8,136,128]{2,1,0:T(8,128)(2,1)S(1)}, bf16[8,136,128]{2,1,0:T(8,128)(2,1)S(1)}, u32[]{:S(2)}, u32[]{:S(2)}) collective-permute-start(bf16[8,136,128]{2,1,0:T(8,128)(2,1)S(1)} %get-tuple-element.17), channel_id=1, source_target_pairs={{0,1},{1,0},{2,3},{3,2},{4,5},{5,4},{6,7},{7,6},{8,9},{9,8},{10,11... | collective-permute-start | bytes 835592 | tf_op jit(solution)/shard_map/ppermute | solution.py:416
  44.6 60.7 %collective-permute-start.4 = (bf16[448,2048]{1,0:T(8,128)(2,1)S(1)}, bf16[448,2048]{1,0:T(8,128)(2,1)}, u32[]{:S(2)}, u32[]{:S(2)}) collective-permute-start(bf16[448,2048]{1,0:T(8,128)(2,1)S(1)} %shard_map.141.refs_4_), channel_id=1, source_target_pairs={{0,1},{1,0},{2,3},{3,2},{4,5},{5,4},{6,7},{7,6},{8,9},{9,8},{10,11... | collective-permute-start | bytes 5505032 | tf_op jit(solution)/shard_map/ppermute | solution.py:403
  53.1 70.0 %collective-permute-start.6 = (bf16[448,2048]{1,0:T(8,128)(2,1)}, bf16[448,2048]{1,0:T(8,128)(2,1)}, u32[]{:S(2)}, u32[]{:S(2)}) collective-permute-start(bf16[448,2048]{1,0:T(8,128)(2,1)} %collective-permute-done.5.refs_6_), channel_id=1, source_target_pairs={{0,1},{1,0},{2,3},{3,2},{4,5},{5,4},{6,7},{7,6},{8,9},{9,8},{10,11... | collective-permute-start | bytes 5505032 | tf_op jit(solution)/shard_map/ppermute | solution.py:404
  101.8 21.4 %all-to-all-start.3 = ((bf16[8,16,2,8,128]{4,3,2,1,0:T(8,128)(2,1)}), bf16[8,16,2,8,128]{4,3,2,1,0:T(8,128)(2,1)S(1)}, u32[]{:S(2)}, u32[]{:S(2)}) async-start(bf16[8,16,2,8,128]{4,3,2,1,0:T(8,128)(2,1)} %shard_map.140), calls=%async_computation.3 | async-start | bytes 1048576 | tf_op jit(solution)/shard_map/all_to_all | solution.py:24

commit v6 on v4

--- a/solution.py
+++ b/solution.py
@@ -40,30 +40,36 @@
 
 
 def opening(
+    core_ref,
     pool_ref,
     docs_ref,
     routes_ref,
     weights_ref,
-    gate_ref,
-    up_ref,
+    gain_ref,
+    norm_ref,
     message_ref,
     slots_ref,
-    values_ref,
-    pack_ref,
-    packed,
+    side_ref,
 ):
-    copies = [
-        pltpu.make_async_copy(source, pack_ref.at[k], packed.at[k])
-        for k, source in enumerate((gate_ref, up_ref))
-    ]
-    for copy in copies:
-        copy.start()
     channels, rows = pool_ref.shape
     square = (rows, rows)
     values = pool_ref[...].astype(F32).T.astype(BF16)
-    values_ref[...] = values
     across = iota((channels, 128), 0)
     lane = iota((channels, 128), 1)
+    first_core = core_ref[0] == 0
+    moved = (lane == across + jnp.where(first_core, 0, channels)).astype(F32).astype(BF16)
+    side_ref[0:128] = matmul(values, moved).astype(BF16)
+    gains = jnp.concatenate([*three_parts(gain_ref[...]), jnp.zeros((5, channels), F32)], axis=0)
+    gains = matmul(gains.astype(BF16), moved)[0:3]
+    norms = jnp.concatenate(three_parts(norm_ref[...]), axis=0)
+    zeros = jnp.zeros((3, 128), F32)
+    tail = [
+        gains,
+        jnp.where(first_core, norms, zeros),
+        jnp.where(first_core, zeros, norms),
+        jnp.zeros((7, 128), F32),
+    ]
+    side_ref[128:144] = jnp.concatenate(tail, axis=0).astype(BF16)
     spread = (lane == across) | ((across % 4 == 3) & (lane == SUM_LANE + across // 4))
     wide = matmul(values, spread.astype(F32).astype(BF16))
     docs = docs_ref[...].astype(F32)
@@ -112,9 +118,9 @@
     message = jnp.broadcast_to(shared[None], (32, 16, 128)).reshape(512, 128)
     for k, value in enumerate((*three_parts(weight), chosen_first)):
         message = jnp.where(place == W_LANE + k, value, message)
-    message_ref[...] = message.reshape(32, 16, 128).astype(BF16)
-    for copy in copies:
-        copy.wait()
+    message = message.reshape(32, 16, 128).astype(BF16)
+    message_ref[:, 0] = message
+    message_ref[:, 1] = message
 
 
 def packing(*refs):
@@ -132,14 +138,27 @@
 
 
 def pooling(
-    index_ref, arrived_ref, pool_ref, docs_ref, gain_ref, project_ref, norm_ref, out_ref
+    index_ref,
+    arrived_ref,
+    side_ref,
+    other_ref,
+    project_other_ref,
+    docs_ref,
+    source_ref,
+    out_ref,
+    project_ref,
+    landed,
 ):
-    rows, channels = pool_ref.shape
+    copy = pltpu.make_async_copy(source_ref, project_ref, landed.at[0])
+    copy.start()
+    rows = channels = 128
     own = index_ref[0]
     docs = docs_ref[...].astype(F32)
     first_doc = docs[:, 0:1]
-    arrived = arrived_ref[...].astype(F32)
-    meta = arrived[:, 0:1]
+    sides = side_ref[...].astype(F32) + other_ref[...].astype(F32)
+    values = sides[0:128].astype(BF16)
+    gain = sides[128:129] + (sides[129:130] + sides[130:131])
+    meta = arrived_ref[:, 0, 0:8].astype(F32)[:, 0:1]
     their_count = meta[:, :, META_LANE : META_LANE + 1]
     their_doc = (
         meta[:, :, META_LANE + 1 : META_LANE + 2] * 128.0
@@ -147,22 +166,27 @@
     )
     block = iota((32, 1, 1), 0)
     joins = (block < own) & (their_doc == first_doc.reshape(1, 1, 1))
+    behind = block == own - 1
     carry_length = jnp.sum(jnp.where(joins, their_count, 0.0), axis=0)
-    sums = jnp.sum(jnp.where(joins, arrived[:, 0:8], 0.0), axis=0)
-    sums = jnp.where(iota((8, 128), 0) < 3, sums, 0.0)
-    back = (iota((128, channels), 0) == SUM_LANE + iota((128, channels), 1) // 4) & (
-        iota((128, channels), 1) % 4 == 3
-    )
-    total = jnp.sum(sums, axis=0, keepdims=True)
-    carry = sum(
-        matmul(jnp.broadcast_to(part, (8, 128)).astype(BF16), back.astype(F32).astype(BF16))
-        for part in three_parts(total)
-    )[0:1]
-
-    behind = block == own - 1
-    rim = jnp.sum(jnp.where(behind, arrived, 0.0), axis=0)[:, :channels]
-    rim_joins = jnp.where(behind & joins, their_count, 0.0)
-    rim_rows = jnp.sum(rim_joins, axis=0)
+    source = iota((128, 128), 0)
+    target = iota((128, 128), 1)
+    carry = jnp.zeros((8, 128), F32)
+    rim = jnp.zeros((16, 128), F32)
+    for side in (0, 1):
+        arrived = arrived_ref[:, side].astype(F32)
+        sums = jnp.sum(jnp.where(joins, arrived[:, 0:8], 0.0), axis=0)
+        total = jnp.sum(jnp.where(iota((8, 128), 0) < 3, sums, 0.0), axis=0, keepdims=True)
+        here = target - 64 * side
+        inside = (here >= 0) & (here < 64)
+        back = inside & (here % 4 == 3) & (source == SUM_LANE + here // 4)
+        back = back.astype(F32).astype(BF16)
+        for part in three_parts(total):
+            carry = carry + matmul(jnp.broadcast_to(part, (8, 128)).astype(BF16), back)
+        their_rim = jnp.sum(jnp.where(behind, arrived, 0.0), axis=0).astype(BF16)
+        rim = rim + matmul(their_rim, (inside & (source == here)).astype(F32).astype(BF16))
+    carry = carry[0:1]
+    rim = rim.astype(BF16)
+    rim_rows = jnp.sum(jnp.where(behind & joins, their_count, 0.0), axis=0)
 
     square = (rows, rows)
     line = jnp.broadcast_to(docs, square)
@@ -174,14 +198,9 @@
     length = jnp.sum(together.astype(F32), axis=1, keepdims=True) + jnp.where(
         opens, carry_length, 0.0
     )
-    values = pool_ref[...]
-    rim = rim.astype(BF16)
     position = iota((rows, 16), 0)
     back_by = 16 - iota((rows, 16), 1)
-    rim_open = (
-        jnp.broadcast_to(opens, (rows, 16))
-        & (back_by.astype(F32) <= rim_rows)
-    )
+    rim_open = jnp.broadcast_to(opens, (rows, 16)) & (back_by.astype(F32) <= rim_rows)
     scale = iota((rows, channels), 1) % 4
     total = matmul(together.astype(F32).astype(BF16), values) + jnp.where(opens, carry, 0.0)
     amount = jnp.broadcast_to(length, (rows, channels))
@@ -191,22 +210,29 @@
         part = matmul(mask, values) + matmul(rim_mask, rim)
         total = jnp.where(scale == k, part, total)
         amount = jnp.where(scale == k, jnp.minimum(length, float(window)), amount)
-    pooled = ((total / amount - values.astype(F32)) * gain_ref[...]).astype(BF16)
-    parts = three_parts(norm_ref[...])
-    tail = jnp.concatenate([*parts, jnp.zeros((5, 128), F32)], axis=0).astype(BF16)
+    pooled = ((total / amount - sides[0:128]) * gain).astype(BF16)
+    first_core = index_ref[1] == 0
+    pooled_own = jnp.where(first_core, pooled[:, :64].astype(F32), pooled[:, 64:].astype(F32))
+    pooled_other = jnp.where(first_core, pooled[:, 64:].astype(F32), pooled[:, :64].astype(F32))
+    pooled_own, pooled_other = pooled_own.astype(BF16), pooled_other.astype(BF16)
+    tail = jnp.concatenate([sides[131:137], jnp.zeros((2, 128), F32)], axis=0).astype(BF16)
+    copy.wait()
     for k in range(8):
-        both = matmul(pooled, project_ref[:, 256 * k : 256 * (k + 1)])
-        for side in (0, 1):
-            out_ref[2 * k + side, 0:128] = both[:, 128 * side : 128 * (side + 1)].astype(BF16)
-            out_ref[2 * k + side, 128:136] = tail
+        cut = pl.ds(pl.multiple_of(256 * k + 128 * index_ref[1], 128), 128)
+        both = matmul(pooled_own, project_ref[:, cut])
+        both = both + matmul(pooled_other, project_other_ref[:, cut])
+        out_ref[k, 0:128] = both.astype(BF16)
+        out_ref[k, 128:136] = tail
 
 
 def sending(arrived_ref, slots_ref, residual_ref, hidden_ref, out_ref, gain_ref):
     projected = jnp.zeros((128, 128), F32)
-    for k in range(16):
+    for k in range(8):
         projected = projected + arrived_ref[k, 0:128].astype(F32)
         tail = arrived_ref[k, 128:136].astype(F32)
-        gain_ref[k : k + 1] = tail[0:1] + tail[1:2] + tail[2:3]
+        for side in (0, 1):
+            part = tail[3 * side : 3 * side + 3]
+            gain_ref[2 * k + side : 2 * k + side + 1] = part[0:1] + part[1:2] + part[2:3]
     hidden = residual_ref[...].astype(F32) + projected.astype(BF16).astype(F32)
     hidden_ref[...] = hidden
     slot = iota((512, 128), 0).astype(F32)
@@ -221,15 +247,15 @@
 
 
 def experts(place_ref, x_ref, message_ref, gain_ref, *refs):
-    sources, out_ref, normed_ref = refs[:8], refs[8], refs[9]
-    near, landed = refs[10:18], refs[18]
+    sources, out_ref, normed_ref = refs[:12], refs[12], refs[13]
+    near, landed = refs[14:26], refs[26]
+    gates, ups, lowers = near[0:4], near[4:8], near[8:12]
+    order = (0, 4, 1, 5, 2, 6, 3, 7, 8, 9, 10, 11)
     copies = [
-        pltpu.make_async_copy(source, target, landed.at[k])
-        for k, (source, target) in enumerate(zip(sources, near))
+        pltpu.make_async_copy(sources[k], near[k], landed.at[k]) for k in order
     ]
-    for copy in copies[:2]:
+    for copy in copies[:6]:
         copy.start()
-    uppers, lowers = near[:4], near[4:]
 
     squares = jnp.zeros((128, 128), F32)
     for k in range(16):
@@ -241,7 +267,7 @@
         normed_ref[:, 128 * k : 128 * (k + 1)] = (part * scaling * gain_ref[k : k + 1]).astype(
             BF16
         )
-    message = message_ref[...].astype(F32).reshape(16, 2, 16, 128)
+    message = message_ref[:, 0].astype(F32).reshape(16, 2, 16, 128)
     message = jnp.where(place_ref[1] == 0, message[:, 0], message[:, 1])
     side = jnp.where(place_ref[0] == 0, message[:, 0:8], message[:, 8:16])
     side = side.reshape(128, 128)
@@ -251,16 +277,16 @@
     first = side[:, W_LANE + 3 : W_LANE + 4]
     normed = normed_ref[...]
     hidden = []
-    for k in range(4):
-        copies[k].wait()
-        copies[k + 2].start()
-        if k == 3:
-            copies[6].start()
-            copies[7].start()
-        lower = matmul(normed, uppers[k][0])
-        upper = matmul(normed, uppers[k][1])
+    for k, (gate, up) in enumerate(zip(gates, ups)):
+        copies[2 * k].wait()
+        copies[2 * k + 1].wait()
+        if k < 3:
+            copies[6 + 2 * k].start()
+            copies[7 + 2 * k].start()
+        lower = matmul(normed, gate[...])
+        upper = matmul(normed, up[...])
         hidden.append((jax.nn.silu(lower) * upper * weight).astype(BF16))
-    for copy in copies[4:]:
+    for copy in copies[8:]:
         copy.wait()
     across = jnp.concatenate(
         [pack[256:320] for pack in lowers] + [pack[320:384] for pack in lowers], axis=0
@@ -353,55 +379,61 @@
     shared_down,
 ):
     docs = doc_ids.reshape(1, 128)
-    message, slots, values, upper = kernel(
+    core = lax.axis_index("c").astype(jnp.int32)
+    index = jnp.stack([lax.axis_index("sp").astype(jnp.int32), core])
+    message, slots, side = kernel(
         opening,
+        (array((32, 2, 16, 128), BF16), array((8, 128), F32), array((144, 128), BF16)),
         (
-            array((32, 16, 128), BF16),
-            array((8, 128), F32),
-            array((128, 64), BF16),
-            pltpu.HBM((2, 2048, 256), BF16),
+            core.reshape(1),
+            pool_input.T,
+            docs,
+            routes.T,
+            route_weights.T,
+            pool_gain.reshape(1, 64),
+            norm_gain.reshape(1, 128),
         ),
-        (pool_input.T, docs, routes.T, route_weights.T),
-        far=(expert_gate[0], expert_up[0]),
-        scratch=[pltpu.SemaphoreType.DMA((2,))],
-    )
-    lower = kernel(
+        scalars=1,
+    )
+    packed = kernel(
         packing,
-        pltpu.HBM((448, 2048), BF16),
+        array((448, 2048), BF16),
         (),
         far=(expert_down[0], shared_gate.T, shared_up.T, shared_down),
         scratch=[pltpu.SemaphoreType.DMA((4,))],
     )
-    uppers, lowers = [upper], [lower]
-    for group in (uppers, lowers):
-        value = group[0]
+    groups = []
+    for value in (expert_gate[0], expert_up[0], packed):
         ring = lax.ppermute(value, ("y", "c"), AROUND)
         own_other = lax.ppermute(value, "c", SWAP)
         ring_other = lax.ppermute(ring, "c", SWAP)
-        group += [own_other, ring, ring_other]
-    arrived = exchanged(message, "sp")
-    index = lax.axis_index("sp").astype(jnp.int32).reshape(1)
+        groups += [value, own_other, ring, ring_other]
+    arrived = exchanged(message.reshape(64, 16, 128), ("sp", "c"))
+    arrived = arrived.reshape(32, 2, 16, 128)
+    other_side = lax.ppermute(side, "c", SWAP)
+    other_project = lax.ppermute(out_proj, "c", SWAP)
     terms = kernel(
         pooling,
-        array((16, 136, 128), BF16),
-        (index, docs, pool_gain.reshape(1, 64), out_proj, norm_gain.reshape(1, 128)),
-        near=(arrived, values),
+        array((8, 136, 128), BF16),
+        (index, docs),
+        near=(arrived, side, other_side, other_project),
+        far=(out_proj,),
         scalars=1,
-    )
-    terms = exchanged(terms, ("y", "c"))
+        scratch=[pltpu.VMEM((64, 2048), BF16), pltpu.SemaphoreType.DMA((1,))],
+    )
+    terms = exchanged(terms, "y")
     hidden_state, outgoing, gains = kernel(
         sending,
         (array((128, 128), F32), array((64, 8, 128), BF16), array((16, 128), F32)),
-        (residual,),
-        near=(terms, slots),
+        (),
+        near=(terms, slots, residual),
     )
     rows = exchanged(outgoing, ("sp", "c"))
     rows = kernel(
         spreading, array((8, 16, 2, 8, 128), BF16), (), near=(rows.reshape(16, 2, 2, 8, 128),)
     )
     rows = exchanged(rows, "y")
-    place = jnp.stack([lax.axis_index("c"), lax.axis_index("y") & 1]).astype(jnp.int32)
-    groups = uppers + lowers
+    place = jnp.stack([core, lax.axis_index("y").astype(jnp.int32) & 1])
     parts = kernel(
         experts,
         array((8, 16, 2, 8, 128), BF16),
@@ -411,7 +443,7 @@
         scalars=1,
         scratch=[pltpu.VMEM((128, 2048), BF16)]
         + [pltpu.VMEM(value.shape, BF16) for value in groups]
-        + [pltpu.SemaphoreType.DMA((8,))],
+        + [pltpu.SemaphoreType.DMA((12,))],
         room=24,
     )
     parts = exchanged(parts, "y")

time: 265 us -> 156 us (0.59)
  Pallas kernels: 137 us -> 16.7 us
  starting transfers between devices: 40.2 us -> 61.7 us
  waiting for transfers between devices: 36.3 us -> 22.3 us
  blocking collectives: 50 us -> 53.7 us
    pallas_call x8, Pallas kernels: 137 us -> 16.7 us  [kernel(): pl.pallas_call(body, out_shape=outs, in_specs=[SMEM] * scalars + [VMEM] *...]
    all_to_all x3, waiting for transfers between devices: 36.3 us -> 22.3 us  [exchanged(): return lax.all_to_all(value, axis, split_axis=0, concat_axis=0, tiled=True)]
    all_to_all x3, starting transfers between devices: 24.2 us -> 33.6 us  [exchanged(): return lax.all_to_all(value, axis, split_axis=0, concat_axis=0, tiled=True)]
    ppermute x2 -> x3, starting transfers between devices: 4.03 us -> 9.24 us  [body(): own_other = lax.ppermute(value, 'c', SWAP)]
    ppermute x0 -> x2, starting transfers between devices: none -> 4.29 us  [the longest x1 2.36 us: body(): other_side = lax.ppermute(side, 'c', SWAP)]
    all_to_all x3, blocking collectives: 50 us -> 53.7 us  [exchanged(): return lax.all_to_all(value, axis, split_axis=0, concat_axis=0, tiled=True)]
    ppermute x2 -> x3, starting transfers between devices: 4.61 us -> 6.25 us  [body(): ring_other = lax.ppermute(ring, 'c', SWAP)]
    ppermute x2 -> x3, starting transfers between devices: 7.36 us -> 8.39 us  [body(): ring = lax.ppermute(value, ('y', 'c'), AROUND)]
  transfers between devices with their start and end apart: 9 -> 14, of which waited for: 3 -> 2; matrix products, arithmetic and copies ran while one was open for 0% -> 0% of each run, Pallas kernels for 23% -> 4%
where the time goes in v6:
time: 156 us; the launch traced here: 155 us
  starting transfers between devices  61.7 us (40%)
  blocking collectives  53.7 us (34%)
  waiting for transfers between devices  22.3 us (14%)
  Pallas kernels  16.7 us (11%)
    all_to_all x3, blocking collectives, exchanged(): return lax.all_to_all(value, axis, split_axis=0, concat_axis=0, tiled=True)  53.7 us
    all_to_all x3, starting transfers between devices, exchanged(): return lax.all_to_all(value, axis, split_axis=0, concat_axis=0, tiled=True)  33.6 us
    all_to_all x3, waiting for transfers between devices, exchanged(): return lax.all_to_all(value, axis, split_axis=0, concat_axis=0, tiled=True)  22.3 us
    pallas_call x8, Pallas kernels, kernel(): pl.pallas_call(body, out_shape=outs, in_specs=[SMEM] * scalars + [VMEM] *...  16.7 us
    ppermute x3, starting transfers between devices, body(): own_other = lax.ppermute(value, 'c', SWAP)  9.24 us
    ppermute x3, starting transfers between devices, body(): ring = lax.ppermute(value, ('y', 'c'), AROUND)  8.39 us
    ppermute x3, starting transfers between devices, body(): ring_other = lax.ppermute(ring, 'c', SWAP)  6.25 us
  transfers between devices with their start and end apart: 14, of which 2 were waited for; matrix products, arithmetic and copies ran while one was open for 0% of the time, Pallas kernels for 4%

profile of v6, /device:TPU:1, one launch (start us, length us, event | category | flops | bytes accessed | tf_op | source)
XLA Modules:
  0.0 154.8 jit_solution(6969882896467221280)
XLA Ops:
  0.0 1.5 shard_map.140.refs_8_
  1.6 4.2 %collective-permute-start.9 = (bf16[448,2048]{1,0:T(8,128)(2,1)S(1)}, bf16[448,2048]{1,0:T(8,128)(2,1)}, u32[]{:S(2)}, u32[]{:S(2)}) collective-permute-start(bf16[448,2048]{1,0:T(8,128)(2,1)S(1)} %shard_map.140.refs_8_), channel_id=1, source_target_pairs={{0,14},{1,3},{2,0},{3,5},{4,2},{5,7},{6,4},{7,9},{8,6},{9,11},{10,... | collective-permute-start | bytes 5505032 | tf_op jit(solution)/shard_map/ppermute | solution.py:407
  5.7 1.9 %shard_map.136 = (bf16[32,2,16,128]{3,2,1,0:T(8,128)(2,1)}, f32[8,128]{1,0:T(8,128)S(1)}, bf16[144,128]{1,0:T(8,128)(2,1)S(1)}) custom-call(s32[1]{0:T(128)} %bitcast.core_ref, bf16[64,128]{1,0:T(8,128)(2,1)} %bitcast.31, s32[1,128]{1,0:T(1,128)} %bitcast.32, s32[2,128]{1,0:T(2,128)} %bitcast.34, f32[2,128]{1,0:T(2,128)} %bitcast.35, f32[1,64]{1,0:T(1,128)} %bitcast.36, ...), custom_call_target="tpu_custom_call" | custom-call | tf_op jit(solution)/shard_map/pallas_call | solution.py:349
  7.7 16.2 %all-to-all-start = ((bf16[64,16,128]{2,1,0:T(8,128)(2,1)}), bf16[64,16,128]{2,1,0:T(8,128)(2,1)S(1)}, u32[]{:S(2)}, u32[]{:S(2)}) async-start(bf16[64,16,128]{2,1,0:T(8,128)(2,1)} %bitcast.9), calls=%async_computation | async-start | bytes 524288 | tf_op jit(solution)/shard_map/all_to_all | solution.py:24
  23.8 2.4 %collective-permute-start = (bf16[144,128]{1,0:T(8,128)(2,1)S(1)}, bf16[144,128]{1,0:T(8,128)(2,1)S(1)}, u32[]{:S(2)}, u32[]{:S(2)}) collective-permute-start(bf16[144,128]{1,0:T(8,128)(2,1)S(1)} %get-tuple-element.12.side_ref), channel_id=1, source_target_pairs={{0,1},{1,0},{2,3},{3,2},{4,5},{5,4},{6,7},{7,6},{8,9},{9,8},{10,11... | collective-permute-start | bytes 110600 | tf_op jit(solution)/shard_map/ppermute | solution.py:413
  26.2 1.9 %collective-permute-start.3 = (bf16[2048,256]{1,0:T(8,128)(2,1)S(1)}, bf16[2048,256]{1,0:T(8,128)(2,1)}, u32[]{:S(2)}, u32[]{:S(2)}) collective-permute-start(bf16[2048,256]{1,0:T(8,128)(2,1)S(1)} %bitcast.24), channel_id=1, source_target_pairs={{0,14},{1,3},{2,0},{3,5},{4,2},{5,7},{6,4},{7,9},{8,6},{9,11},{10,... | collective-permute-start | bytes 3145736 | tf_op jit(solution)/shard_map/ppermute | solution.py:407
  28.1 3.3 %collective-permute-start.2 = (bf16[2048,256]{1,0:T(8,128)(2,1)S(1)}, bf16[2048,256]{1,0:T(8,128)(2,1)}, u32[]{:S(2)}, u32[]{:S(2)}) collective-permute-start(bf16[2048,256]{1,0:T(8,128)(2,1)S(1)} %bitcast.25), channel_id=1, source_target_pairs={{0,1},{1,0},{2,3},{3,2},{4,5},{5,4},{6,7},{7,6},{8,9},{9,8},{10,11... | collective-permute-start | bytes 3145736 | tf_op jit(solution)/shard_map/ppermute | solution.py:408
  31.5 1.9 %collective-permute-start.1 = (bf16[64,2048]{1,0:T(8,128)(2,1)}, bf16[64,2048]{1,0:T(8,128)(2,1)S(1)}, u32[]{:S(2)}, u32[]{:S(2)}) collective-permute-start(bf16[64,2048]{1,0:T(8,128)(2,1)} %source_ref.1), channel_id=1, source_target_pairs={{0,1},{1,0},{2,3},{3,2},{4,5},{5,4},{6,7},{7,6},{8,9},{9,8},{10,11... | collective-permute-start | bytes 786440 | tf_op jit(solution)/shard_map/ppermute | solution.py:414
  33.4 2.3 %collective-permute-start.6 = (bf16[2048,256]{1,0:T(8,128)(2,1)}, bf16[2048,256]{1,0:T(8,128)(2,1)}, u32[]{:S(2)}, u32[]{:S(2)}) collective-permute-start(bf16[2048,256]{1,0:T(8,128)(2,1)} %bitcast.26), channel_id=1, source_target_pairs={{0,14},{1,3},{2,0},{3,5},{4,2},{5,7},{6,4},{7,9},{8,6},{9,11},{10,... | collective-permute-start | bytes 3145736 | tf_op jit(solution)/shard_map/ppermute | solution.py:407
  35.7 3.6 %collective-permute-start.8 = (bf16[448,2048]{1,0:T(8,128)(2,1)S(1)}, bf16[448,2048]{1,0:T(8,128)(2,1)}, u32[]{:S(2)}, u32[]{:S(2)}) collective-permute-start(bf16[448,2048]{1,0:T(8,128)(2,1)S(1)} %shard_map.140.refs_8_), channel_id=1, source_target_pairs={{0,1},{1,0},{2,3},{3,2},{4,5},{5,4},{6,7},{7,6},{8,9},{9,8},{10,11... | collective-permute-start | bytes 5505032 | tf_op jit(solution)/shard_map/ppermute | solution.py:408
  39.3 1.9 %collective-permute-start.10 = (bf16[448,2048]{1,0:T(8,128)(2,1)}, bf16[448,2048]{1,0:T(8,128)(2,1)}, u32[]{:S(2)}, u32[]{:S(2)}) collective-permute-start(bf16[448,2048]{1,0:T(8,128)(2,1)} %collective-permute-done.9.refs_10_), channel_id=1, source_target_pairs={{0,1},{1,0},{2,3},{3,2},{4,5},{5,4},{6,7},{7,6},{8,9},{9,8},{10,11... | collective-permute-start | bytes 5505032 | tf_op jit(solution)/shard_map/ppermute | solution.py:409
  41.3 2.4 %shard_map.137 = bf16[8,136,128]{2,1,0:T(8,128)(2,1)S(1)} custom-call(s32[2]{0:T(128)S(1)} %pad_add_fusion.1.index_ref, bf16[32,2,16,128]{3,2,1,0:T(8,128)(2,1)S(1)} %bitcast.18, bf16[144,128]{1,0:T(8,128)(2,1)S(1)} %get-tuple-element.12.side_ref, bf16[144,128]{1,0:T(8,128)(2,1)S(1)} %collective-permute-done.other_ref, ...), custom_call_target="tpu_custom_call" | custom-call | tf_op jit(solution)/shard_map/pallas_call | solution.py:349
  43.7 16.5 %all_to_all.30.arrived_ref = bf16[8,136,128]{2,1,0:T(8,128)(2,1)S(1)} all-to-all(bf16[8,136,128]{2,1,0:T(8,128)(2,1)S(1)} %shard_map.137), channel_id=1, replica_groups=mesh['sp'=32,'y'=8,'c'=2] {'y'}, dimensions={0} | all-to-all | bytes 557056 | tf_op jit(solution)/shard_map/all_to_all | solution.py:24
  61.0 11.4 %all-to-all-start.2 = ((bf16[64,8,128]{2,1,0:T(8,128)(2,1)}), bf16[64,8,128]{2,1,0:T(8,128)(2,1)S(1)}, u32[]{:S(2)}, u32[]{:S(2)}) async-start(bf16[64,8,128]{2,1,0:T(8,128)(2,1)} %get-tuple-element.14), calls=%async_computation.2 | async-start | bytes 262144 | tf_op jit(solution)/shard_map/all_to_all | solution.py:24
  72.5 2.4 %collective-permute-start.5 = (bf16[2048,256]{1,0:T(8,128)(2,1)}, bf16[2048,256]{1,0:T(8,128)(2,1)}, u32[]{:S(2)}, u32[]{:S(2)}) collective-permute-start(bf16[2048,256]{1,0:T(8,128)(2,1)} %bitcast.27), channel_id=1, source_target_pairs={{0,1},{1,0},{2,3},{3,2},{4,5},{5,4},{6,7},{7,6},{8,9},{9,8},{10,11... | collective-permute-start | bytes 3145736 | tf_op jit(solution)/shard_map/ppermute | solution.py:408
  74.9 2.0 %collective-permute-start.4 = (bf16[2048,256]{1,0:T(8,128)(2,1)}, bf16[2048,256]{1,0:T(8,128)(2,1)}, u32[]{:S(2)}, u32[]{:S(2)}) collective-permute-start(bf16[2048,256]{1,0:T(8,128)(2,1)} %collective-permute-done.3.refs_2_), channel_id=1, source_target_pairs={{0,1},{1,0},{2,3},{3,2},{4,5},{5,4},{6,7},{7,6},{8,9},{9,8},{10,11... | collective-permute-start | bytes 3145736 | tf_op jit(solution)/shard_map/ppermute | solution.py:409
  76.9 2.4 %collective-permute-start.7 = (bf16[2048,256]{1,0:T(8,128)(2,1)}, bf16[2048,256]{1,0:T(8,128)(2,1)}, u32[]{:S(2)}, u32[]{:S(2)}) collective-permute-start(bf16[2048,256]{1,0:T(8,128)(2,1)} %collective-permute-done.6.refs_6_), channel_id=1, source_target_pairs={{0,1},{1,0},{2,3},{3,2},{4,5},{5,4},{6,7},{7,6},{8,9},{9,8},{10,11... | collective-permute-start | bytes 3145736 | tf_op jit(solution)/shard_map/ppermute | solution.py:409
  79.2 4.4 %all-to-all-done.2 = bf16[64,8,128]{2,1,0:T(8,128)(2,1)S(1)} async-done(((bf16[64,8,128]{2,1,0:T(8,128)(2,1)}), bf16[64,8,128]{2,1,0:T(8,128)(2,1)S(1)}, u32[]{:S(2)}, u32[]{:S(2)}) %all-to-all-start.2) | async-done | bytes 131104 | tf_op jit(solution)/shard_map/all_to_all | solution.py:24
  84.5 6.0 %all-to-all-start.3 = ((bf16[8,16,2,8,128]{4,3,2,1,0:T(8,128)(2,1)}), bf16[8,16,2,8,128]{4,3,2,1,0:T(8,128)(2,1)S(1)}, u32[]{:S(2)}, u32[]{:S(2)}) async-start(bf16[8,16,2,8,128]{4,3,2,1,0:T(8,128)(2,1)} %shard_map.139), calls=%async_computation.3 | async-start | bytes 1048576 | tf_op jit(solution)/shard_map/all_to_all | solution.py:24
  90.6 17.9 %all-to-all-done.3.x_ref = bf16[8,16,2,8,128]{4,3,2,1,0:T(8,128)(2,1)S(1)} async-done(((bf16[8,16,2,8,128]{4,3,2,1,0:T(8,128)(2,1)}), bf16[8,16,2,8,128]{4,3,2,1,0:T(8,128)(2,1)S(1)}, u32[]{:S(2)}, u32[]{:S(2)}) %all-to-all-start.3) | async-done | bytes 524320 | tf_op jit(solution)/shard_map/all_to_all | solution.py:24
  108.4 8.2 %shard_map.141 = bf16[8,16,2,8,128]{4,3,2,1,0:T(8,128)(2,1)S(1)} custom-call(s32[2]{0:T(128)S(1)} %pad_add_fusion.place_ref, bf16[8,16,2,8,128]{4,3,2,1,0:T(8,128)(2,1)S(1)} %all-to-all-done.3.x_ref, bf16[32,2,16,128]{3,2,1,0:T(8,128)(2,1)S(1)} %bitcast.19, f32[16,128]{1,0:T(8,128)S(1)} %get-tuple-element.15.gain_ref, bf16[2048,256]{1,0:T(8,128)(2,1)} %bitcast.23, ...), custom_call_target="tpu_custom_call" | custom-call | tf_op jit(solution)/shard_map/pallas_call | solution.py:349
  116.6 20.2 %all_to_all.31.arrived_ref = bf16[8,16,2,8,128]{4,3,2,1,0:T(8,128)(2,1)S(1)} all-to-all(bf16[8,16,2,8,128]{4,3,2,1,0:T(8,128)(2,1)S(1)} %shard_map.141), channel_id=1, replica_groups=mesh['sp'=32,'y'=8,'c'=2] {'y'}, dimensions={0} | all-to-all | bytes 1048576 | tf_op jit(solution)/shard_map/all_to_all | solution.py:24
  136.9 17.0 %all_to_all.32.arrived_ref = bf16[64,8,128]{2,1,0:T(8,128)(2,1)S(1)} all-to-all(bf16[64,8,128]{2,1,0:T(8,128)(2,1)S(1)} %bitcast.21), channel_id=1, replica_groups=mesh['sp'=32,'y'=8,'c'=2] {'sp','c'}, dimensions={0} | all-to-all | bytes 262144 | tf_op jit(solution)/shard_map/all_to_all | solution.py:24
  153.9 0.9 shard_map.143
  (23 shorter events, 2.0 us)
Async XLA Ops:
  0.0 26.2 %copy-start.2 = (bf16[1,2048,256]{2,1,0:T(8,128)(2,1)S(1)}, bf16[1,2048,256]{2,1,0:T(8,128)(2,1)}, u32[]{:S(2)}) copy-start(bf16[1,2048,256]{2,1,0:T(8,128)(2,1)} %param.22) | copy-start | bytes 3145732
  1.6 83.0 %copy-start = (bf16[448,2048]{1,0:T(8,128)(2,1)}, bf16[448,2048]{1,0:T(8,128)(2,1)S(1)}, u32[]{:S(2)}) copy-start(bf16[448,2048]{1,0:T(8,128)(2,1)S(1)} %shard_map.140.refs_8_) | copy-start | bytes 5505028
  1.6 58.6 %copy-start.1 = (bf16[128,128]{1,0:T(8,128)(2,1)S(1)}, bf16[128,128]{1,0:T(8,128)(2,1)}, u32[]{:S(2)}) copy-start(bf16[128,128]{1,0:T(8,128)(2,1)} %residual_ref.1) | copy-start | bytes 98308
  1.6 37.7 %collective-permute-start.9 = (bf16[448,2048]{1,0:T(8,128)(2,1)S(1)}, bf16[448,2048]{1,0:T(8,128)(2,1)}, u32[]{:S(2)}, u32[]{:S(2)}) collective-permute-start(bf16[448,2048]{1,0:T(8,128)(2,1)S(1)} %shard_map.140.refs_8_), channel_id=1, source_target_pairs={{0,14},{1,3},{2,0},{3,5},{4,2},{5,7},{6,4},{7,9},{8,6},{9,11},{10,... | collective-permute-start | bytes 5505032 | tf_op jit(solution)/shard_map/ppermute | solution.py:407
  7.7 33.7 %all-to-all-start = ((bf16[64,16,128]{2,1,0:T(8,128)(2,1)}), bf16[64,16,128]{2,1,0:T(8,128)(2,1)S(1)}, u32[]{:S(2)}, u32[]{:S(2)}) async-start(bf16[64,16,128]{2,1,0:T(8,128)(2,1)} %bitcast.9), calls=%async_computation | async-start | bytes 524288 | tf_op jit(solution)/shard_map/all_to_all | solution.py:24
  23.8 9.6 %collective-permute-start = (bf16[144,128]{1,0:T(8,128)(2,1)S(1)}, bf16[144,128]{1,0:T(8,128)(2,1)S(1)}, u32[]{:S(2)}, u32[]{:S(2)}) collective-permute-start(bf16[144,128]{1,0:T(8,128)(2,1)S(1)} %get-tuple-element.12.side_ref), channel_id=1, source_target_pairs={{0,1},{1,0},{2,3},{3,2},{4,5},{5,4},{6,7},{7,6},{8,9},{9,8},{10,11... | collective-permute-start | bytes 110600 | tf_op jit(solution)/shard_map/ppermute | solution.py:413
  26.2 46.3 %collective-permute-start.3 = (bf16[2048,256]{1,0:T(8,128)(2,1)S(1)}, bf16[2048,256]{1,0:T(8,128)(2,1)}, u32[]{:S(2)}, u32[]{:S(2)}) collective-permute-start(bf16[2048,256]{1,0:T(8,128)(2,1)S(1)} %bitcast.24), channel_id=1, source_target_pairs={{0,14},{1,3},{2,0},{3,5},{4,2},{5,7},{6,4},{7,9},{8,6},{9,11},{10,... | collective-permute-start | bytes 3145736 | tf_op jit(solution)/shard_map/ppermute | solution.py:407
  28.1 46.7 %collective-permute-start.2 = (bf16[2048,256]{1,0:T(8,128)(2,1)S(1)}, bf16[2048,256]{1,0:T(8,128)(2,1)}, u32[]{:S(2)}, u32[]{:S(2)}) collective-permute-start(bf16[2048,256]{1,0:T(8,128)(2,1)S(1)} %bitcast.25), channel_id=1, source_target_pairs={{0,1},{1,0},{2,3},{3,2},{4,5},{5,4},{6,7},{7,6},{8,9},{9,8},{10,11... | collective-permute-start | bytes 3145736 | tf_op jit(solution)/shard_map/ppermute | solution.py:408
  31.5 4.3 %collective-permute-start.1 = (bf16[64,2048]{1,0:T(8,128)(2,1)}, bf16[64,2048]{1,0:T(8,128)(2,1)S(1)}, u32[]{:S(2)}, u32[]{:S(2)}) collective-permute-start(bf16[64,2048]{1,0:T(8,128)(2,1)} %source_ref.1), channel_id=1, source_target_pairs={{0,1},{1,0},{2,3},{3,2},{4,5},{5,4},{6,7},{7,6},{8,9},{9,8},{10,11... | collective-permute-start | bytes 786440 | tf_op jit(solution)/shard_map/ppermute | solution.py:414
  33.4 43.5 %collective-permute-start.6 = (bf16[2048,256]{1,0:T(8,128)(2,1)}, bf16[2048,256]{1,0:T(8,128)(2,1)}, u32[]{:S(2)}, u32[]{:S(2)}) collective-permute-start(bf16[2048,256]{1,0:T(8,128)(2,1)} %bitcast.26), channel_id=1, source_target_pairs={{0,14},{1,3},{2,0},{3,5},{4,2},{5,7},{6,4},{7,9},{8,6},{9,11},{10,... | collective-permute-start | bytes 3145736 | tf_op jit(solution)/shard_map/ppermute | solution.py:407
  35.7 54.8 %collective-permute-start.8 = (bf16[448,2048]{1,0:T(8,128)(2,1)S(1)}, bf16[448,2048]{1,0:T(8,128)(2,1)}, u32[]{:S(2)}, u32[]{:S(2)}) collective-permute-start(bf16[448,2048]{1,0:T(8,128)(2,1)S(1)} %shard_map.140.refs_8_), channel_id=1, source_target_pairs={{0,1},{1,0},{2,3},{3,2},{4,5},{5,4},{6,7},{7,6},{8,9},{9,8},{10,11... | collective-permute-start | bytes 5505032 | tf_op jit(solution)/shard_map/ppermute | solution.py:408
  39.3 69.1 %collective-permute-start.10 = (bf16[448,2048]{1,0:T(8,128)(2,1)}, bf16[448,2048]{1,0:T(8,128)(2,1)}, u32[]{:S(2)}, u32[]{:S(2)}) collective-permute-start(bf16[448,2048]{1,0:T(8,128)(2,1)} %collective-permute-done.9.refs_10_), channel_id=1, source_target_pairs={{0,1},{1,0},{2,3},{3,2},{4,5},{5,4},{6,7},{7,6},{8,9},{9,8},{10,11... | collective-permute-start | bytes 5505032 | tf_op jit(solution)/shard_map/ppermute | solution.py:409
  61.0 22.6 %all-to-all-start.2 = ((bf16[64,8,128]{2,1,0:T(8,128)(2,1)}), bf16[64,8,128]{2,1,0:T(8,128)(2,1)S(1)}, u32[]{:S(2)}, u32[]{:S(2)}) async-start(bf16[64,8,128]{2,1,0:T(8,128)(2,1)} %get-tuple-element.14), calls=%async_computation.2 | async-start | bytes 262144 | tf_op jit(solution)/shard_map/all_to_all | solution.py:24
  72.5 18.1 %collective-permute-start.5 = (bf16[2048,256]{1,0:T(8,128)(2,1)}, bf16[2048,256]{1,0:T(8,128)(2,1)}, u32[]{:S(2)}, u32[]{:S(2)}) collective-permute-start(bf16[2048,256]{1,0:T(8,128)(2,1)} %bitcast.27), channel_id=1, source_target_pairs={{0,1},{1,0},{2,3},{3,2},{4,5},{5,4},{6,7},{7,6},{8,9},{9,8},{10,11... | collective-permute-start | bytes 3145736 | tf_op jit(solution)/shard_map/ppermute | solution.py:408
  74.9 15.7 %collective-permute-start.4 = (bf16[2048,256]{1,0:T(8,128)(2,1)}, bf16[2048,256]{1,0:T(8,128)(2,1)}, u32[]{:S(2)}, u32[]{:S(2)}) collective-permute-start(bf16[2048,256]{1,0:T(8,128)(2,1)} %collective-permute-done.3.refs_2_), channel_id=1, source_target_pairs={{0,1},{1,0},{2,3},{3,2},{4,5},{5,4},{6,7},{7,6},{8,9},{9,8},{10,11... | collective-permute-start | bytes 3145736 | tf_op jit(solution)/shard_map/ppermute | solution.py:409
  76.9 13.7 %collective-permute-start.7 = (bf16[2048,256]{1,0:T(8,128)(2,1)}, bf16[2048,256]{1,0:T(8,128)(2,1)}, u32[]{:S(2)}, u32[]{:S(2)}) collective-permute-start(bf16[2048,256]{1,0:T(8,128)(2,1)} %collective-permute-done.6.refs_6_), channel_id=1, source_target_pairs={{0,1},{1,0},{2,3},{3,2},{4,5},{5,4},{6,7},{7,6},{8,9},{9,8},{10,11... | collective-permute-start | bytes 3145736 | tf_op jit(solution)/shard_map/ppermute | solution.py:409
  84.5 23.9 %all-to-all-start.3 = ((bf16[8,16,2,8,128]{4,3,2,1,0:T(8,128)(2,1)}), bf16[8,16,2,8,128]{4,3,2,1,0:T(8,128)(2,1)S(1)}, u32[]{:S(2)}, u32[]{:S(2)}) async-start(bf16[8,16,2,8,128]{4,3,2,1,0:T(8,128)(2,1)} %shard_map.139), calls=%async_computation.3 | async-start | bytes 1048576 | tf_op jit(solution)/shard_map/all_to_all | solution.py:24

commit v7 on v6

--- a/solution.py
+++ b/solution.py
@@ -9,9 +9,6 @@
 
 F32 = jnp.float32
 BF16 = jnp.bfloat16
-SUM_LANE = 64
-W_LANE = 80
-META_LANE = 88
 
 
 SWAP = ((0, 1), (1, 0))
@@ -70,12 +67,14 @@
         jnp.zeros((7, 128), F32),
     ]
     side_ref[128:144] = jnp.concatenate(tail, axis=0).astype(BF16)
-    spread = (lane == across) | ((across % 4 == 3) & (lane == SUM_LANE + across // 4))
-    wide = matmul(values, spread.astype(F32).astype(BF16))
+    low = (lane == across).astype(F32).astype(BF16)
+    high = (lane == across + channels).astype(F32).astype(BF16)
+    rim = matmul(values[rows - 16 :], low)[0:8] + matmul(values[rows - 16 :], high)[8:16]
     docs = docs_ref[...].astype(F32)
     last_doc = docs[:, rows - 1 :]
     trailing = (docs == last_doc).astype(F32)
-    sums = matmul(jnp.broadcast_to(trailing, (8, rows)).astype(BF16), wide.astype(BF16))[0:1]
+    sums = matmul(jnp.broadcast_to(trailing, (8, rows)).astype(BF16), values)
+    parts = [matmul(part.astype(BF16), low)[0:1] for part in three_parts(sums)]
     count = jnp.sum(trailing, axis=1, keepdims=True)
 
     lines = [jnp.broadcast_to(routes_ref[k : k + 1].astype(F32), square) for k in (0, 1)]
@@ -93,32 +92,31 @@
         [first_slot, second_slot, jnp.zeros((6, rows), F32)], axis=0
     )
     share = [weights_ref[k : k + 1] for k in (0, 1)]
-    slot = iota((512, rows), 0).astype(F32)
-    is_first = slot == first_slot
-    is_second = slot == second_slot
-    weight = jnp.sum(
-        jnp.where(is_first, share[0], 0.0) + jnp.where(is_second, share[1], 0.0),
-        axis=1,
-        keepdims=True,
-    )
-    chosen_first = jnp.sum(is_first.astype(F32), axis=1, keepdims=True)
-
-    row = iota((16, 128), 0)
-    at = iota((16, 128), 1)
-    parts = three_parts(sums)
-    shared = jnp.where(at < channels, wide[rows - 16 :], 0.0)
-    in_sums = (at >= SUM_LANE) & (at < SUM_LANE + 16)
+    line = iota((256, rows), 0)
+    row = iota((8, 128), 0)
+    at = iota((8, 128), 1)
+    in_sums = (at < channels) & (at % 4 == 3)
     for k in range(3):
-        shared = jnp.where(in_sums & (row == k), parts[k], shared)
+        rim = jnp.where(in_sums & (row == k), parts[k], rim)
     doc_high = jnp.floor(last_doc * (1.0 / 128.0))
     doc_low = last_doc - doc_high * 128.0
     for k, value in enumerate((count, doc_high, doc_low)):
-        shared = jnp.where(at == META_LANE + k, value, shared)
-    place = iota((512, 128), 1)
-    message = jnp.broadcast_to(shared[None], (32, 16, 128)).reshape(512, 128)
-    for k, value in enumerate((*three_parts(weight), chosen_first)):
-        message = jnp.where(place == W_LANE + k, value, message)
-    message = message.reshape(32, 16, 128).astype(BF16)
+        rim = jnp.where((row == 3) & (at == 3 + 4 * k), value, rim)
+    place = iota((256, 128), 1)
+    message = jnp.broadcast_to(rim[None], (32, 8, 128)).reshape(256, 128)
+    for half in (0, 1):
+        slot = (line // 8 * 16 + line % 8 + 8 * half).astype(F32)
+        is_first = slot == first_slot
+        is_second = slot == second_slot
+        weight = jnp.sum(
+            jnp.where(is_first, share[0], 0.0) + jnp.where(is_second, share[1], 0.0),
+            axis=1,
+            keepdims=True,
+        )
+        chosen_first = jnp.sum(is_first.astype(F32), axis=1, keepdims=True)
+        for k, value in enumerate((*three_parts(weight), chosen_first)):
+            message = jnp.where(place == 1 + 4 * k + 16 * half, value, message)
+    message = message.reshape(32, 8, 128).astype(BF16)
     message_ref[:, 0] = message
     message_ref[:, 1] = message
 
@@ -158,12 +156,9 @@
     sides = side_ref[...].astype(F32) + other_ref[...].astype(F32)
     values = sides[0:128].astype(BF16)
     gain = sides[128:129] + (sides[129:130] + sides[130:131])
-    meta = arrived_ref[:, 0, 0:8].astype(F32)[:, 0:1]
-    their_count = meta[:, :, META_LANE : META_LANE + 1]
-    their_doc = (
-        meta[:, :, META_LANE + 1 : META_LANE + 2] * 128.0
-        + meta[:, :, META_LANE + 2 : META_LANE + 3]
-    )
+    meta = arrived_ref[:, 0].astype(F32)[:, 3:4]
+    their_count = meta[:, :, 3:4]
+    their_doc = meta[:, :, 7:8] * 128.0 + meta[:, :, 11:12]
     block = iota((32, 1, 1), 0)
     joins = (block < own) & (their_doc == first_doc.reshape(1, 1, 1))
     behind = block == own - 1
@@ -171,21 +166,23 @@
     source = iota((128, 128), 0)
     target = iota((128, 128), 1)
     carry = jnp.zeros((8, 128), F32)
-    rim = jnp.zeros((16, 128), F32)
+    upper_rim = jnp.zeros((8, 128), F32)
+    lower_rim = jnp.zeros((8, 128), F32)
     for side in (0, 1):
         arrived = arrived_ref[:, side].astype(F32)
-        sums = jnp.sum(jnp.where(joins, arrived[:, 0:8], 0.0), axis=0)
+        sums = jnp.sum(jnp.where(joins, arrived, 0.0), axis=0)
         total = jnp.sum(jnp.where(iota((8, 128), 0) < 3, sums, 0.0), axis=0, keepdims=True)
         here = target - 64 * side
         inside = (here >= 0) & (here < 64)
-        back = inside & (here % 4 == 3) & (source == SUM_LANE + here // 4)
-        back = back.astype(F32).astype(BF16)
+        low = (inside & (source == here)).astype(F32).astype(BF16)
+        high = (inside & (source == here + 64)).astype(F32).astype(BF16)
         for part in three_parts(total):
-            carry = carry + matmul(jnp.broadcast_to(part, (8, 128)).astype(BF16), back)
+            carry = carry + matmul(jnp.broadcast_to(part, (8, 128)).astype(BF16), low)
         their_rim = jnp.sum(jnp.where(behind, arrived, 0.0), axis=0).astype(BF16)
-        rim = rim + matmul(their_rim, (inside & (source == here)).astype(F32).astype(BF16))
+        upper_rim = upper_rim + matmul(their_rim, low)
+        lower_rim = lower_rim + matmul(their_rim, high)
     carry = carry[0:1]
-    rim = rim.astype(BF16)
+    rim = jnp.concatenate([upper_rim, lower_rim], axis=0).astype(BF16)
     rim_rows = jnp.sum(jnp.where(behind & joins, their_count, 0.0), axis=0)
 
     square = (rows, rows)
@@ -247,15 +244,14 @@
 
 
 def experts(place_ref, x_ref, message_ref, gain_ref, *refs):
-    sources, out_ref, normed_ref = refs[:12], refs[12], refs[13]
-    near, landed = refs[14:26], refs[26]
+    sources, out_ref, normed_ref, sum_ref = refs[:12], refs[12], refs[13], refs[14]
+    near, landed = refs[15:27], refs[27]
     gates, ups, lowers = near[0:4], near[4:8], near[8:12]
-    order = (0, 4, 1, 5, 2, 6, 3, 7, 8, 9, 10, 11)
     copies = [
-        pltpu.make_async_copy(sources[k], near[k], landed.at[k]) for k in order
+        pltpu.make_async_copy(sources[k], near[k], landed.at[k]) for k in range(12)
     ]
-    for copy in copies[:6]:
-        copy.start()
+    for k in (0, 4, 1, 5, 2, 6, 8, 9, 10, 11, 3, 7):
+        copies[k].start()
 
     squares = jnp.zeros((128, 128), F32)
     for k in range(16):
@@ -267,25 +263,22 @@
         normed_ref[:, 128 * k : 128 * (k + 1)] = (part * scaling * gain_ref[k : k + 1]).astype(
             BF16
         )
-    message = message_ref[:, 0].astype(F32).reshape(16, 2, 16, 128)
-    message = jnp.where(place_ref[1] == 0, message[:, 0], message[:, 1])
-    side = jnp.where(place_ref[0] == 0, message[:, 0:8], message[:, 8:16])
-    side = side.reshape(128, 128)
-    weight = side[:, W_LANE : W_LANE + 1] + (
-        side[:, W_LANE + 1 : W_LANE + 2] + side[:, W_LANE + 2 : W_LANE + 3]
-    )
-    first = side[:, W_LANE + 3 : W_LANE + 4]
+    message = message_ref[:, 0].astype(F32).reshape(16, 2, 8, 128)
+    side = jnp.where(place_ref[1] == 0, message[:, 0], message[:, 1]).reshape(128, 128)
+    left = place_ref[0] == 0
+    told = [jnp.where(left, side[:, k : k + 1], side[:, k + 16 : k + 17]) for k in (1, 5, 9, 13)]
+    weight = told[0] + (told[1] + told[2])
+    first = told[3]
     normed = normed_ref[...]
-    hidden = []
-    for k, (gate, up) in enumerate(zip(gates, ups)):
-        copies[2 * k].wait()
-        copies[2 * k + 1].wait()
-        if k < 3:
-            copies[6 + 2 * k].start()
-            copies[7 + 2 * k].start()
-        lower = matmul(normed, gate[...])
-        upper = matmul(normed, up[...])
-        hidden.append((jax.nn.silu(lower) * upper * weight).astype(BF16))
+
+    def hidden(k):
+        copies[k].wait()
+        copies[k + 4].wait()
+        lower = matmul(normed, gates[k][...])
+        upper = matmul(normed, ups[k][...])
+        return (jax.nn.silu(lower) * upper * weight).astype(BF16)
+
+    early = [hidden(k) for k in range(3)]
     for copy in copies[8:]:
         copy.wait()
     across = jnp.concatenate(
@@ -299,8 +292,13 @@
     for k in range(8):
         cut = slice(256 * k, 256 * (k + 1))
         total = matmul(shared, shared_down[:, cut])
-        for value, pack in zip(hidden, lowers):
+        for value, pack in zip(early, lowers):
             total = total + matmul(value, pack[0:256, cut])
+        sum_ref[k] = total
+    last = hidden(3)
+    for k in range(8):
+        cut = slice(256 * k, 256 * (k + 1))
+        total = sum_ref[k] + matmul(last, lowers[3][0:256, cut])
         out_ref[k, :, 0] = total[:, :128].reshape(16, 8, 128).astype(BF16)
         out_ref[k, :, 1] = total[:, 128:].reshape(16, 8, 128).astype(BF16)
 
@@ -383,7 +381,7 @@
     index = jnp.stack([lax.axis_index("sp").astype(jnp.int32), core])
     message, slots, side = kernel(
         opening,
-        (array((32, 2, 16, 128), BF16), array((8, 128), F32), array((144, 128), BF16)),
+        (array((32, 2, 8, 128), BF16), array((8, 128), F32), array((144, 128), BF16)),
         (
             core.reshape(1),
             pool_input.T,
@@ -408,8 +406,8 @@
         own_other = lax.ppermute(value, "c", SWAP)
         ring_other = lax.ppermute(ring, "c", SWAP)
         groups += [value, own_other, ring, ring_other]
-    arrived = exchanged(message.reshape(64, 16, 128), ("sp", "c"))
-    arrived = arrived.reshape(32, 2, 16, 128)
+    arrived = exchanged(message.reshape(64, 8, 128), ("sp", "c"))
+    arrived = arrived.reshape(32, 2, 8, 128)
     other_side = lax.ppermute(side, "c", SWAP)
     other_project = lax.ppermute(out_proj, "c", SWAP)
     terms = kernel(
@@ -441,7 +439,7 @@
         near=(rows, arrived, gains),
         far=groups,
         scalars=1,
-        scratch=[pltpu.VMEM((128, 2048), BF16)]
+        scratch=[pltpu.VMEM((128, 2048), BF16), pltpu.VMEM((8, 128, 256), F32)]
         + [pltpu.VMEM(value.shape, BF16) for value in groups]
         + [pltpu.SemaphoreType.DMA((12,))],
         room=24,

time: 156 us -> 155 us (level)
  waiting for transfers between devices: 22.3 us -> 29 us
  starting transfers between devices: 61.7 us -> 56.1 us
    all_to_all x3, starting transfers between devices: 33.6 us -> 24.4 us  [exchanged(): return lax.all_to_all(value, axis, split_axis=0, concat_axis=0, tiled=True)]
    all_to_all x3, waiting for transfers between devices: 22.3 us -> 29 us  [exchanged(): return lax.all_to_all(value, axis, split_axis=0, concat_axis=0, tiled=True)]
    ppermute x1, starting transfers between devices: 2.36 us -> 6.63 us  [body(): other_side = lax.ppermute(side, 'c', SWAP)]
    ppermute x3, starting transfers between devices: 9.24 us -> 6.65 us  [body(): own_other = lax.ppermute(value, 'c', SWAP)]
  transfers between devices with their start and end apart: 14 -> 14, of which waited for: 2 -> 3; matrix products, arithmetic and copies ran while one was open for 0% -> 0% of each run, Pallas kernels for 4% -> 4%
where the time goes in v7:
time: 155 us; the launch traced here: 154 us
  starting transfers between devices  56.1 us (36%)
  blocking collectives  52.5 us (34%)
  waiting for transfers between devices  29 us (19%)
  Pallas kernels  16.3 us (11%)
    all_to_all x3, blocking collectives, exchanged(): return lax.all_to_all(value, axis, split_axis=0, concat_axis=0, tiled=True)  52.5 us
    all_to_all x3, waiting for transfers between devices, exchanged(): return lax.all_to_all(value, axis, split_axis=0, concat_axis=0, tiled=True)  29 us
    all_to_all x3, starting transfers between devices, exchanged(): return lax.all_to_all(value, axis, split_axis=0, concat_axis=0, tiled=True)  24.4 us
    pallas_call x8, Pallas kernels, kernel(): pl.pallas_call(body, out_shape=outs, in_specs=[SMEM] * scalars + [VMEM] *...  16.3 us
    ppermute x3, starting transfers between devices, body(): ring = lax.ppermute(value, ('y', 'c'), AROUND)  9.72 us
    ppermute x3, starting transfers between devices, body(): own_other = lax.ppermute(value, 'c', SWAP)  6.65 us
    ppermute x1, starting transfers between devices, body(): other_side = lax.ppermute(side, 'c', SWAP)  6.63 us
    ppermute x3, starting transfers between devices, body(): ring_other = lax.ppermute(ring, 'c', SWAP)  6.29 us
  transfers between devices with their start and end apart: 14, of which 3 were waited for; matrix products, arithmetic and copies ran while one was open for 0% of the time, Pallas kernels for 4%

profile of v7, /device:TPU:1, one launch (start us, length us, event | category | flops | bytes accessed | tf_op | source)
XLA Modules:
  0.0 154.4 jit_solution(12591342700694410031)
XLA Ops:
  0.0 1.5 %shard_map.140.refs_8_ = bf16[448,2048]{1,0:T(8,128)(2,1)S(1)} custom-call(bf16[256,2048]{1,0:T(8,128)(2,1)} %bitcast.22, bf16[64,2048]{1,0:T(8,128)(2,1)} %bitcast.29, bf16[64,2048]{1,0:T(8,128)(2,1)} %bitcast.30, bf16[64,2048]{1,0:T(8,128)(2,1)} %refs_3_.1), custom_call_target="tpu_custom_call" | custom-call | tf_op jit(solution)/shard_map/pallas_call | solution.py:347
  1.6 4.2 %collective-permute-start.9 = (bf16[448,2048]{1,0:T(8,128)(2,1)S(1)}, bf16[448,2048]{1,0:T(8,128)(2,1)}, u32[]{:S(2)}, u32[]{:S(2)}) collective-permute-start(bf16[448,2048]{1,0:T(8,128)(2,1)S(1)} %shard_map.140.refs_8_), channel_id=1, source_target_pairs={{0,14},{1,3},{2,0},{3,5},{4,2},{5,7},{6,4},{7,9},{8,6},{9,11},{10,... | collective-permute-start | bytes 5505032 | tf_op jit(solution)/shard_map/ppermute | solution.py:405
  5.7 1.8 %shard_map.136 = (bf16[32,2,8,128]{3,2,1,0:T(8,128)(2,1)}, f32[8,128]{1,0:T(8,128)S(1)}, bf16[144,128]{1,0:T(8,128)(2,1)S(1)}) custom-call(s32[1]{0:T(128)} %bitcast.core_ref, bf16[64,128]{1,0:T(8,128)(2,1)} %bitcast.31, s32[1,128]{1,0:T(1,128)} %bitcast.32, s32[2,128]{1,0:T(2,128)} %bitcast.34, f32[2,128]{1,0:T(2,128)} %bitcast.35, f32[1,64]{1,0:T(1,128)} %bitcast.36, ...), custom_call_target="tpu_custom_call" | custom-call | tf_op jit(solution)/shard_map/pallas_call | solution.py:347
  7.6 6.6 %collective-permute-start = (bf16[144,128]{1,0:T(8,128)(2,1)S(1)}, bf16[144,128]{1,0:T(8,128)(2,1)S(1)}, u32[]{:S(2)}, u32[]{:S(2)}) collective-permute-start(bf16[144,128]{1,0:T(8,128)(2,1)S(1)} %get-tuple-element.12.side_ref), channel_id=1, source_target_pairs={{0,1},{1,0},{2,3},{3,2},{4,5},{5,4},{6,7},{7,6},{8,9},{9,8},{10,11... | collective-permute-start | bytes 110600 | tf_op jit(solution)/shard_map/ppermute | solution.py:411
  14.2 3.6 %collective-permute-start.3 = (bf16[2048,256]{1,0:T(8,128)(2,1)S(1)}, bf16[2048,256]{1,0:T(8,128)(2,1)}, u32[]{:S(2)}, u32[]{:S(2)}) collective-permute-start(bf16[2048,256]{1,0:T(8,128)(2,1)S(1)} %bitcast.24), channel_id=1, source_target_pairs={{0,14},{1,3},{2,0},{3,5},{4,2},{5,7},{6,4},{7,9},{8,6},{9,11},{10,... | collective-permute-start | bytes 3145736 | tf_op jit(solution)/shard_map/ppermute | solution.py:405
  17.9 1.9 %collective-permute-start.2 = (bf16[2048,256]{1,0:T(8,128)(2,1)S(1)}, bf16[2048,256]{1,0:T(8,128)(2,1)}, u32[]{:S(2)}, u32[]{:S(2)}) collective-permute-start(bf16[2048,256]{1,0:T(8,128)(2,1)S(1)} %bitcast.25), channel_id=1, source_target_pairs={{0,1},{1,0},{2,3},{3,2},{4,5},{5,4},{6,7},{7,6},{8,9},{9,8},{10,11... | collective-permute-start | bytes 3145736 | tf_op jit(solution)/shard_map/ppermute | solution.py:406
  19.8 2.4 %collective-permute-start.1 = (bf16[64,2048]{1,0:T(8,128)(2,1)}, bf16[64,2048]{1,0:T(8,128)(2,1)S(1)}, u32[]{:S(2)}, u32[]{:S(2)}) collective-permute-start(bf16[64,2048]{1,0:T(8,128)(2,1)} %source_ref.1), channel_id=1, source_target_pairs={{0,1},{1,0},{2,3},{3,2},{4,5},{5,4},{6,7},{7,6},{8,9},{9,8},{10,11... | collective-permute-start | bytes 786440 | tf_op jit(solution)/shard_map/ppermute | solution.py:412
  22.3 1.9 %collective-permute-start.6 = (bf16[2048,256]{1,0:T(8,128)(2,1)}, bf16[2048,256]{1,0:T(8,128)(2,1)}, u32[]{:S(2)}, u32[]{:S(2)}) collective-permute-start(bf16[2048,256]{1,0:T(8,128)(2,1)} %bitcast.26), channel_id=1, source_target_pairs={{0,14},{1,3},{2,0},{3,5},{4,2},{5,7},{6,4},{7,9},{8,6},{9,11},{10,... | collective-permute-start | bytes 3145736 | tf_op jit(solution)/shard_map/ppermute | solution.py:405
  24.2 12.7 %all-to-all-start = ((bf16[64,8,128]{2,1,0:T(8,128)(2,1)}), bf16[64,8,128]{2,1,0:T(8,128)(2,1)S(1)}, u32[]{:S(2)}, u32[]{:S(2)}) async-start(bf16[64,8,128]{2,1,0:T(8,128)(2,1)} %bitcast.9), calls=%async_computation | async-start | bytes 262144 | tf_op jit(solution)/shard_map/all_to_all | solution.py:21
  36.9 2.4 %collective-permute-start.8 = (bf16[448,2048]{1,0:T(8,128)(2,1)S(1)}, bf16[448,2048]{1,0:T(8,128)(2,1)}, u32[]{:S(2)}, u32[]{:S(2)}) collective-permute-start(bf16[448,2048]{1,0:T(8,128)(2,1)S(1)} %shard_map.140.refs_8_), channel_id=1, source_target_pairs={{0,1},{1,0},{2,3},{3,2},{4,5},{5,4},{6,7},{7,6},{8,9},{9,8},{10,11... | collective-permute-start | bytes 5505032 | tf_op jit(solution)/shard_map/ppermute | solution.py:406
  39.3 2.0 %collective-permute-start.10 = (bf16[448,2048]{1,0:T(8,128)(2,1)}, bf16[448,2048]{1,0:T(8,128)(2,1)}, u32[]{:S(2)}, u32[]{:S(2)}) collective-permute-start(bf16[448,2048]{1,0:T(8,128)(2,1)} %collective-permute-done.9.refs_10_), channel_id=1, source_target_pairs={{0,1},{1,0},{2,3},{3,2},{4,5},{5,4},{6,7},{7,6},{8,9},{9,8},{10,11... | collective-permute-start | bytes 5505032 | tf_op jit(solution)/shard_map/ppermute | solution.py:407
  41.3 6.7 %all-to-all-done = bf16[64,8,128]{2,1,0:T(8,128)(2,1)S(1)} async-done(((bf16[64,8,128]{2,1,0:T(8,128)(2,1)}), bf16[64,8,128]{2,1,0:T(8,128)(2,1)S(1)}, u32[]{:S(2)}, u32[]{:S(2)}) %all-to-all-start) | async-done | bytes 131104 | tf_op jit(solution)/shard_map/all_to_all | solution.py:21
  48.0 2.5 %shard_map.137 = bf16[8,136,128]{2,1,0:T(8,128)(2,1)S(1)} custom-call(s32[2]{0:T(128)S(1)} %pad_add_fusion.1.index_ref, bf16[32,2,8,128]{3,2,1,0:T(8,128)(2,1)S(1)} %bitcast.18, bf16[144,128]{1,0:T(8,128)(2,1)S(1)} %get-tuple-element.12.side_ref, bf16[144,128]{1,0:T(8,128)(2,1)S(1)} %collective-permute-done.other_ref, ...), custom_call_target="tpu_custom_call" | custom-call | tf_op jit(solution)/shard_map/pallas_call | solution.py:347
  50.5 15.3 %all_to_all.30.arrived_ref = bf16[8,136,128]{2,1,0:T(8,128)(2,1)S(1)} all-to-all(bf16[8,136,128]{2,1,0:T(8,128)(2,1)S(1)} %shard_map.137), channel_id=1, replica_groups=mesh['sp'=32,'y'=8,'c'=2] {'y'}, dimensions={0} | all-to-all | bytes 557056 | tf_op jit(solution)/shard_map/all_to_all | solution.py:21
  66.7 5.9 %all-to-all-start.2 = ((bf16[64,8,128]{2,1,0:T(8,128)(2,1)}), bf16[64,8,128]{2,1,0:T(8,128)(2,1)S(1)}, u32[]{:S(2)}, u32[]{:S(2)}) async-start(bf16[64,8,128]{2,1,0:T(8,128)(2,1)} %get-tuple-element.14), calls=%async_computation.2 | async-start | bytes 262144 | tf_op jit(solution)/shard_map/all_to_all | solution.py:21
  72.6 2.4 %collective-permute-start.5 = (bf16[2048,256]{1,0:T(8,128)(2,1)}, bf16[2048,256]{1,0:T(8,128)(2,1)}, u32[]{:S(2)}, u32[]{:S(2)}) collective-permute-start(bf16[2048,256]{1,0:T(8,128)(2,1)} %bitcast.27), channel_id=1, source_target_pairs={{0,1},{1,0},{2,3},{3,2},{4,5},{5,4},{6,7},{7,6},{8,9},{9,8},{10,11... | collective-permute-start | bytes 3145736 | tf_op jit(solution)/shard_map/ppermute | solution.py:406
  75.0 2.0 %collective-permute-start.4 = (bf16[2048,256]{1,0:T(8,128)(2,1)}, bf16[2048,256]{1,0:T(8,128)(2,1)}, u32[]{:S(2)}, u32[]{:S(2)}) collective-permute-start(bf16[2048,256]{1,0:T(8,128)(2,1)} %collective-permute-done.3.refs_2_), channel_id=1, source_target_pairs={{0,1},{1,0},{2,3},{3,2},{4,5},{5,4},{6,7},{7,6},{8,9},{9,8},{10,11... | collective-permute-start | bytes 3145736 | tf_op jit(solution)/shard_map/ppermute | solution.py:407
  76.9 2.4 %collective-permute-start.7 = (bf16[2048,256]{1,0:T(8,128)(2,1)}, bf16[2048,256]{1,0:T(8,128)(2,1)}, u32[]{:S(2)}, u32[]{:S(2)}) collective-permute-start(bf16[2048,256]{1,0:T(8,128)(2,1)} %collective-permute-done.6.refs_6_), channel_id=1, source_target_pairs={{0,1},{1,0},{2,3},{3,2},{4,5},{5,4},{6,7},{7,6},{8,9},{9,8},{10,11... | collective-permute-start | bytes 3145736 | tf_op jit(solution)/shard_map/ppermute | solution.py:407
  79.3 4.4 %all-to-all-done.2 = bf16[64,8,128]{2,1,0:T(8,128)(2,1)S(1)} async-done(((bf16[64,8,128]{2,1,0:T(8,128)(2,1)}), bf16[64,8,128]{2,1,0:T(8,128)(2,1)S(1)}, u32[]{:S(2)}, u32[]{:S(2)}) %all-to-all-start.2) | async-done | bytes 131104 | tf_op jit(solution)/shard_map/all_to_all | solution.py:21
  84.6 5.9 %all-to-all-start.3 = ((bf16[8,16,2,8,128]{4,3,2,1,0:T(8,128)(2,1)}), bf16[8,16,2,8,128]{4,3,2,1,0:T(8,128)(2,1)S(1)}, u32[]{:S(2)}, u32[]{:S(2)}) async-start(bf16[8,16,2,8,128]{4,3,2,1,0:T(8,128)(2,1)} %shard_map.139), calls=%async_computation.3 | async-start | bytes 1048576 | tf_op jit(solution)/shard_map/all_to_all | solution.py:21
  90.6 17.9 %all-to-all-done.3.x_ref = bf16[8,16,2,8,128]{4,3,2,1,0:T(8,128)(2,1)S(1)} async-done(((bf16[8,16,2,8,128]{4,3,2,1,0:T(8,128)(2,1)}), bf16[8,16,2,8,128]{4,3,2,1,0:T(8,128)(2,1)S(1)}, u32[]{:S(2)}, u32[]{:S(2)}) %all-to-all-start.3) | async-done | bytes 524320 | tf_op jit(solution)/shard_map/all_to_all | solution.py:21
  108.4 7.7 %shard_map.141 = bf16[8,16,2,8,128]{4,3,2,1,0:T(8,128)(2,1)S(1)} custom-call(s32[2]{0:T(128)S(1)} %pad_add_fusion.place_ref, bf16[8,16,2,8,128]{4,3,2,1,0:T(8,128)(2,1)S(1)} %all-to-all-done.3.x_ref, bf16[32,2,8,128]{3,2,1,0:T(8,128)(2,1)S(1)} %bitcast.19, f32[16,128]{1,0:T(8,128)S(1)} %get-tuple-element.15.gain_ref, bf16[2048,256]{1,0:T(8,128)(2,1)} %bitcast.23, ...), custom_call_target="tpu_custom_call" | custom-call | tf_op jit(solution)/shard_map/pallas_call | solution.py:347
  116.2 20.2 %all_to_all.31.arrived_ref = bf16[8,16,2,8,128]{4,3,2,1,0:T(8,128)(2,1)S(1)} all-to-all(bf16[8,16,2,8,128]{4,3,2,1,0:T(8,128)(2,1)S(1)} %shard_map.141), channel_id=1, replica_groups=mesh['sp'=32,'y'=8,'c'=2] {'y'}, dimensions={0} | all-to-all | bytes 1048576 | tf_op jit(solution)/shard_map/all_to_all | solution.py:21
  136.5 17.0 %all_to_all.32.arrived_ref = bf16[64,8,128]{2,1,0:T(8,128)(2,1)S(1)} all-to-all(bf16[64,8,128]{2,1,0:T(8,128)(2,1)S(1)} %bitcast.21), channel_id=1, replica_groups=mesh['sp'=32,'y'=8,'c'=2] {'sp','c'}, dimensions={0} | all-to-all | bytes 262144 | tf_op jit(solution)/shard_map/all_to_all | solution.py:21
  (23 shorter events, 2.9 us)
Async XLA Ops:
  0.0 14.2 %copy-start.2 = (bf16[1,2048,256]{2,1,0:T(8,128)(2,1)S(1)}, bf16[1,2048,256]{2,1,0:T(8,128)(2,1)}, u32[]{:S(2)}) copy-start(bf16[1,2048,256]{2,1,0:T(8,128)(2,1)} %param.22) | copy-start | bytes 3145732
  1.6 83.0 %copy-start = (bf16[448,2048]{1,0:T(8,128)(2,1)}, bf16[448,2048]{1,0:T(8,128)(2,1)S(1)}, u32[]{:S(2)}) copy-start(bf16[448,2048]{1,0:T(8,128)(2,1)S(1)} %shard_map.140.refs_8_) | copy-start | bytes 5505028
  1.6 64.2 %copy-start.1 = (bf16[128,128]{1,0:T(8,128)(2,1)S(1)}, bf16[128,128]{1,0:T(8,128)(2,1)}, u32[]{:S(2)}) copy-start(bf16[128,128]{1,0:T(8,128)(2,1)} %residual_ref.1) | copy-start | bytes 98308
  1.6 37.7 %collective-permute-start.9 = (bf16[448,2048]{1,0:T(8,128)(2,1)S(1)}, bf16[448,2048]{1,0:T(8,128)(2,1)}, u32[]{:S(2)}, u32[]{:S(2)}) collective-permute-start(bf16[448,2048]{1,0:T(8,128)(2,1)S(1)} %shard_map.140.refs_8_), channel_id=1, source_target_pairs={{0,14},{1,3},{2,0},{3,5},{4,2},{5,7},{6,4},{7,9},{8,6},{9,11},{10,... | collective-permute-start | bytes 5505032 | tf_op jit(solution)/shard_map/ppermute | solution.py:405
  7.6 14.7 %collective-permute-start = (bf16[144,128]{1,0:T(8,128)(2,1)S(1)}, bf16[144,128]{1,0:T(8,128)(2,1)S(1)}, u32[]{:S(2)}, u32[]{:S(2)}) collective-permute-start(bf16[144,128]{1,0:T(8,128)(2,1)S(1)} %get-tuple-element.12.side_ref), channel_id=1, source_target_pairs={{0,1},{1,0},{2,3},{3,2},{4,5},{5,4},{6,7},{7,6},{8,9},{9,8},{10,11... | collective-permute-start | bytes 110600 | tf_op jit(solution)/shard_map/ppermute | solution.py:411
  14.2 58.3 %collective-permute-start.3 = (bf16[2048,256]{1,0:T(8,128)(2,1)S(1)}, bf16[2048,256]{1,0:T(8,128)(2,1)}, u32[]{:S(2)}, u32[]{:S(2)}) collective-permute-start(bf16[2048,256]{1,0:T(8,128)(2,1)S(1)} %bitcast.24), channel_id=1, source_target_pairs={{0,14},{1,3},{2,0},{3,5},{4,2},{5,7},{6,4},{7,9},{8,6},{9,11},{10,... | collective-permute-start | bytes 3145736 | tf_op jit(solution)/shard_map/ppermute | solution.py:405
  17.9 57.1 %collective-permute-start.2 = (bf16[2048,256]{1,0:T(8,128)(2,1)S(1)}, bf16[2048,256]{1,0:T(8,128)(2,1)}, u32[]{:S(2)}, u32[]{:S(2)}) collective-permute-start(bf16[2048,256]{1,0:T(8,128)(2,1)S(1)} %bitcast.25), channel_id=1, source_target_pairs={{0,1},{1,0},{2,3},{3,2},{4,5},{5,4},{6,7},{7,6},{8,9},{9,8},{10,11... | collective-permute-start | bytes 3145736 | tf_op jit(solution)/shard_map/ppermute | solution.py:406
  19.8 17.0 %collective-permute-start.1 = (bf16[64,2048]{1,0:T(8,128)(2,1)}, bf16[64,2048]{1,0:T(8,128)(2,1)S(1)}, u32[]{:S(2)}, u32[]{:S(2)}) collective-permute-start(bf16[64,2048]{1,0:T(8,128)(2,1)} %source_ref.1), channel_id=1, source_target_pairs={{0,1},{1,0},{2,3},{3,2},{4,5},{5,4},{6,7},{7,6},{8,9},{9,8},{10,11... | collective-permute-start | bytes 786440 | tf_op jit(solution)/shard_map/ppermute | solution.py:412
  22.3 54.7 %collective-permute-start.6 = (bf16[2048,256]{1,0:T(8,128)(2,1)}, bf16[2048,256]{1,0:T(8,128)(2,1)}, u32[]{:S(2)}, u32[]{:S(2)}) collective-permute-start(bf16[2048,256]{1,0:T(8,128)(2,1)} %bitcast.26), channel_id=1, source_target_pairs={{0,14},{1,3},{2,0},{3,5},{4,2},{5,7},{6,4},{7,9},{8,6},{9,11},{10,... | collective-permute-start | bytes 3145736 | tf_op jit(solution)/shard_map/ppermute | solution.py:405
  24.2 23.8 %all-to-all-start = ((bf16[64,8,128]{2,1,0:T(8,128)(2,1)}), bf16[64,8,128]{2,1,0:T(8,128)(2,1)S(1)}, u32[]{:S(2)}, u32[]{:S(2)}) async-start(bf16[64,8,128]{2,1,0:T(8,128)(2,1)} %bitcast.9), calls=%async_computation | async-start | bytes 262144 | tf_op jit(solution)/shard_map/all_to_all | solution.py:21
  36.9 53.7 %collective-permute-start.8 = (bf16[448,2048]{1,0:T(8,128)(2,1)S(1)}, bf16[448,2048]{1,0:T(8,128)(2,1)}, u32[]{:S(2)}, u32[]{:S(2)}) collective-permute-start(bf16[448,2048]{1,0:T(8,128)(2,1)S(1)} %shard_map.140.refs_8_), channel_id=1, source_target_pairs={{0,1},{1,0},{2,3},{3,2},{4,5},{5,4},{6,7},{7,6},{8,9},{9,8},{10,11... | collective-permute-start | bytes 5505032 | tf_op jit(solution)/shard_map/ppermute | solution.py:406
  39.3 69.2 %collective-permute-start.10 = (bf16[448,2048]{1,0:T(8,128)(2,1)}, bf16[448,2048]{1,0:T(8,128)(2,1)}, u32[]{:S(2)}, u32[]{:S(2)}) collective-permute-start(bf16[448,2048]{1,0:T(8,128)(2,1)} %collective-permute-done.9.refs_10_), channel_id=1, source_target_pairs={{0,1},{1,0},{2,3},{3,2},{4,5},{5,4},{6,7},{7,6},{8,9},{9,8},{10,11... | collective-permute-start | bytes 5505032 | tf_op jit(solution)/shard_map/ppermute | solution.py:407
  66.7 17.0 %all-to-all-start.2 = ((bf16[64,8,128]{2,1,0:T(8,128)(2,1)}), bf16[64,8,128]{2,1,0:T(8,128)(2,1)S(1)}, u32[]{:S(2)}, u32[]{:S(2)}) async-start(bf16[64,8,128]{2,1,0:T(8,128)(2,1)} %get-tuple-element.14), calls=%async_computation.2 | async-start | bytes 262144 | tf_op jit(solution)/shard_map/all_to_all | solution.py:21
  72.6 18.0 %collective-permute-start.5 = (bf16[2048,256]{1,0:T(8,128)(2,1)}, bf16[2048,256]{1,0:T(8,128)(2,1)}, u32[]{:S(2)}, u32[]{:S(2)}) collective-permute-start(bf16[2048,256]{1,0:T(8,128)(2,1)} %bitcast.27), channel_id=1, source_target_pairs={{0,1},{1,0},{2,3},{3,2},{4,5},{5,4},{6,7},{7,6},{8,9},{9,8},{10,11... | collective-permute-start | bytes 3145736 | tf_op jit(solution)/shard_map/ppermute | solution.py:406
  75.0 33.5 %collective-permute-start.4 = (bf16[2048,256]{1,0:T(8,128)(2,1)}, bf16[2048,256]{1,0:T(8,128)(2,1)}, u32[]{:S(2)}, u32[]{:S(2)}) collective-permute-start(bf16[2048,256]{1,0:T(8,128)(2,1)} %collective-permute-done.3.refs_2_), channel_id=1, source_target_pairs={{0,1},{1,0},{2,3},{3,2},{4,5},{5,4},{6,7},{7,6},{8,9},{9,8},{10,11... | collective-permute-start | bytes 3145736 | tf_op jit(solution)/shard_map/ppermute | solution.py:407
  76.9 31.5 %collective-permute-start.7 = (bf16[2048,256]{1,0:T(8,128)(2,1)}, bf16[2048,256]{1,0:T(8,128)(2,1)}, u32[]{:S(2)}, u32[]{:S(2)}) collective-permute-start(bf16[2048,256]{1,0:T(8,128)(2,1)} %collective-permute-done.6.refs_6_), channel_id=1, source_target_pairs={{0,1},{1,0},{2,3},{3,2},{4,5},{5,4},{6,7},{7,6},{8,9},{9,8},{10,11... | collective-permute-start | bytes 3145736 | tf_op jit(solution)/shard_map/ppermute | solution.py:407
  84.6 23.8 %all-to-all-start.3 = ((bf16[8,16,2,8,128]{4,3,2,1,0:T(8,128)(2,1)}), bf16[8,16,2,8,128]{4,3,2,1,0:T(8,128)(2,1)S(1)}, u32[]{:S(2)}, u32[]{:S(2)}) async-start(bf16[8,16,2,8,128]{4,3,2,1,0:T(8,128)(2,1)} %shard_map.139), calls=%async_computation.3 | async-start | bytes 1048576 | tf_op jit(solution)/shard_map/all_to_all | solution.py:21

commit v8 on v7

--- a/solution.py
+++ b/solution.py
@@ -44,10 +44,16 @@
     weights_ref,
     gain_ref,
     norm_ref,
+    source_ref,
     message_ref,
     slots_ref,
     side_ref,
+    mine_ref,
+    project_ref,
+    landed,
 ):
+    copy = pltpu.make_async_copy(source_ref, project_ref, landed.at[0])
+    copy.start()
     channels, rows = pool_ref.shape
     square = (rows, rows)
     values = pool_ref[...].astype(F32).T.astype(BF16)
@@ -89,7 +95,7 @@
     first_slot = lines[0][0:1] * 16.0 + first_rank
     second_slot = lines[1][0:1] * 16.0 + second_rank
     slots_ref[...] = jnp.concatenate(
-        [first_slot, second_slot, jnp.zeros((6, rows), F32)], axis=0
+        [first_slot, second_slot, docs, jnp.zeros((5, rows), F32)], axis=0
     )
     share = [weights_ref[k : k + 1] for k in (0, 1)]
     line = iota((256, rows), 0)
@@ -119,6 +125,12 @@
     message = message.reshape(32, 8, 128).astype(BF16)
     message_ref[:, 0] = message
     message_ref[:, 1] = message
+    copy.wait()
+    for k in range(8):
+        here = pl.ds(pl.multiple_of(256 * k + 128 * core_ref[0], 128), 128)
+        there = pl.ds(pl.multiple_of(256 * k + 128 - 128 * core_ref[0], 128), 128)
+        mine_ref[64 * k : 64 * (k + 1)] = project_ref[:, here]
+        side_ref[144 + 64 * k : 208 + 64 * k] = project_ref[:, there]
 
 
 def packing(*refs):
@@ -140,20 +152,15 @@
     arrived_ref,
     side_ref,
     other_ref,
-    project_other_ref,
-    docs_ref,
-    source_ref,
+    mine_ref,
+    slots_ref,
     out_ref,
-    project_ref,
-    landed,
 ):
-    copy = pltpu.make_async_copy(source_ref, project_ref, landed.at[0])
-    copy.start()
     rows = channels = 128
     own = index_ref[0]
-    docs = docs_ref[...].astype(F32)
+    docs = slots_ref[2:3]
     first_doc = docs[:, 0:1]
-    sides = side_ref[...].astype(F32) + other_ref[...].astype(F32)
+    sides = side_ref[0:144].astype(F32) + other_ref[0:144].astype(F32)
     values = sides[0:128].astype(BF16)
     gain = sides[128:129] + (sides[129:130] + sides[130:131])
     meta = arrived_ref[:, 0].astype(F32)[:, 3:4]
@@ -213,11 +220,9 @@
     pooled_other = jnp.where(first_core, pooled[:, 64:].astype(F32), pooled[:, :64].astype(F32))
     pooled_own, pooled_other = pooled_own.astype(BF16), pooled_other.astype(BF16)
     tail = jnp.concatenate([sides[131:137], jnp.zeros((2, 128), F32)], axis=0).astype(BF16)
-    copy.wait()
-    for k in range(8):
-        cut = pl.ds(pl.multiple_of(256 * k + 128 * index_ref[1], 128), 128)
-        both = matmul(pooled_own, project_ref[:, cut])
-        both = both + matmul(pooled_other, project_other_ref[:, cut])
+    for k in range(8):
+        both = matmul(pooled_own, mine_ref[64 * k : 64 * (k + 1)])
+        both = both + matmul(pooled_other, other_ref[144 + 64 * k : 208 + 64 * k])
         out_ref[k, 0:128] = both.astype(BF16)
         out_ref[k, 128:136] = tail
 
@@ -379,9 +384,14 @@
     docs = doc_ids.reshape(1, 128)
     core = lax.axis_index("c").astype(jnp.int32)
     index = jnp.stack([lax.axis_index("sp").astype(jnp.int32), core])
-    message, slots, side = kernel(
+    message, slots, side, mine = kernel(
         opening,
-        (array((32, 2, 8, 128), BF16), array((8, 128), F32), array((144, 128), BF16)),
+        (
+            array((32, 2, 8, 128), BF16),
+            array((8, 128), F32),
+            array((656, 128), BF16),
+            array((512, 128), BF16),
+        ),
         (
             core.reshape(1),
             pool_input.T,
@@ -391,7 +401,9 @@
             pool_gain.reshape(1, 64),
             norm_gain.reshape(1, 128),
         ),
+        far=(out_proj,),
         scalars=1,
+        scratch=[pltpu.VMEM((64, 2048), BF16), pltpu.SemaphoreType.DMA((1,))],
     )
     packed = kernel(
         packing,
@@ -409,15 +421,12 @@
     arrived = exchanged(message.reshape(64, 8, 128), ("sp", "c"))
     arrived = arrived.reshape(32, 2, 8, 128)
     other_side = lax.ppermute(side, "c", SWAP)
-    other_project = lax.ppermute(out_proj, "c", SWAP)
     terms = kernel(
         pooling,
         array((8, 136, 128), BF16),
-        (index, docs),
-        near=(arrived, side, other_side, other_project),
-        far=(out_proj,),
+        (index,),
+        near=(arrived, side, other_side, mine, slots),
         scalars=1,
-        scratch=[pltpu.VMEM((64, 2048), BF16), pltpu.SemaphoreType.DMA((1,))],
     )
     terms = exchanged(terms, "y")
     hidden_state, outgoing, gains = kernel(

time: 155 us -> 155 us (level)
    ppermute x1, starting transfers between devices: 6.63 us -> 1.92 us  [body(): other_side = lax.ppermute(side, 'c', SWAP)]
    ppermute x3, starting transfers between devices: 6.65 us -> 10.1 us  [body(): own_other = lax.ppermute(value, 'c', SWAP)]
    all_to_all x3, starting transfers between devices: 24.4 us -> 27.2 us  [exchanged(): return lax.all_to_all(value, axis, split_axis=0, concat_axis=0, tiled=True)]
    ppermute x1 -> x0, starting transfers between devices: 2.41 us -> none  [body(): other_project = lax.ppermute(out_proj, 'c', SWAP)]
  transfers between devices with their start and end apart: 14 -> 13, of which waited for: 3 -> 3; matrix products, arithmetic and copies ran while one was open for 0% -> 0% of each run, Pallas kernels for 4% -> 4%
where the time goes in v8:
time: 155 us; the launch traced here: 154 us
  starting transfers between devices  56.5 us (36%)
  blocking collectives  52.7 us (34%)
  waiting for transfers between devices  28.9 us (19%)
  Pallas kernels  15.9 us (10%)
    all_to_all x3, blocking collectives, exchanged(): return lax.all_to_all(value, axis, split_axis=0, concat_axis=0, tiled=True)  52.7 us
    all_to_all x3, waiting for transfers between devices, exchanged(): return lax.all_to_all(value, axis, split_axis=0, concat_axis=0, tiled=True)  28.8 us
    all_to_all x3, starting transfers between devices, exchanged(): return lax.all_to_all(value, axis, split_axis=0, concat_axis=0, tiled=True)  27.2 us
    pallas_call x8, Pallas kernels, kernel(): pl.pallas_call(body, out_shape=outs, in_specs=[SMEM] * scalars + [VMEM] *...  15.9 us
    ppermute x3, starting transfers between devices, body(): ring = lax.ppermute(value, ('y', 'c'), AROUND)  11 us
    ppermute x3, starting transfers between devices, body(): own_other = lax.ppermute(value, 'c', SWAP)  10.1 us
    ppermute x3, starting transfers between devices, body(): ring_other = lax.ppermute(ring, 'c', SWAP)  6.29 us
  transfers between devices with their start and end apart: 13, of which 3 were waited for; matrix products, arithmetic and copies ran while one was open for 0% of the time, Pallas kernels for 4%

profile of v8, /device:TPU:1, one launch (start us, length us, event | category | flops | bytes accessed | tf_op | source)
XLA Modules:
  0.0 154.3 jit_solution(6263094403332797903)
XLA Ops:
  0.0 1.5 shard_map.140.refs_8_
  1.5 4.2 %collective-permute-start.8 = (bf16[448,2048]{1,0:T(8,128)(2,1)S(1)}, bf16[448,2048]{1,0:T(8,128)(2,1)}, u32[]{:S(2)}, u32[]{:S(2)}) collective-permute-start(bf16[448,2048]{1,0:T(8,128)(2,1)S(1)} %shard_map.140.refs_8_), channel_id=1, source_target_pairs={{0,14},{1,3},{2,0},{3,5},{4,2},{5,7},{6,4},{7,9},{8,6},{9,11},{10,... | collective-permute-start | bytes 5505032 | tf_op jit(solution)/shard_map/ppermute | solution.py:417
  5.7 3.2 %collective-permute-start.2 = (bf16[2048,256]{1,0:T(8,128)(2,1)}, bf16[2048,256]{1,0:T(8,128)(2,1)}, u32[]{:S(2)}, u32[]{:S(2)}) collective-permute-start(bf16[2048,256]{1,0:T(8,128)(2,1)} %bitcast.12.refs_0_), channel_id=1, source_target_pairs={{0,14},{1,3},{2,0},{3,5},{4,2},{5,7},{6,4},{7,9},{8,6},{9,11},{10,... | collective-permute-start | bytes 3145736 | tf_op jit(solution)/shard_map/ppermute | solution.py:417
  8.9 5.4 %collective-permute-start.1 = (bf16[2048,256]{1,0:T(8,128)(2,1)}, bf16[2048,256]{1,0:T(8,128)(2,1)}, u32[]{:S(2)}, u32[]{:S(2)}) collective-permute-start(bf16[2048,256]{1,0:T(8,128)(2,1)} %bitcast.12.refs_0_), channel_id=1, source_target_pairs={{0,1},{1,0},{2,3},{3,2},{4,5},{5,4},{6,7},{7,6},{8,9},{9,8},{10,11... | collective-permute-start | bytes 3145736 | tf_op jit(solution)/shard_map/ppermute | solution.py:418
  14.2 3.6 %collective-permute-start.5 = (bf16[2048,256]{1,0:T(8,128)(2,1)}, bf16[2048,256]{1,0:T(8,128)(2,1)}, u32[]{:S(2)}, u32[]{:S(2)}) collective-permute-start(bf16[2048,256]{1,0:T(8,128)(2,1)} %bitcast.13.refs_4_), channel_id=1, source_target_pairs={{0,14},{1,3},{2,0},{3,5},{4,2},{5,7},{6,4},{7,9},{8,6},{9,11},{10,... | collective-permute-start | bytes 3145736 | tf_op jit(solution)/shard_map/ppermute | solution.py:417
  17.9 2.4 %shard_map.136 = (bf16[32,2,8,128]{3,2,1,0:T(8,128)(2,1)}, f32[8,128]{1,0:T(8,128)S(1)}, bf16[656,128]{1,0:T(8,128)(2,1)S(1)}, bf16[512,128]{1,0:T(8,128)(2,1)S(1)}) custom-call(s32[1]{0:T(128)} %bitcast.core_ref, bf16[64,128]{1,0:T(8,128)(2,1)} %bitcast.25, s32[1,128]{1,0:T(1,128)} %bitcast.28, s32[2,128]{1,0:T(2,128)} %bitcast.26, f32[2,128]{1,0:T(2,128)} %bitcast.27, ...), custom_call_target="tpu_custom_call" | custom-call | tf_op jit(solution)/shard_map/pallas_call | solution.py:352
  20.3 1.9 %collective-permute-start = (bf16[656,128]{1,0:T(8,128)(2,1)S(1)}, bf16[656,128]{1,0:T(8,128)(2,1)S(1)}, u32[]{:S(2)}, u32[]{:S(2)}) collective-permute-start(bf16[656,128]{1,0:T(8,128)(2,1)S(1)} %get-tuple-element.13.side_ref), channel_id=1, source_target_pairs={{0,1},{1,0},{2,3},{3,2},{4,5},{5,4},{6,7},{7,6},{8,9},{9,8},{10,11... | collective-permute-start | bytes 503816 | tf_op jit(solution)/shard_map/ppermute | solution.py:423
  22.3 12.5 %all-to-all-start = ((bf16[64,8,128]{2,1,0:T(8,128)(2,1)}), bf16[64,8,128]{2,1,0:T(8,128)(2,1)S(1)}, u32[]{:S(2)}, u32[]{:S(2)}) async-start(bf16[64,8,128]{2,1,0:T(8,128)(2,1)} %bitcast.9), calls=%async_computation | async-start | bytes 262144 | tf_op jit(solution)/shard_map/all_to_all | solution.py:21
  34.8 2.4 %collective-permute-start.7 = (bf16[448,2048]{1,0:T(8,128)(2,1)S(1)}, bf16[448,2048]{1,0:T(8,128)(2,1)}, u32[]{:S(2)}, u32[]{:S(2)}) collective-permute-start(bf16[448,2048]{1,0:T(8,128)(2,1)S(1)} %shard_map.140.refs_8_), channel_id=1, source_target_pairs={{0,1},{1,0},{2,3},{3,2},{4,5},{5,4},{6,7},{7,6},{8,9},{9,8},{10,11... | collective-permute-start | bytes 5505032 | tf_op jit(solution)/shard_map/ppermute | solution.py:418
  37.2 2.0 %collective-permute-start.9 = (bf16[448,2048]{1,0:T(8,128)(2,1)}, bf16[448,2048]{1,0:T(8,128)(2,1)}, u32[]{:S(2)}, u32[]{:S(2)}) collective-permute-start(bf16[448,2048]{1,0:T(8,128)(2,1)} %collective-permute-done.8.refs_10_), channel_id=1, source_target_pairs={{0,1},{1,0},{2,3},{3,2},{4,5},{5,4},{6,7},{7,6},{8,9},{9,8},{10,11... | collective-permute-start | bytes 5505032 | tf_op jit(solution)/shard_map/ppermute | solution.py:419
  39.2 6.6 %all-to-all-done = bf16[64,8,128]{2,1,0:T(8,128)(2,1)S(1)} async-done(((bf16[64,8,128]{2,1,0:T(8,128)(2,1)}), bf16[64,8,128]{2,1,0:T(8,128)(2,1)S(1)}, u32[]{:S(2)}, u32[]{:S(2)}) %all-to-all-start) | async-done | bytes 131104 | tf_op jit(solution)/shard_map/all_to_all | solution.py:21
  45.9 1.6 %shard_map.137 = bf16[8,136,128]{2,1,0:T(8,128)(2,1)S(1)} custom-call(s32[2]{0:T(128)S(1)} %pad_add_fusion.1.index_ref, bf16[32,2,8,128]{3,2,1,0:T(8,128)(2,1)S(1)} %bitcast.18, bf16[656,128]{1,0:T(8,128)(2,1)S(1)} %get-tuple-element.13.side_ref, bf16[656,128]{1,0:T(8,128)(2,1)S(1)} %collective-permute-done.other_ref, ...), custom_call_target="tpu_custom_call" | custom-call | tf_op jit(solution)/shard_map/pallas_call | solution.py:352
  47.4 15.4 %all_to_all.30.arrived_ref = bf16[8,136,128]{2,1,0:T(8,128)(2,1)S(1)} all-to-all(bf16[8,136,128]{2,1,0:T(8,128)(2,1)S(1)} %shard_map.137), channel_id=1, replica_groups=mesh['sp'=32,'y'=8,'c'=2] {'y'}, dimensions={0} | all-to-all | bytes 557056 | tf_op jit(solution)/shard_map/all_to_all | solution.py:21
  63.7 8.7 %all-to-all-start.2 = ((bf16[64,8,128]{2,1,0:T(8,128)(2,1)}), bf16[64,8,128]{2,1,0:T(8,128)(2,1)S(1)}, u32[]{:S(2)}, u32[]{:S(2)}) async-start(bf16[64,8,128]{2,1,0:T(8,128)(2,1)} %get-tuple-element.16), calls=%async_computation.2 | async-start | bytes 262144 | tf_op jit(solution)/shard_map/all_to_all | solution.py:21
  72.4 2.4 %collective-permute-start.4 = (bf16[2048,256]{1,0:T(8,128)(2,1)}, bf16[2048,256]{1,0:T(8,128)(2,1)}, u32[]{:S(2)}, u32[]{:S(2)}) collective-permute-start(bf16[2048,256]{1,0:T(8,128)(2,1)} %bitcast.13.refs_4_), channel_id=1, source_target_pairs={{0,1},{1,0},{2,3},{3,2},{4,5},{5,4},{6,7},{7,6},{8,9},{9,8},{10,11... | collective-permute-start | bytes 3145736 | tf_op jit(solution)/shard_map/ppermute | solution.py:418
  74.8 2.0 %collective-permute-start.3 = (bf16[2048,256]{1,0:T(8,128)(2,1)}, bf16[2048,256]{1,0:T(8,128)(2,1)}, u32[]{:S(2)}, u32[]{:S(2)}) collective-permute-start(bf16[2048,256]{1,0:T(8,128)(2,1)} %collective-permute-done.2.refs_2_), channel_id=1, source_target_pairs={{0,1},{1,0},{2,3},{3,2},{4,5},{5,4},{6,7},{7,6},{8,9},{9,8},{10,11... | collective-permute-start | bytes 3145736 | tf_op jit(solution)/shard_map/ppermute | solution.py:419
  76.8 2.4 %collective-permute-start.6 = (bf16[2048,256]{1,0:T(8,128)(2,1)}, bf16[2048,256]{1,0:T(8,128)(2,1)}, u32[]{:S(2)}, u32[]{:S(2)}) collective-permute-start(bf16[2048,256]{1,0:T(8,128)(2,1)} %collective-permute-done.5.refs_6_), channel_id=1, source_target_pairs={{0,1},{1,0},{2,3},{3,2},{4,5},{5,4},{6,7},{7,6},{8,9},{9,8},{10,11... | collective-permute-start | bytes 3145736 | tf_op jit(solution)/shard_map/ppermute | solution.py:419
  79.1 4.3 %all-to-all-done.2 = bf16[64,8,128]{2,1,0:T(8,128)(2,1)S(1)} async-done(((bf16[64,8,128]{2,1,0:T(8,128)(2,1)}), bf16[64,8,128]{2,1,0:T(8,128)(2,1)S(1)}, u32[]{:S(2)}, u32[]{:S(2)}) %all-to-all-start.2) | async-done | bytes 131104 | tf_op jit(solution)/shard_map/all_to_all | solution.py:21
  84.4 6.0 %all-to-all-start.3 = ((bf16[8,16,2,8,128]{4,3,2,1,0:T(8,128)(2,1)}), bf16[8,16,2,8,128]{4,3,2,1,0:T(8,128)(2,1)S(1)}, u32[]{:S(2)}, u32[]{:S(2)}) async-start(bf16[8,16,2,8,128]{4,3,2,1,0:T(8,128)(2,1)} %shard_map.139), calls=%async_computation.3 | async-start | bytes 1048576 | tf_op jit(solution)/shard_map/all_to_all | solution.py:21
  90.4 17.9 %all-to-all-done.3.x_ref = bf16[8,16,2,8,128]{4,3,2,1,0:T(8,128)(2,1)S(1)} async-done(((bf16[8,16,2,8,128]{4,3,2,1,0:T(8,128)(2,1)}), bf16[8,16,2,8,128]{4,3,2,1,0:T(8,128)(2,1)S(1)}, u32[]{:S(2)}, u32[]{:S(2)}) %all-to-all-start.3) | async-done | bytes 524320 | tf_op jit(solution)/shard_map/all_to_all | solution.py:21
  108.3 7.7 %shard_map.141 = bf16[8,16,2,8,128]{4,3,2,1,0:T(8,128)(2,1)S(1)} custom-call(s32[2]{0:T(128)S(1)} %pad_add_fusion.place_ref, bf16[8,16,2,8,128]{4,3,2,1,0:T(8,128)(2,1)S(1)} %all-to-all-done.3.x_ref, bf16[32,2,8,128]{3,2,1,0:T(8,128)(2,1)S(1)} %bitcast.19, f32[16,128]{1,0:T(8,128)S(1)} %get-tuple-element.17.gain_ref, bf16[2048,256]{1,0:T(8,128)(2,1)} %bitcast.12.refs_0_, ...), custom_call_target="tpu_custom_call" | custom-call | tf_op jit(solution)/shard_map/pallas_call | solution.py:352
  116.0 20.2 %all_to_all.31.arrived_ref = bf16[8,16,2,8,128]{4,3,2,1,0:T(8,128)(2,1)S(1)} all-to-all(bf16[8,16,2,8,128]{4,3,2,1,0:T(8,128)(2,1)S(1)} %shard_map.141), channel_id=1, replica_groups=mesh['sp'=32,'y'=8,'c'=2] {'y'}, dimensions={0} | all-to-all | bytes 1048576 | tf_op jit(solution)/shard_map/all_to_all | solution.py:21
  136.3 17.1 %all_to_all.32.arrived_ref = bf16[64,8,128]{2,1,0:T(8,128)(2,1)S(1)} all-to-all(bf16[64,8,128]{2,1,0:T(8,128)(2,1)S(1)} %bitcast.21), channel_id=1, replica_groups=mesh['sp'=32,'y'=8,'c'=2] {'sp','c'}, dimensions={0} | all-to-all | bytes 262144 | tf_op jit(solution)/shard_map/all_to_all | solution.py:21
  153.4 0.9 shard_map.143
  (19 shorter events, 2.0 us)
Async XLA Ops:
  1.5 82.9 %copy-start = (bf16[448,2048]{1,0:T(8,128)(2,1)}, bf16[448,2048]{1,0:T(8,128)(2,1)S(1)}, u32[]{:S(2)}) copy-start(bf16[448,2048]{1,0:T(8,128)(2,1)S(1)} %shard_map.140.refs_8_) | copy-start | bytes 5505028
  1.5 61.3 %copy-start.1 = (bf16[128,128]{1,0:T(8,128)(2,1)S(1)}, bf16[128,128]{1,0:T(8,128)(2,1)}, u32[]{:S(2)}) copy-start(bf16[128,128]{1,0:T(8,128)(2,1)} %residual_ref.1) | copy-start | bytes 98308
  1.5 35.7 %collective-permute-start.8 = (bf16[448,2048]{1,0:T(8,128)(2,1)S(1)}, bf16[448,2048]{1,0:T(8,128)(2,1)}, u32[]{:S(2)}, u32[]{:S(2)}) collective-permute-start(bf16[448,2048]{1,0:T(8,128)(2,1)S(1)} %shard_map.140.refs_8_), channel_id=1, source_target_pairs={{0,14},{1,3},{2,0},{3,5},{4,2},{5,7},{6,4},{7,9},{8,6},{9,11},{10,... | collective-permute-start | bytes 5505032 | tf_op jit(solution)/shard_map/ppermute | solution.py:417
  5.7 66.7 %collective-permute-start.2 = (bf16[2048,256]{1,0:T(8,128)(2,1)}, bf16[2048,256]{1,0:T(8,128)(2,1)}, u32[]{:S(2)}, u32[]{:S(2)}) collective-permute-start(bf16[2048,256]{1,0:T(8,128)(2,1)} %bitcast.12.refs_0_), channel_id=1, source_target_pairs={{0,14},{1,3},{2,0},{3,5},{4,2},{5,7},{6,4},{7,9},{8,6},{9,11},{10,... | collective-permute-start | bytes 3145736 | tf_op jit(solution)/shard_map/ppermute | solution.py:417
  8.9 65.9 %collective-permute-start.1 = (bf16[2048,256]{1,0:T(8,128)(2,1)}, bf16[2048,256]{1,0:T(8,128)(2,1)}, u32[]{:S(2)}, u32[]{:S(2)}) collective-permute-start(bf16[2048,256]{1,0:T(8,128)(2,1)} %bitcast.12.refs_0_), channel_id=1, source_target_pairs={{0,1},{1,0},{2,3},{3,2},{4,5},{5,4},{6,7},{7,6},{8,9},{9,8},{10,11... | collective-permute-start | bytes 3145736 | tf_op jit(solution)/shard_map/ppermute | solution.py:418
  14.2 62.5 %collective-permute-start.5 = (bf16[2048,256]{1,0:T(8,128)(2,1)}, bf16[2048,256]{1,0:T(8,128)(2,1)}, u32[]{:S(2)}, u32[]{:S(2)}) collective-permute-start(bf16[2048,256]{1,0:T(8,128)(2,1)} %bitcast.13.refs_4_), channel_id=1, source_target_pairs={{0,14},{1,3},{2,0},{3,5},{4,2},{5,7},{6,4},{7,9},{8,6},{9,11},{10,... | collective-permute-start | bytes 3145736 | tf_op jit(solution)/shard_map/ppermute | solution.py:417
  20.3 14.5 %collective-permute-start = (bf16[656,128]{1,0:T(8,128)(2,1)S(1)}, bf16[656,128]{1,0:T(8,128)(2,1)S(1)}, u32[]{:S(2)}, u32[]{:S(2)}) collective-permute-start(bf16[656,128]{1,0:T(8,128)(2,1)S(1)} %get-tuple-element.13.side_ref), channel_id=1, source_target_pairs={{0,1},{1,0},{2,3},{3,2},{4,5},{5,4},{6,7},{7,6},{8,9},{9,8},{10,11... | collective-permute-start | bytes 503816 | tf_op jit(solution)/shard_map/ppermute | solution.py:423
  22.3 23.6 %all-to-all-start = ((bf16[64,8,128]{2,1,0:T(8,128)(2,1)}), bf16[64,8,128]{2,1,0:T(8,128)(2,1)S(1)}, u32[]{:S(2)}, u32[]{:S(2)}) async-start(bf16[64,8,128]{2,1,0:T(8,128)(2,1)} %bitcast.9), calls=%async_computation | async-start | bytes 262144 | tf_op jit(solution)/shard_map/all_to_all | solution.py:21
  34.8 55.6 %collective-permute-start.7 = (bf16[448,2048]{1,0:T(8,128)(2,1)S(1)}, bf16[448,2048]{1,0:T(8,128)(2,1)}, u32[]{:S(2)}, u32[]{:S(2)}) collective-permute-start(bf16[448,2048]{1,0:T(8,128)(2,1)S(1)} %shard_map.140.refs_8_), channel_id=1, source_target_pairs={{0,1},{1,0},{2,3},{3,2},{4,5},{5,4},{6,7},{7,6},{8,9},{9,8},{10,11... | collective-permute-start | bytes 5505032 | tf_op jit(solution)/shard_map/ppermute | solution.py:418
  37.2 71.1 %collective-permute-start.9 = (bf16[448,2048]{1,0:T(8,128)(2,1)}, bf16[448,2048]{1,0:T(8,128)(2,1)}, u32[]{:S(2)}, u32[]{:S(2)}) collective-permute-start(bf16[448,2048]{1,0:T(8,128)(2,1)} %collective-permute-done.8.refs_10_), channel_id=1, source_target_pairs={{0,1},{1,0},{2,3},{3,2},{4,5},{5,4},{6,7},{7,6},{8,9},{9,8},{10,11... | collective-permute-start | bytes 5505032 | tf_op jit(solution)/shard_map/ppermute | solution.py:419
  63.7 19.8 %all-to-all-start.2 = ((bf16[64,8,128]{2,1,0:T(8,128)(2,1)}), bf16[64,8,128]{2,1,0:T(8,128)(2,1)S(1)}, u32[]{:S(2)}, u32[]{:S(2)}) async-start(bf16[64,8,128]{2,1,0:T(8,128)(2,1)} %get-tuple-element.16), calls=%async_computation.2 | async-start | bytes 262144 | tf_op jit(solution)/shard_map/all_to_all | solution.py:21
  72.4 18.0 %collective-permute-start.4 = (bf16[2048,256]{1,0:T(8,128)(2,1)}, bf16[2048,256]{1,0:T(8,128)(2,1)}, u32[]{:S(2)}, u32[]{:S(2)}) collective-permute-start(bf16[2048,256]{1,0:T(8,128)(2,1)} %bitcast.13.refs_4_), channel_id=1, source_target_pairs={{0,1},{1,0},{2,3},{3,2},{4,5},{5,4},{6,7},{7,6},{8,9},{9,8},{10,11... | collective-permute-start | bytes 3145736 | tf_op jit(solution)/shard_map/ppermute | solution.py:418
  74.8 33.5 %collective-permute-start.3 = (bf16[2048,256]{1,0:T(8,128)(2,1)}, bf16[2048,256]{1,0:T(8,128)(2,1)}, u32[]{:S(2)}, u32[]{:S(2)}) collective-permute-start(bf16[2048,256]{1,0:T(8,128)(2,1)} %collective-permute-done.2.refs_2_), channel_id=1, source_target_pairs={{0,1},{1,0},{2,3},{3,2},{4,5},{5,4},{6,7},{7,6},{8,9},{9,8},{10,11... | collective-permute-start | bytes 3145736 | tf_op jit(solution)/shard_map/ppermute | solution.py:419
  76.8 31.5 %collective-permute-start.6 = (bf16[2048,256]{1,0:T(8,128)(2,1)}, bf16[2048,256]{1,0:T(8,128)(2,1)}, u32[]{:S(2)}, u32[]{:S(2)}) collective-permute-start(bf16[2048,256]{1,0:T(8,128)(2,1)} %collective-permute-done.5.refs_6_), channel_id=1, source_target_pairs={{0,1},{1,0},{2,3},{3,2},{4,5},{5,4},{6,7},{7,6},{8,9},{9,8},{10,11... | collective-permute-start | bytes 3145736 | tf_op jit(solution)/shard_map/ppermute | solution.py:419
  84.4 23.9 %all-to-all-start.3 = ((bf16[8,16,2,8,128]{4,3,2,1,0:T(8,128)(2,1)}), bf16[8,16,2,8,128]{4,3,2,1,0:T(8,128)(2,1)S(1)}, u32[]{:S(2)}, u32[]{:S(2)}) async-start(bf16[8,16,2,8,128]{4,3,2,1,0:T(8,128)(2,1)} %shard_map.139), calls=%async_computation.3 | async-start | bytes 1048576 | tf_op jit(solution)/shard_map/all_to_all | solution.py:21

commit v9 on v8

--- a/solution.py
+++ b/solution.py
@@ -248,14 +248,14 @@
         out_ref[k] = arrived_ref[:, k % 2]
 
 
-def experts(place_ref, x_ref, message_ref, gain_ref, *refs):
-    sources, out_ref, normed_ref, sum_ref = refs[:12], refs[12], refs[13], refs[14]
-    near, landed = refs[15:27], refs[27]
-    gates, ups, lowers = near[0:4], near[4:8], near[8:12]
+def experts(place_ref, x_ref, message_ref, gain_ref, gate_ref, *refs):
+    sources, out_ref, normed_ref, sum_ref = refs[:11], refs[11], refs[12], refs[13]
+    near, landed = refs[14:25], refs[25]
+    gates, ups, lowers = (gate_ref, *near[0:3]), near[3:7], near[7:11]
     copies = [
-        pltpu.make_async_copy(sources[k], near[k], landed.at[k]) for k in range(12)
+        pltpu.make_async_copy(sources[k], near[k], landed.at[k]) for k in range(11)
     ]
-    for k in (0, 4, 1, 5, 2, 6, 8, 9, 10, 11, 3, 7):
+    for k in (3, 0, 4, 1, 5, 7, 8, 9, 10, 2, 6):
         copies[k].start()
 
     squares = jnp.zeros((128, 128), F32)
@@ -277,14 +277,15 @@
     normed = normed_ref[...]
 
     def hidden(k):
-        copies[k].wait()
-        copies[k + 4].wait()
+        if k > 0:
+            copies[k - 1].wait()
+        copies[k + 3].wait()
         lower = matmul(normed, gates[k][...])
         upper = matmul(normed, ups[k][...])
         return (jax.nn.silu(lower) * upper * weight).astype(BF16)
 
     early = [hidden(k) for k in range(3)]
-    for copy in copies[8:]:
+    for copy in copies[7:]:
         copy.wait()
     across = jnp.concatenate(
         [pack[256:320] for pack in lowers] + [pack[320:384] for pack in lowers], axis=0
@@ -445,12 +446,12 @@
         experts,
         array((8, 16, 2, 8, 128), BF16),
         (place,),
-        near=(rows, arrived, gains),
-        far=groups,
+        near=(rows, arrived, gains, groups[0]),
+        far=groups[1:],
         scalars=1,
         scratch=[pltpu.VMEM((128, 2048), BF16), pltpu.VMEM((8, 128, 256), F32)]
-        + [pltpu.VMEM(value.shape, BF16) for value in groups]
-        + [pltpu.SemaphoreType.DMA((12,))],
+        + [pltpu.VMEM(value.shape, BF16) for value in groups[1:]]
+        + [pltpu.SemaphoreType.DMA((11,))],
         room=24,
     )
     parts = exchanged(parts, "y")

time: 155 us -> 156 us (level)
  local copies, waits for them, and re-layouts: 0.01 us -> 2.22 us
    unnamed x4 -> x14, local copies, waits for them, and re-layouts: 0.01 us -> 2.22 us
where the time goes in v9:
time: 156 us; the launch traced here: 155 us
  starting transfers between devices  55.9 us (36%)
  blocking collectives  52.5 us (34%)
  waiting for transfers between devices  28.2 us (18%)
  Pallas kernels  15.7 us (10%)
  local copies, waits for them, and re-layouts  2.22 us (1%)
    all_to_all x3, blocking collectives, exchanged(): return lax.all_to_all(value, axis, split_axis=0, concat_axis=0, tiled=True)  52.5 us
    all_to_all x3, waiting for transfers between devices, exchanged(): return lax.all_to_all(value, axis, split_axis=0, concat_axis=0, tiled=True)  28.1 us
    all_to_all x3, starting transfers between devices, exchanged(): return lax.all_to_all(value, axis, split_axis=0, concat_axis=0, tiled=True)  26.6 us
    pallas_call x8, Pallas kernels, kernel(): pl.pallas_call(body, out_shape=outs, in_specs=[SMEM] * scalars + [VMEM] *...  15.7 us
    ppermute x3, starting transfers between devices, body(): ring = lax.ppermute(value, ('y', 'c'), AROUND)  11 us
    ppermute x3, starting transfers between devices, body(): own_other = lax.ppermute(value, 'c', SWAP)  10.1 us
    ppermute x3, starting transfers between devices, body(): ring_other = lax.ppermute(ring, 'c', SWAP)  6.29 us
  transfers between devices with their start and end apart: 13, of which 3 were waited for; matrix products, arithmetic and copies ran while one was open for 0% of the time, Pallas kernels for 4%

profile of v9, /device:TPU:1, one launch (start us, length us, event | category | flops | bytes accessed | tf_op | source)
XLA Modules:
  0.0 154.9 jit_solution(6231264521908613691)
XLA Ops:
  0.0 1.5 shard_map.140.refs_7_
  1.6 4.2 %collective-permute-start.8 = (bf16[448,2048]{1,0:T(8,128)(2,1)S(1)}, bf16[448,2048]{1,0:T(8,128)(2,1)}, u32[]{:S(2)}, u32[]{:S(2)}) collective-permute-start(bf16[448,2048]{1,0:T(8,128)(2,1)S(1)} %shard_map.140.refs_7_), channel_id=1, source_target_pairs={{0,14},{1,3},{2,0},{3,5},{4,2},{5,7},{6,4},{7,9},{8,6},{9,11},{10,... | collective-permute-start | bytes 5505032 | tf_op jit(solution)/shard_map/ppermute | solution.py:418
  5.8 3.2 %collective-permute-start.2 = (bf16[2048,256]{1,0:T(8,128)(2,1)S(1)}, bf16[2048,256]{1,0:T(8,128)(2,1)}, u32[]{:S(2)}, u32[]{:S(2)}) collective-permute-start(bf16[2048,256]{1,0:T(8,128)(2,1)S(1)} %bitcast.20), channel_id=1, source_target_pairs={{0,14},{1,3},{2,0},{3,5},{4,2},{5,7},{6,4},{7,9},{8,6},{9,11},{10,... | collective-permute-start | bytes 3145736 | tf_op jit(solution)/shard_map/ppermute | solution.py:418
  9.0 5.4 %collective-permute-start.1 = (bf16[2048,256]{1,0:T(8,128)(2,1)S(1)}, bf16[2048,256]{1,0:T(8,128)(2,1)}, u32[]{:S(2)}, u32[]{:S(2)}) collective-permute-start(bf16[2048,256]{1,0:T(8,128)(2,1)S(1)} %bitcast.21), channel_id=1, source_target_pairs={{0,1},{1,0},{2,3},{3,2},{4,5},{5,4},{6,7},{7,6},{8,9},{9,8},{10,11... | collective-permute-start | bytes 3145736 | tf_op jit(solution)/shard_map/ppermute | solution.py:419
  14.3 3.6 %collective-permute-start.5 = (bf16[2048,256]{1,0:T(8,128)(2,1)}, bf16[2048,256]{1,0:T(8,128)(2,1)}, u32[]{:S(2)}, u32[]{:S(2)}) collective-permute-start(bf16[2048,256]{1,0:T(8,128)(2,1)} %bitcast.13.refs_3_), channel_id=1, source_target_pairs={{0,14},{1,3},{2,0},{3,5},{4,2},{5,7},{6,4},{7,9},{8,6},{9,11},{10,... | collective-permute-start | bytes 3145736 | tf_op jit(solution)/shard_map/ppermute | solution.py:418
  18.0 2.5 %shard_map.136 = (bf16[32,2,8,128]{3,2,1,0:T(8,128)(2,1)}, f32[8,128]{1,0:T(8,128)S(1)}, bf16[656,128]{1,0:T(8,128)(2,1)S(1)}, bf16[512,128]{1,0:T(8,128)(2,1)S(1)}) custom-call(s32[1]{0:T(128)} %bitcast.core_ref, bf16[64,128]{1,0:T(8,128)(2,1)} %bitcast.28, s32[1,128]{1,0:T(1,128)} %bitcast.31, s32[2,128]{1,0:T(2,128)} %bitcast.29, f32[2,128]{1,0:T(2,128)} %bitcast.30, ...), custom_call_target="tpu_custom_call" | custom-call | tf_op jit(solution)/shard_map/pallas_call | solution.py:353
  20.5 1.9 %collective-permute-start = (bf16[656,128]{1,0:T(8,128)(2,1)S(1)}, bf16[656,128]{1,0:T(8,128)(2,1)S(1)}, u32[]{:S(2)}, u32[]{:S(2)}) collective-permute-start(bf16[656,128]{1,0:T(8,128)(2,1)S(1)} %get-tuple-element.13.side_ref), channel_id=1, source_target_pairs={{0,1},{1,0},{2,3},{3,2},{4,5},{5,4},{6,7},{7,6},{8,9},{9,8},{10,11... | collective-permute-start | bytes 503816 | tf_op jit(solution)/shard_map/ppermute | solution.py:424
  22.4 12.5 %all-to-all-start = ((bf16[64,8,128]{2,1,0:T(8,128)(2,1)}), bf16[64,8,128]{2,1,0:T(8,128)(2,1)S(1)}, u32[]{:S(2)}, u32[]{:S(2)}) async-start(bf16[64,8,128]{2,1,0:T(8,128)(2,1)} %bitcast.9), calls=%async_computation | async-start | bytes 262144 | tf_op jit(solution)/shard_map/all_to_all | solution.py:21
  35.6 2.4 %collective-permute-start.7 = (bf16[448,2048]{1,0:T(8,128)(2,1)S(1)}, bf16[448,2048]{1,0:T(8,128)(2,1)}, u32[]{:S(2)}, u32[]{:S(2)}) collective-permute-start(bf16[448,2048]{1,0:T(8,128)(2,1)S(1)} %shard_map.140.refs_7_), channel_id=1, source_target_pairs={{0,1},{1,0},{2,3},{3,2},{4,5},{5,4},{6,7},{7,6},{8,9},{9,8},{10,11... | collective-permute-start | bytes 5505032 | tf_op jit(solution)/shard_map/ppermute | solution.py:419
  38.0 2.0 %collective-permute-start.9 = (bf16[448,2048]{1,0:T(8,128)(2,1)}, bf16[448,2048]{1,0:T(8,128)(2,1)}, u32[]{:S(2)}, u32[]{:S(2)}) collective-permute-start(bf16[448,2048]{1,0:T(8,128)(2,1)} %collective-permute-done.8.refs_9_), channel_id=1, source_target_pairs={{0,1},{1,0},{2,3},{3,2},{4,5},{5,4},{6,7},{7,6},{8,9},{9,8},{10,11... | collective-permute-start | bytes 5505032 | tf_op jit(solution)/shard_map/ppermute | solution.py:420
  40.0 5.9 %all-to-all-done = bf16[64,8,128]{2,1,0:T(8,128)(2,1)S(1)} async-done(((bf16[64,8,128]{2,1,0:T(8,128)(2,1)}), bf16[64,8,128]{2,1,0:T(8,128)(2,1)S(1)}, u32[]{:S(2)}, u32[]{:S(2)}) %all-to-all-start) | async-done | bytes 131104 | tf_op jit(solution)/shard_map/all_to_all | solution.py:21
  46.8 1.6 %shard_map.137 = bf16[8,136,128]{2,1,0:T(8,128)(2,1)S(1)} custom-call(s32[2]{0:T(128)S(1)} %pad_add_fusion.1.index_ref, bf16[32,2,8,128]{3,2,1,0:T(8,128)(2,1)S(1)} %bitcast.18, bf16[656,128]{1,0:T(8,128)(2,1)S(1)} %get-tuple-element.13.side_ref, bf16[656,128]{1,0:T(8,128)(2,1)S(1)} %copy-done.3, bf16[512,128]{1,0:T(8,128)(2,1)S(1)} %get-tuple-element.14.mine_ref, ...), custom_call_target="tpu_custom_call" | custom-call | tf_op jit(solution)/shard_map/pallas_call | solution.py:353
  48.4 15.1 %all_to_all.30.arrived_ref = bf16[8,136,128]{2,1,0:T(8,128)(2,1)S(1)} all-to-all(bf16[8,136,128]{2,1,0:T(8,128)(2,1)S(1)} %shard_map.137), channel_id=1, replica_groups=mesh['sp'=32,'y'=8,'c'=2] {'y'}, dimensions={0} | all-to-all | bytes 557056 | tf_op jit(solution)/shard_map/all_to_all | solution.py:21
  65.0 8.2 %all-to-all-start.2 = ((bf16[64,8,128]{2,1,0:T(8,128)(2,1)}), bf16[64,8,128]{2,1,0:T(8,128)(2,1)S(1)}, u32[]{:S(2)}, u32[]{:S(2)}) async-start(bf16[64,8,128]{2,1,0:T(8,128)(2,1)} %get-tuple-element.16), calls=%async_computation.2 | async-start | bytes 262144 | tf_op jit(solution)/shard_map/all_to_all | solution.py:21
  73.2 2.4 %collective-permute-start.4 = (bf16[2048,256]{1,0:T(8,128)(2,1)}, bf16[2048,256]{1,0:T(8,128)(2,1)}, u32[]{:S(2)}, u32[]{:S(2)}) collective-permute-start(bf16[2048,256]{1,0:T(8,128)(2,1)} %bitcast.13.refs_3_), channel_id=1, source_target_pairs={{0,1},{1,0},{2,3},{3,2},{4,5},{5,4},{6,7},{7,6},{8,9},{9,8},{10,11... | collective-permute-start | bytes 3145736 | tf_op jit(solution)/shard_map/ppermute | solution.py:419
  75.6 2.0 %collective-permute-start.3 = (bf16[2048,256]{1,0:T(8,128)(2,1)}, bf16[2048,256]{1,0:T(8,128)(2,1)}, u32[]{:S(2)}, u32[]{:S(2)}) collective-permute-start(bf16[2048,256]{1,0:T(8,128)(2,1)} %collective-permute-done.2.refs_1_), channel_id=1, source_target_pairs={{0,1},{1,0},{2,3},{3,2},{4,5},{5,4},{6,7},{7,6},{8,9},{9,8},{10,11... | collective-permute-start | bytes 3145736 | tf_op jit(solution)/shard_map/ppermute | solution.py:420
  77.6 2.4 %collective-permute-start.6 = (bf16[2048,256]{1,0:T(8,128)(2,1)}, bf16[2048,256]{1,0:T(8,128)(2,1)}, u32[]{:S(2)}, u32[]{:S(2)}) collective-permute-start(bf16[2048,256]{1,0:T(8,128)(2,1)} %collective-permute-done.5.refs_5_), channel_id=1, source_target_pairs={{0,1},{1,0},{2,3},{3,2},{4,5},{5,4},{6,7},{7,6},{8,9},{9,8},{10,11... | collective-permute-start | bytes 3145736 | tf_op jit(solution)/shard_map/ppermute | solution.py:420
  79.9 4.3 %all-to-all-done.2 = bf16[64,8,128]{2,1,0:T(8,128)(2,1)S(1)} async-done(((bf16[64,8,128]{2,1,0:T(8,128)(2,1)}), bf16[64,8,128]{2,1,0:T(8,128)(2,1)S(1)}, u32[]{:S(2)}, u32[]{:S(2)}) %all-to-all-start.2) | async-done | bytes 131104 | tf_op jit(solution)/shard_map/all_to_all | solution.py:21
  85.2 5.9 %all-to-all-start.3 = ((bf16[8,16,2,8,128]{4,3,2,1,0:T(8,128)(2,1)}), bf16[8,16,2,8,128]{4,3,2,1,0:T(8,128)(2,1)S(1)}, u32[]{:S(2)}, u32[]{:S(2)}) async-start(bf16[8,16,2,8,128]{4,3,2,1,0:T(8,128)(2,1)} %shard_map.139), calls=%async_computation.3 | async-start | bytes 1048576 | tf_op jit(solution)/shard_map/all_to_all | solution.py:21
  91.1 17.9 %all-to-all-done.3.x_ref = bf16[8,16,2,8,128]{4,3,2,1,0:T(8,128)(2,1)S(1)} async-done(((bf16[8,16,2,8,128]{4,3,2,1,0:T(8,128)(2,1)}), bf16[8,16,2,8,128]{4,3,2,1,0:T(8,128)(2,1)S(1)}, u32[]{:S(2)}, u32[]{:S(2)}) %all-to-all-start.3) | async-done | bytes 524320 | tf_op jit(solution)/shard_map/all_to_all | solution.py:21
  109.0 7.4 %shard_map.141 = bf16[8,16,2,8,128]{4,3,2,1,0:T(8,128)(2,1)S(1)} custom-call(s32[2]{0:T(128)S(1)} %pad_add_fusion.place_ref, bf16[8,16,2,8,128]{4,3,2,1,0:T(8,128)(2,1)S(1)} %all-to-all-done.3.x_ref, bf16[32,2,8,128]{3,2,1,0:T(8,128)(2,1)S(1)} %bitcast.19, f32[16,128]{1,0:T(8,128)S(1)} %get-tuple-element.17.gain_ref, bf16[2048,256]{1,0:T(8,128)(2,1)S(1)} %bitcast.22, ...), custom_call_target="tpu_custom_call" | custom-call | tf_op jit(solution)/shard_map/pallas_call | solution.py:353
  116.5 20.4 %all_to_all.31.arrived_ref = bf16[8,16,2,8,128]{4,3,2,1,0:T(8,128)(2,1)S(1)} all-to-all(bf16[8,16,2,8,128]{4,3,2,1,0:T(8,128)(2,1)S(1)} %shard_map.141), channel_id=1, replica_groups=mesh['sp'=32,'y'=8,'c'=2] {'y'}, dimensions={0} | all-to-all | bytes 1048576 | tf_op jit(solution)/shard_map/all_to_all | solution.py:21
  136.9 17.0 %all_to_all.32.arrived_ref = bf16[64,8,128]{2,1,0:T(8,128)(2,1)S(1)} all-to-all(bf16[64,8,128]{2,1,0:T(8,128)(2,1)S(1)} %bitcast.24), channel_id=1, replica_groups=mesh['sp'=32,'y'=8,'c'=2] {'sp','c'}, dimensions={0} | all-to-all | bytes 262144 | tf_op jit(solution)/shard_map/all_to_all | solution.py:21
  153.9 0.9 shard_map.143
  (29 shorter events, 4.2 us)
Async XLA Ops:
  0.0 5.7 %copy-start.1 = (bf16[1,2048,256]{2,1,0:T(8,128)(2,1)S(1)}, bf16[1,2048,256]{2,1,0:T(8,128)(2,1)}, u32[]{:S(2)}) copy-start(bf16[1,2048,256]{2,1,0:T(8,128)(2,1)} %param.22) | copy-start | bytes 3145732
  1.6 83.6 %copy-start = (bf16[448,2048]{1,0:T(8,128)(2,1)}, bf16[448,2048]{1,0:T(8,128)(2,1)S(1)}, u32[]{:S(2)}) copy-start(bf16[448,2048]{1,0:T(8,128)(2,1)S(1)} %shard_map.140.refs_7_) | copy-start | bytes 5505028
  1.6 61.9 %copy-start.6 = (bf16[128,128]{1,0:T(8,128)(2,1)S(1)}, bf16[128,128]{1,0:T(8,128)(2,1)}, u32[]{:S(2)}) copy-start(bf16[128,128]{1,0:T(8,128)(2,1)} %residual_ref.1) | copy-start | bytes 98308
  1.6 36.4 %collective-permute-start.8 = (bf16[448,2048]{1,0:T(8,128)(2,1)S(1)}, bf16[448,2048]{1,0:T(8,128)(2,1)}, u32[]{:S(2)}, u32[]{:S(2)}) collective-permute-start(bf16[448,2048]{1,0:T(8,128)(2,1)S(1)} %shard_map.140.refs_7_), channel_id=1, source_target_pairs={{0,14},{1,3},{2,0},{3,5},{4,2},{5,7},{6,4},{7,9},{8,6},{9,11},{10,... | collective-permute-start | bytes 5505032 | tf_op jit(solution)/shard_map/ppermute | solution.py:418
  5.8 67.4 %collective-permute-start.2 = (bf16[2048,256]{1,0:T(8,128)(2,1)S(1)}, bf16[2048,256]{1,0:T(8,128)(2,1)}, u32[]{:S(2)}, u32[]{:S(2)}) collective-permute-start(bf16[2048,256]{1,0:T(8,128)(2,1)S(1)} %bitcast.20), channel_id=1, source_target_pairs={{0,14},{1,3},{2,0},{3,5},{4,2},{5,7},{6,4},{7,9},{8,6},{9,11},{10,... | collective-permute-start | bytes 3145736 | tf_op jit(solution)/shard_map/ppermute | solution.py:418
  9.0 66.6 %collective-permute-start.1 = (bf16[2048,256]{1,0:T(8,128)(2,1)S(1)}, bf16[2048,256]{1,0:T(8,128)(2,1)}, u32[]{:S(2)}, u32[]{:S(2)}) collective-permute-start(bf16[2048,256]{1,0:T(8,128)(2,1)S(1)} %bitcast.21), channel_id=1, source_target_pairs={{0,1},{1,0},{2,3},{3,2},{4,5},{5,4},{6,7},{7,6},{8,9},{9,8},{10,11... | collective-permute-start | bytes 3145736 | tf_op jit(solution)/shard_map/ppermute | solution.py:419
  14.3 63.2 %collective-permute-start.5 = (bf16[2048,256]{1,0:T(8,128)(2,1)}, bf16[2048,256]{1,0:T(8,128)(2,1)}, u32[]{:S(2)}, u32[]{:S(2)}) collective-permute-start(bf16[2048,256]{1,0:T(8,128)(2,1)} %bitcast.13.refs_3_), channel_id=1, source_target_pairs={{0,14},{1,3},{2,0},{3,5},{4,2},{5,7},{6,4},{7,9},{8,6},{9,11},{10,... | collective-permute-start | bytes 3145736 | tf_op jit(solution)/shard_map/ppermute | solution.py:418
  20.5 14.5 %collective-permute-start = (bf16[656,128]{1,0:T(8,128)(2,1)S(1)}, bf16[656,128]{1,0:T(8,128)(2,1)S(1)}, u32[]{:S(2)}, u32[]{:S(2)}) collective-permute-start(bf16[656,128]{1,0:T(8,128)(2,1)S(1)} %get-tuple-element.13.side_ref), channel_id=1, source_target_pairs={{0,1},{1,0},{2,3},{3,2},{4,5},{5,4},{6,7},{7,6},{8,9},{9,8},{10,11... | collective-permute-start | bytes 503816 | tf_op jit(solution)/shard_map/ppermute | solution.py:424
  22.4 23.5 %all-to-all-start = ((bf16[64,8,128]{2,1,0:T(8,128)(2,1)}), bf16[64,8,128]{2,1,0:T(8,128)(2,1)S(1)}, u32[]{:S(2)}, u32[]{:S(2)}) async-start(bf16[64,8,128]{2,1,0:T(8,128)(2,1)} %bitcast.9), calls=%async_computation | async-start | bytes 262144 | tf_op jit(solution)/shard_map/all_to_all | solution.py:21
  34.9 0.7 copy-start.2
  35.6 55.5 %collective-permute-start.7 = (bf16[448,2048]{1,0:T(8,128)(2,1)S(1)}, bf16[448,2048]{1,0:T(8,128)(2,1)}, u32[]{:S(2)}, u32[]{:S(2)}) collective-permute-start(bf16[448,2048]{1,0:T(8,128)(2,1)S(1)} %shard_map.140.refs_7_), channel_id=1, source_target_pairs={{0,1},{1,0},{2,3},{3,2},{4,5},{5,4},{6,7},{7,6},{8,9},{9,8},{10,11... | collective-permute-start | bytes 5505032 | tf_op jit(solution)/shard_map/ppermute | solution.py:419
  38.0 71.0 %collective-permute-start.9 = (bf16[448,2048]{1,0:T(8,128)(2,1)}, bf16[448,2048]{1,0:T(8,128)(2,1)}, u32[]{:S(2)}, u32[]{:S(2)}) collective-permute-start(bf16[448,2048]{1,0:T(8,128)(2,1)} %collective-permute-done.8.refs_9_), channel_id=1, source_target_pairs={{0,1},{1,0},{2,3},{3,2},{4,5},{5,4},{6,7},{7,6},{8,9},{9,8},{10,11... | collective-permute-start | bytes 5505032 | tf_op jit(solution)/shard_map/ppermute | solution.py:420
  45.9 0.9 copy-start.3
  64.3 0.6 copy-start.4
  65.0 19.3 %all-to-all-start.2 = ((bf16[64,8,128]{2,1,0:T(8,128)(2,1)}), bf16[64,8,128]{2,1,0:T(8,128)(2,1)S(1)}, u32[]{:S(2)}, u32[]{:S(2)}) async-start(bf16[64,8,128]{2,1,0:T(8,128)(2,1)} %get-tuple-element.16), calls=%async_computation.2 | async-start | bytes 262144 | tf_op jit(solution)/shard_map/all_to_all | solution.py:21
  73.2 17.9 %collective-permute-start.4 = (bf16[2048,256]{1,0:T(8,128)(2,1)}, bf16[2048,256]{1,0:T(8,128)(2,1)}, u32[]{:S(2)}, u32[]{:S(2)}) collective-permute-start(bf16[2048,256]{1,0:T(8,128)(2,1)} %bitcast.13.refs_3_), channel_id=1, source_target_pairs={{0,1},{1,0},{2,3},{3,2},{4,5},{5,4},{6,7},{7,6},{8,9},{9,8},{10,11... | collective-permute-start | bytes 3145736 | tf_op jit(solution)/shard_map/ppermute | solution.py:419
  75.6 33.4 %collective-permute-start.3 = (bf16[2048,256]{1,0:T(8,128)(2,1)}, bf16[2048,256]{1,0:T(8,128)(2,1)}, u32[]{:S(2)}, u32[]{:S(2)}) collective-permute-start(bf16[2048,256]{1,0:T(8,128)(2,1)} %collective-permute-done.2.refs_1_), channel_id=1, source_target_pairs={{0,1},{1,0},{2,3},{3,2},{4,5},{5,4},{6,7},{7,6},{8,9},{9,8},{10,11... | collective-permute-start | bytes 3145736 | tf_op jit(solution)/shard_map/ppermute | solution.py:420
  77.6 31.4 %collective-permute-start.6 = (bf16[2048,256]{1,0:T(8,128)(2,1)}, bf16[2048,256]{1,0:T(8,128)(2,1)}, u32[]{:S(2)}, u32[]{:S(2)}) collective-permute-start(bf16[2048,256]{1,0:T(8,128)(2,1)} %collective-permute-done.5.refs_5_), channel_id=1, source_target_pairs={{0,1},{1,0},{2,3},{3,2},{4,5},{5,4},{6,7},{7,6},{8,9},{9,8},{10,11... | collective-permute-start | bytes 3145736 | tf_op jit(solution)/shard_map/ppermute | solution.py:420
  85.2 23.8 %all-to-all-start.3 = ((bf16[8,16,2,8,128]{4,3,2,1,0:T(8,128)(2,1)}), bf16[8,16,2,8,128]{4,3,2,1,0:T(8,128)(2,1)S(1)}, u32[]{:S(2)}, u32[]{:S(2)}) async-start(bf16[8,16,2,8,128]{4,3,2,1,0:T(8,128)(2,1)} %shard_map.139), calls=%async_computation.3 | async-start | bytes 1048576 | tf_op jit(solution)/shard_map/all_to_all | solution.py:21
  116.4 37.5 %copy-start.5 = (f32[128,128]{1,0:T(8,128)S(1)}, f32[128,128]{1,0:T(8,128)}, u32[]{:S(2)}) copy-start(f32[128,128]{1,0:T(8,128)} %copy-done.4) | copy-start | bytes 196612
